TPU v7x, 32 devices: a whole 2x2x4 slice. The times are simulated.
32 devices in a mesh: grp: 2 (over y), kv: 4 (over z), tp: 4 (over x, core).
Axes of the slice: x: 2, y: 2, z: 4, core: 2. Of those that a mesh axis runs over, the one named last changes fastest.
Arguments:
- tokens: bfloat16 [256, 4, 2048], P(('grp', 'kv'), None, 'tp'), parts along dimension 0, may hold values from -6 to 6
- in_gain: float32 [2048], replicated, may hold values from 0.1 to 1.9
- w_query: bfloat16 [2048, 1024], P('kv', 'tp'), may hold values from -0.125 to 0.125
- w_key: bfloat16 [2048, 1024], P('kv', 'tp'), may hold values from -0.125 to 0.125
- w_value: bfloat16 [2048, 1024], P('kv', 'tp'), may hold values from -0.125 to 0.125
- w_gate: bfloat16 [2048, 1024], P('kv', 'tp'), may hold values from -0.125 to 0.125
- w_beta: bfloat16 [2048, 16], replicated, may hold values from -0.125 to 0.125
- w_decay: bfloat16 [2048, 16], replicated, may hold values from -0.125 to 0.125
- decay_base: float32 [16], P('tp'), may hold values from 0.05 to 1
- out_gain: float32 [64], replicated, may hold values from 0.1 to 1.9
- w_out: bfloat16 [1024, 2048], P('tp', 'kv'), may hold values from -0.1875 to 0.1875
- state: float32 [256, 64, 1024], P(('grp', 'kv'), None, 'tp'), parts along dimension 0, may hold values from -0.8 to 0.8
- prev_keys: bfloat16 [256, 4, 1024], P(('grp', 'kv'), None, 'tp'), parts along dimension 0, may hold values from -6 to 6
- prev_values: bfloat16 [256, 4, 1024], P(('grp', 'kv'), None, 'tp'), parts along dimension 0, may hold values from -6 to 6
- prev_beta: float32 [256, 4, 16], P(('grp', 'kv'), None, 'tp'), parts along dimension 0, may hold values from -6 to 6
- prev_decay: float32 [256, 4, 16], P(('grp', 'kv'), None, 'tp'), parts along dimension 0, may hold values from -1 to -0.02
- accepted: int32 [256], P(('grp', 'kv')), parts along dimension 0, may hold values from 0 to 4
Outputs:
- mixed: bfloat16 [256, 4, 2048], P(('grp', 'kv'), None, 'tp'), parts along dimension 0
- new_state: float32 [256, 64, 1024], P(('grp', 'kv'), None, 'tp'), parts along dimension 0
There are 2 independent parts, one for each index of `grp`. A program takes and returns all parts, laid end to end along the dimension named above; an argument that names none is the same for every part. Nothing has to cross between parts.
All inputs are finite; a program needn't handle non-finite values.
Results may differ from a plain program's by a relative error of at most 0.012.
Values may be sent and summed in bfloat16 or wider, within the bound.
No kernel may reach another device: no remote copies, remote signals or barrier semaphores. Data moves between devices by JAX's collectives and lax.ppermute only.
A program may use at most 128 MiB of HBM per device.

v0:
```python
import jax
import jax.numpy as jnp
from jax import lax
from jax.sharding import PartitionSpec as P

EPS = 1e-06


def normalize_rows(vector):
    return vector * lax.rsqrt(jnp.sum(vector * vector, -1, keepdims=True) + EPS)


def delta_block(saved, queries, keys_in, values_in, strength, log_decay):
    highest = lax.Precision.HIGHEST
    steps_len = queries.shape[1]
    cumul = jnp.transpose(jnp.cumsum(log_decay, axis=1), (0, 2, 1))
    q_heads = jnp.transpose(queries, (0, 2, 1, 3))
    k_heads = jnp.transpose(keys_in, (0, 2, 1, 3))
    v_heads = jnp.transpose(values_in, (0, 2, 1, 3))
    weight_t = jnp.transpose(strength, (0, 2, 1))
    spread = cumul[..., :, None] - cumul[..., None, :]
    order = jnp.arange(steps_len)
    inside = order[:, None] >= order[None, :]
    below = order[:, None] > order[None, :]
    dec_incl = jnp.where(inside, jnp.exp(jnp.where(inside, spread, 0.0)), 0.0)
    dec_strict = jnp.where(below, dec_incl, 0.0)
    lower_mat = (
        weight_t[..., :, None]
        * jnp.einsum("bhik,bhjk->bhij", k_heads, k_heads, precision=highest)
        * dec_strict
    )
    growth = jnp.exp(cumul)
    rhs_all = jnp.concatenate(
        [weight_t[..., None] * v_heads, (weight_t * growth)[..., None] * k_heads], axis=-1
    )
    solved = []
    for row_index in range(steps_len):
        current = rhs_all[:, :, row_index]
        for col_index in range(row_index):
            current = current - lower_mat[:, :, row_index, col_index, None] * solved[col_index]
        solved.append(current)
    solution = jnp.stack(solved, axis=2)
    value_size = v_heads.shape[-1]
    update = solution[..., :value_size] - jnp.einsum(
        "bhpk,bhkv->bhpv", solution[..., value_size:], saved, precision=highest
    )
    scores = jnp.einsum("bhik,bhjk->bhij", q_heads, k_heads, precision=highest) * dec_incl
    output = jnp.einsum(
        "bhpk,bhkv->bhpv", growth[..., None] * q_heads, saved, precision=highest
    ) + jnp.einsum("bhij,bhjv->bhiv", scores, update, precision=highest)
    tail = jnp.exp(cumul[..., -1:] - cumul)[..., None] * k_heads
    renewed = jnp.exp(cumul[..., -1])[..., None, None] * saved + jnp.einsum(
        "bhpk,bhpv->bhkv", tail, update, precision=highest
    )
    return (jnp.transpose(output, (0, 2, 1, 3)), renewed)


def body(
    tokens,
    in_gain,
    w_query,
    w_key,
    w_value,
    w_gate,
    w_beta,
    w_decay,
    decay_base,
    out_gain,
    w_out,
    state,
    prev_keys,
    prev_values,
    prev_beta,
    prev_decay,
    accepted,
):
    seq_count, props, _ = tokens.shape
    heads = decay_base.shape[0]
    head_size = out_gain.shape[0]
    width = heads * head_size
    rows = seq_count * props
    whole = lax.all_gather(tokens, "tp", axis=2, tiled=True)
    wide = whole.astype(jnp.float32)
    normed = (wide * lax.rsqrt(jnp.mean(wide * wide, -1, keepdims=True) + EPS) * in_gain).astype(
        jnp.bfloat16
    )
    normed = normed.reshape(rows, -1)

    def add_rows(piece):
        return jnp.dot(normed, piece, preferred_element_type=jnp.float32)

    query = add_rows(lax.all_gather(w_query, "kv", axis=0, tiled=True))
    key_vec = add_rows(lax.all_gather(w_key, "kv", axis=0, tiled=True))
    value_vec = add_rows(lax.all_gather(w_value, "kv", axis=0, tiled=True))
    gate = add_rows(lax.all_gather(w_gate, "kv", axis=0, tiled=True))
    offset = lax.axis_index("tp") * heads
    beta_cols = lax.dynamic_slice_in_dim(w_beta, offset, heads, 1)
    decay_cols = lax.dynamic_slice_in_dim(w_decay, offset, heads, 1)
    shape4 = (seq_count, props, heads, head_size)
    query = normalize_rows(query.reshape(shape4)) * head_size ** (-0.5)
    key_vec = normalize_rows(key_vec.reshape(shape4))
    value_vec = value_vec.reshape(shape4)
    gate = gate.reshape(shape4)
    strength = jax.nn.sigmoid(
        jnp.dot(normed, beta_cols, preferred_element_type=jnp.float32)
    ).reshape(seq_count, props, heads)
    log_decay = (
        -decay_base
        * jax.nn.softplus(jnp.dot(normed, decay_cols, preferred_element_type=jnp.float32))
    ).reshape(seq_count, props, heads)
    live = (jnp.arange(props, dtype=jnp.int32)[None, :] < accepted[:, None]).astype(jnp.float32)
    prev_strength = jax.nn.sigmoid(prev_beta) * live[..., None]
    prev_log = prev_decay * live[..., None]
    prev_k = normalize_rows(prev_keys.astype(jnp.float32).reshape(shape4))
    prev_v = prev_values.astype(jnp.float32).reshape(shape4)
    saved = jnp.transpose(state.reshape(seq_count, head_size, heads, head_size), (0, 2, 1, 3))
    committed = delta_block(saved, prev_k, prev_k, prev_v, prev_strength, prev_log)[1]
    output = delta_block(committed, query, key_vec, value_vec, strength, log_decay)[0]
    gated = (
        (
            output
            * lax.rsqrt(jnp.mean(output * output, -1, keepdims=True) + EPS)
            * out_gain
            * jax.nn.silu(gate)
        )
        .astype(jnp.bfloat16)
        .reshape(rows, width)
    )
    new_state = jnp.transpose(committed, (0, 2, 1, 3)).reshape(seq_count, head_size, width)
    terms = jnp.dot(
        gated, lax.all_gather(w_out, "kv", axis=1, tiled=True), preferred_element_type=jnp.float32
    )
    mixed = lax.psum_scatter(terms.astype(jnp.bfloat16), "tp", scatter_dimension=1, tiled=True)
    return (mixed.reshape(seq_count, props, -1), new_state)


def solution(mesh):
    placed = (
        P(("grp", "kv"), None, "tp"),
        P(),
        P("kv", "tp"),
        P("kv", "tp"),
        P("kv", "tp"),
        P("kv", "tp"),
        P(),
        P(),
        P("tp"),
        P(),
        P("tp", "kv"),
        P(("grp", "kv"), None, "tp"),
        P(("grp", "kv"), None, "tp"),
        P(("grp", "kv"), None, "tp"),
        P(("grp", "kv"), None, "tp"),
        P(("grp", "kv"), None, "tp"),
        P(("grp", "kv")),
    )
    return jax.shard_map(
        body,
        mesh=mesh,
        in_specs=placed,
        out_specs=(P(("grp", "kv"), None, "tp"), P(("grp", "kv"), None, "tp")),
        check_vma=False,
    )
```

profile of v0, /device:TPU:9, one launch (start us, length us, event | category | flops | bytes accessed | tf_op | source)
XLA Modules:
  0.0 190.5 jit_solution(15288922309329087683)
XLA Ops:
  7.3 0.7 all-gather.12.cloned.1.call-update
  8.0 0.7 all-gather.6.cloned.1.call-update
  8.8 0.7 all-gather.8.cloned.1.call-update
  9.5 0.5 all-gather.10.cloned.1.call-update
  10.1 0.5 all-gather.14.cloned.1.call-update
  10.6 7.9 %all_gather.18 = bf16[32,4,2048]{2,1,0:T(4,128)(2,1)S(1)} all-gather(bf16[32,4,512]{2,1,0:T(4,128)(2,1)} %param.17), channel_id=1, replica_groups=mesh['grp'=2,'kv'=4,'tp'=4] {'tp'}, dimensions={2}, use_global_device_ids=true | all-gather | bytes 655360 | tf_op jit(solution)/shard_map/all_gather | solution.py:82
  18.5 0.4 fusion.17
  18.9 1.8 fusion.93
  20.7 1.0 fusion.19
  21.8 0.1 reshape.137
  22.0 0.2 fusion.16
  22.2 0.1 reshape.143
  22.5 0.7 copy.452
  23.2 0.7 copy.524
  24.0 1.0 fusion.69
  25.3 0.6 copy.380
  25.9 0.6 copy.419
  26.6 3.3 %reshape.139 = f32[32,64,4,64]{3,2,1,0:T(4,128)} reshape(f32[32,64,256]{2,1,0:T(8,128)S(1)} %copy-done.4) | data formatting | bytes 4194304 | tf_op jit(solution)/shard_map/reshape | solution.py:116
  30.1 0.2 reshape.158
  30.4 0.2 reshape.148
  30.6 0.2 multiply_reduce_fusion.1
  30.8 0.3 copy.387
  31.3 1.4 fusion.12
  32.7 0.6 fusion.81
  34.5 0.5 bitcast_multiply_fusion.4
  35.0 1.5 multiply_subtract_fusion
  36.6 0.3 pad_maximum_fusion
  36.8 5.7 %fusion.8 = f32[32,4,4,64]{3,2,1,0:T(4,128)S(1)} fusion(f32[32,64,4,64]{3,2,1,0:T(4,128)} %reshape.139, f32[32,4,4,128]{3,2,1,0:T(4,128)S(1)} %pad_maximum_fusion), kind=kOutput, calls=%fused_computation.11 | convolution fusion | flops 25198592 | bytes 2752512 | tf_op jit(solution)/shard_map/bhpk,bhkv->bhpv/dot_general | solution.py:44
  42.5 9.6 %bitcast_add_fusion = (f32[32,64,4,64]{3,1,2,0:T(8,128)}, f32[32,4,64,64]{3,2,1,0:T(8,128)}) fusion(f32[32,64,4,64]{3,2,1,0:T(4,128)S(1)} %copy-done.1, f32[32,4]{1,0:T(8,128)S(1)} %copy.381, f32[32,4,4,64]{3,2,1,0:T(4,128)S(1)} %fusion.8, f32[32,4,4,64]{3,2,0,1:T(4,128)S(1)} %reshape.148, f32[32,4,4]{1,2,0:T(4,128)S(1)} %copy.387, f32[32,4,4]{2,1,0:T(4,128)S(1)} %copy.383), kind=kOutput, calls=%fused_computation | convolution fusion | flops 26279936 | bytes 6558208 | tf_op jit(solution)/shard_map/bhpk,bhpv->bhkv/dot_general | solution.py:52
  52.1 1.5 copy.436
  53.7 13.2 %all-gather.6.cloned.1.call-done = bf16[2048,256]{1,0:T(8,128)(2,1)} async-done(((bf16[512,256]{1,0:T(8,128)(2,1)}), bf16[2048,256]{1,0:T(8,128)(2,1)}) %all-gather.6.cloned.1.call-update) | async-done | bytes 1048592 | tf_op jit(solution)/shard_map/all_gather | solution.py:92
  66.9 1.5 copy.377
  68.4 0.8 multiply_reduce_fusion.2
  69.2 0.6 rsqrt_bitcast_fusion.1
  69.8 26.0 %all-gather.8.cloned.1.call-done = bf16[2048,256]{1,0:T(8,128)(2,1)} async-done(((bf16[512,256]{1,0:T(8,128)(2,1)}), bf16[2048,256]{1,0:T(8,128)(2,1)}) %all-gather.8.cloned.1.call-update) | async-done | bytes 1048592 | tf_op jit(solution)/shard_map/all_gather | solution.py:93
  95.9 1.7 copy.409
  97.6 1.4 multiply_reduce_fusion
  99.0 0.6 rsqrt_bitcast_fusion
  99.6 25.1 %all-gather.10.cloned.1.call-done = bf16[2048,256]{1,0:T(8,128)(2,1)} async-done(((bf16[512,256]{1,0:T(8,128)(2,1)}), bf16[2048,256]{1,0:T(8,128)(2,1)}) %all-gather.10.cloned.1.call-update) | async-done | bytes 1048592 | tf_op jit(solution)/shard_map/all_gather | solution.py:94
  124.7 1.5 copy.417
  126.2 1.3 fusion.42
  127.5 2.0 %convolution_multiply_fusion.1 = f32[32,4,4,4]{3,2,1,0:T(4,128)S(1)} fusion(f32[32,4,4,64]{3,0,1,2:T(8,128)S(1)} %get-tuple-element.15, f32[32,4,4,64]{3,0,1,2:T(8,128)S(1)} %get-tuple-element.38, f32[32,4,4]{2,1,0:T(4,128)S(1)} %copy.413, pred[4,4]{1,0:T(4,128)(4,1)} %copy-done.13), kind=kOutput, calls=%fused_computation.14 | convolution fusion | flops 1581056 | bytes 272400 | tf_op jit(solution)/shard_map/bhik,bhjk->bhij/dot_general | solution.py:47
  129.5 2.0 %fusion.11 = f32[32,4,4,4]{3,2,1,0:T(4,128)S(1)} fusion(f32[32,4,4,64]{3,0,1,2:T(8,128)S(1)} %get-tuple-element.38, f32[32,4,4]{2,1,0:T(4,128)} %bitcast.126, f32[32,4,4]{2,1,0:T(4,128)S(1)} %copy.413, pred[4,4]{1,0:T(4,128)(4,1)} %copy-done.13, pred[4,4]{1,0:T(4,128)(4,1)} %copy-done.14), kind=kOutput, calls=%fused_computation.13 | convolution fusion | flops 1585152 | bytes 143392 | tf_op jit(solution)/shard_map/bhik,bhjk->bhij/dot_general | solution.py:29
  131.5 1.2 fusion.82
  132.7 1.5 copy.428
  134.2 1.5 copy.427
  135.7 1.5 copy.426
  137.2 1.5 copy.425
  138.7 1.5 copy.424
  140.2 0.7 copy.423
  140.9 1.4 fusion.13
  142.3 1.0 fusion.61
  143.2 0.1 slice.129
  143.4 8.0 %fusion.4 = f32[32,4,4,64]{3,2,1,0:T(4,128)S(1)} fusion(f32[32,4,64,64]{3,2,1,0:T(8,128)} %get-tuple-element.36, f32[32,64,4,64]{3,2,1,0:T(4,128)} %reshape.139, f32[32,4]{1,0:T(8,128)S(1)} %copy.381, f32[32,4,4,64]{3,0,1,2:T(8,128)S(1)} %slice.129), kind=kOutput, calls=%fused_computation.7 | convolution fusion | flops 26214400 | bytes 4456960 | tf_op jit(solution)/shard_map/bhpk,bhkv->bhpv/dot_general | solution.py:44
  151.5 1.1 fusion.34
  152.7 3.8 %fusion.6 = f32[32,4,4,64]{3,2,1,0:T(4,128)S(1)} fusion(f32[32,4,64,64]{3,2,1,0:T(8,128)S(1)} %copy-done.3, f32[32,64,4,64]{3,2,1,0:T(4,128)S(1)} %copy-done.2, f32[32,4]{1,0:T(8,128)S(1)} %copy.381, f32[32,4,4,64]{3,0,1,2:T(8,128)S(1)} %get-tuple-element.14), kind=kOutput, calls=%fused_computation.8 | convolution fusion | flops 26214400 | bytes 4456960 | tf_op jit(solution)/shard_map/bhpk,bhkv->bhpv/dot_general | solution.py:48
  156.4 0.2 fusion.28
  156.7 0.8 fusion.31
  157.6 0.1 reshape.144
  157.8 2.4 %convolution_convert_fusion = bf16[128,2048]{1,0:T(8,128)(2,1)} fusion(bf16[128,256]{1,0:T(8,128)(2,1)S(1)} %reshape.144, bf16[256,2048]{1,0:T(8,128)(2,1)} %all-gather.14.cloned.1.call-done), kind=kOutput, calls=%fused_computation.6 | convolution fusion | flops 134479872 | bytes 1638400 | tf_op jit(solution)/shard_map/dot_general | solution.py:130
  160.2 7.8 %copy.441 = f32[32,64,4,64]{3,2,1,0:T(4,128)} copy(f32[32,64,4,64]{3,1,2,0:T(8,128)} %get-tuple-element.35) | data formatting | bytes 4194304 | tf_op jit(solution)/shard_map/add | solution.py:52
  168.0 5.3 %reshape.146 = f32[32,64,256]{2,1,0:T(8,128)} reshape(f32[32,64,4,64]{3,2,1,0:T(4,128)} %copy.441) | data formatting | bytes 4194304 | tf_op jit(solution)/shard_map/reshape | solution.py:129
  173.3 8.8 %reduce-scatter.2.cloned.1.call-done = bf16[128,512]{1,0:T(8,128)(2,1)} async-done(((bf16[128,2048]{1,0:T(8,128)(2,1)}), bf16[128,512]{1,0:T(8,128)(2,1)}) %reduce-scatter.2.cloned.1.call-update) | async-done | bytes 131088 | tf_op jit(solution)/shard_map/reduce_scatter | solution.py:133
  182.0 1.6 reshape.145
  (76 shorter events, 2.8 us)
Async XLA Ops:
  7.2 14.8 %copy-start = (bf16[2048,16]{0,1:T(8,128)(2,1)S(1)}, bf16[2048,16]{0,1:T(8,128)(2,1)}, u32[]{:S(2)}) copy-start(bf16[2048,16]{0,1:T(8,128)(2,1)} %param.23) | copy-start | bytes 196612
  7.2 16.7 %copy-start.10 = (s32[32]{0:T(128)S(1)}, s32[32]{0:T(128)}, u32[]{:S(2)}) copy-start(s32[32]{0:T(128)} %param.33) | copy-start | bytes 388
  7.2 16.7 %copy-start.8 = (f32[32,4,4]{0,2,1:T(4,128)S(1)}, f32[32,4,4]{0,2,1:T(4,128)}, u32[]{:S(2)}) copy-start(f32[32,4,4]{0,2,1:T(4,128)} %param.32) | copy-start | bytes 6148
  7.2 16.8 %copy-start.11 = (f32[4]{0:T(128)S(1)}, f32[4]{0:T(128)}, u32[]{:S(2)}) copy-start(f32[4]{0:T(128)} %param.25) | copy-start | bytes 52
  7.2 19.4 %copy-start.4 = (f32[32,64,256]{2,1,0:T(8,128)S(1)}, f32[32,64,256]{2,1,0:T(8,128)}, u32[]{:S(2)}) copy-start(f32[32,64,256]{2,1,0:T(8,128)} %param.28) | copy-start | bytes 6291460
  7.2 44.9 %all-gather.12.cloned.1.call-start = ((), (), s32[]{:S(2)}) async-start(), calls=%async_computation.4 | async-start | bytes 1310720 | tf_op jit(solution)/shard_map/all_gather | solution.py:95
  8.0 58.9 %all-gather.6.cloned.1.call-start = ((), (), s32[]{:S(2)}) async-start(), calls=%async_computation.1 | async-start | bytes 1310720 | tf_op jit(solution)/shard_map/all_gather | solution.py:92
  8.7 87.2 %all-gather.8.cloned.1.call-start = ((), (), s32[]{:S(2)}) async-start(), calls=%async_computation.2 | async-start | bytes 1310720 | tf_op jit(solution)/shard_map/all_gather | solution.py:93
  9.4 115.2 %all-gather.10.cloned.1.call-start = ((), (), s32[]{:S(2)}) async-start(), calls=%async_computation.3 | async-start | bytes 1310720 | tf_op jit(solution)/shard_map/all_gather | solution.py:94
  10.0 147.8 %all-gather.14.cloned.1.call-start = ((), (), s32[]{:S(2)}) async-start(), calls=%async_computation.5 | async-start | bytes 1310720 | tf_op jit(solution)/shard_map/all_gather | solution.py:131
  10.6 171.4 %reduce-scatter.2.cloned.1.call-start = ((), (), s32[]{:S(2)}) async-start(), calls=%async_computation.6 | async-start | bytes 655360 | tf_op jit(solution)/shard_map/reduce_scatter | solution.py:133
  21.8 9.4 %copy-start.13 = (pred[4,4]{1,0:T(4,128)(4,1)}, pred[4,4]{1,0:T(4,128)(4,1)S(1)}, u32[]{:S(2)}) copy-start(pred[4,4]{1,0:T(4,128)(4,1)S(1)} %get-tuple-element.39) | copy-start | bytes 52
  21.8 9.4 %copy-start.14 = (pred[4,4]{1,0:T(4,128)(4,1)}, pred[4,4]{1,0:T(4,128)(4,1)S(1)}, u32[]{:S(2)}) copy-start(pred[4,4]{1,0:T(4,128)(4,1)S(1)} %get-tuple-element.40) | copy-start | bytes 52
  21.9 8.1 %copy-start.6 = (bf16[32,4,256]{2,1,0:T(4,128)(2,1)S(1)}, bf16[32,4,256]{2,1,0:T(4,128)(2,1)}, u32[]{:S(2)}) copy-start(bf16[32,4,256]{2,1,0:T(4,128)(2,1)} %param.30) | copy-start | bytes 196612
  22.0 8.3 %copy-start.9 = (f32[32,4,4]{0,2,1:T(4,128)S(1)}, f32[32,4,4]{0,2,1:T(4,128)}, u32[]{:S(2)}) copy-start(f32[32,4,4]{0,2,1:T(4,128)} %param.31) | copy-start | bytes 6148
  22.0 8.4 %copy-start.7 = (bf16[32,4,256]{2,1,0:T(4,128)(2,1)S(1)}, bf16[32,4,256]{2,1,0:T(4,128)(2,1)}, u32[]{:S(2)}) copy-start(bf16[32,4,256]{2,1,0:T(4,128)(2,1)} %param.29) | copy-start | bytes 196612
  34.5 8.0 %copy-start.1 = (f32[32,64,4,64]{3,2,1,0:T(4,128)S(1)}, f32[32,64,4,64]{3,2,1,0:T(4,128)}, u32[]{:S(2)}) copy-start(f32[32,64,4,64]{3,2,1,0:T(4,128)} %reshape.139) | copy-start | bytes 6291460
  52.1 16.3 %copy-start.5 = (bf16[32,4,2048,1]{2,1,0,3:T(4,128)(2,1)S(1)}, bf16[32,4,2048,1]{2,1,0,3:T(4,128)(2,1)}, u32[]{:S(2)}) copy-start(bf16[32,4,2048,1]{2,1,0,3:T(4,128)(2,1)} %fusion.93) | copy-start | bytes 1572868
  143.4 9.3 %copy-start.2 = (f32[32,64,4,64]{3,2,1,0:T(4,128)S(1)}, f32[32,64,4,64]{3,2,1,0:T(4,128)}, u32[]{:S(2)}) copy-start(f32[32,64,4,64]{3,2,1,0:T(4,128)} %reshape.139) | copy-start | bytes 6291460
  143.4 9.3 %copy-start.3 = (f32[32,4,64,64]{3,2,1,0:T(8,128)S(1)}, f32[32,4,64,64]{3,2,1,0:T(8,128)}, u32[]{:S(2)}) copy-start(f32[32,4,64,64]{3,2,1,0:T(8,128)} %get-tuple-element.36) | copy-start | bytes 6291460
  152.7 4.0 %copy-start.12 = (f32[64]{0:T(128)S(1)}, f32[64]{0:T(128)}, u32[]{:S(2)}) copy-start(f32[64]{0:T(128)} %param.26) | copy-start | bytes 772
Sparse Core Ops, SparseCore 0:
  9.6 28.2 all-gather.11
  39.5 27.3 all-gather.5
  68.5 27.3 all-gather.7
  97.3 27.3 all-gather.9
  126.1 27.3 all-gather.13
  160.3 21.6 reduce-scatter.1
where the time goes:
time: 193 us; the launch traced here: 190 us
  waiting for transfers between devices  76.3 us (40%)
  matrix products  41.6 us (22%)
  local copies, waits for them, and re-layouts  40.1 us (21%)
  between operations  14.7 us (8%)
  other arithmetic  9.66 us (5%)
  blocking collectives  7.9 us (4%)
    all_gather x1, waiting for transfers between devices, body(): key_vec = add_rows(lax.all_gather(w_key, 'kv', axis=0, tiled=True))  26 us
    all_gather x1, waiting for transfers between devices, body(): value_vec = add_rows(lax.all_gather(w_value, 'kv', axis=0, tiled=True))  25.1 us
    dot_general x2, matrix products, delta_block(): jnp.einsum('bhpk,bhkv->bhpv', solution[..., value_size:], saved, precisio...  13.7 us
    all_gather x1, waiting for transfers between devices, body(): query = add_rows(lax.all_gather(w_query, 'kv', axis=0, tiled=True))  13.2 us
    slice x14, local copies, waits for them, and re-layouts, delta_block(): lower_mat[:, :, row_index, col_index, None] * solved[col_index]  10.5 us
    dot_general x1, matrix products, delta_block(): jnp.einsum('bhpk,bhpv->bhkv', tail, update, precision=highest)  9.64 us
    reduce_scatter x1, waiting for transfers between devices, body(): lax.psum_scatter(terms.astype(jnp.bfloat16), 'tp', scatter_dimension=1, t...  8.75 us
    all_gather x1, blocking collectives, body(): whole = lax.all_gather(tokens, 'tp', axis=2, tiled=True)  7.9 us
  transfers between devices with their start and end apart: 6, of which 4 were waited for; matrix products, arithmetic and copies ran while one was open for 46% of the time, Pallas kernels for 0%

commit v1 on v0

v1 whole, which is shorter than its diff:
```python
import functools

import jax
import jax.numpy as jnp
from jax import lax
from jax.experimental import pallas as pl
from jax.experimental.pallas import tpu as pltpu
from jax.sharding import PartitionSpec as P

EPS = 1e-06
CHUNKS = 1
F32 = jnp.float32
BF16 = jnp.bfloat16
VMEM = pltpu.VMEM
SMEM = pltpu.SMEM
ANY = pl.ANY


def whole(space=VMEM):
    return pl.BlockSpec(memory_space=space)


def dot(a, b, contract=((1,), (0,)), precision=None):
    return lax.dot_general(
        a, b, (contract, ((), ())), precision=precision, preferred_element_type=F32
    )


def head_ones(width, size):
    row = lax.broadcasted_iota(jnp.int32, (width, width), 0) // size
    col = lax.broadcasted_iota(jnp.int32, (width, width), 1) // size
    return jnp.where(row == col, 1.0, 0.0).astype(BF16)


def head_sum(values, ones):
    high = values.astype(BF16)
    low = (values - high.astype(F32)).astype(BF16)
    return dot(high, ones) + dot(low, ones)


def head_mask(first, group, steps, width, size):
    sub = lax.broadcasted_iota(jnp.int32, (group * steps, width), 0) // steps + first
    lane = lax.broadcasted_iota(jnp.int32, (group * steps, width), 1) // size
    return sub == lane


def prep_kernel(steps, place, tok_ref, gain_ref, wt_ref, *out_refs):
    chunk_refs, stat_ref = out_refs[:-1], out_refs[-1]
    seqs = tok_ref.shape[0]
    each = seqs // len(chunk_refs)
    raw = [tok_ref[:, t, :].astype(F32) for t in range(steps)]
    gain = gain_ref[...]
    scaled = [(x * gain).astype(BF16) for x in raw]
    for c, ref in enumerate(chunk_refs):
        for t in range(steps):
            ref[t * each : (t + 1) * each, :] = scaled[t][c * each : (c + 1) * each]
    full = jnp.concatenate(scaled, 0)
    logits = dot(wt_ref[...], full, ((1,), (1,)))
    square = jnp.concatenate([x * x for x in raw], 0)
    ones = jnp.ones((8, square.shape[1]), F32)
    total = dot(ones, square, ((1,), (1,)), lax.Precision.HIGHEST)
    count = logits.shape[0]
    stat_ref[0:count, :] = logits
    stat_ref[count : count + 8, :] = total


def prepare(tokens, in_gain, w_beta, w_decay, place, n_tp, chunks):
    seqs, steps, local = tokens.shape
    heads_all = w_beta.shape[1]
    wt = jnp.concatenate([w_beta, w_decay], 1).T
    each = seqs // chunks
    shapes = [jax.ShapeDtypeStruct((steps * each, local), BF16) for _ in range(chunks)]
    shapes.append(jax.ShapeDtypeStruct((2 * heads_all + 8, seqs * steps), F32))
    grid = pltpu.PrefetchScalarGridSpec(
        num_scalar_prefetch=1,
        grid=(1,),
        in_specs=[
            pl.BlockSpec((seqs, steps, local), lambda i, p: (0, 0, 0)),
            pl.BlockSpec((1, local), lambda i, p: (0, p[2])),
            pl.BlockSpec((2 * heads_all, local), lambda i, p: (0, p[2])),
        ],
        out_specs=[pl.BlockSpec(s.shape, lambda i, p: (0, 0)) for s in shapes],
    )
    out = pl.pallas_call(
        functools.partial(prep_kernel, steps), out_shape=shapes, grid_spec=grid, name="prep"
    )(place, tokens, in_gain.reshape(1, -1), wt)
    return out[:-1], out[-1]


def project_kernel(count, x_ref, *refs):
    weights, outs = refs[:count], refs[count:]
    width = weights[0].shape[1]
    order = list(range(1, len(outs))) + [0]
    for d in order:
        for w in range(count):
            outs[d][:, w * width : (w + 1) * width] = dot(x_ref[d], weights[w][...]).astype(
                outs[d].dtype
            )


def project(x, weights):
    owners, rows, _ = x.shape
    width = weights[0].shape[1] * len(weights)
    flops = 2 * x.size * width
    return pl.pallas_call(
        functools.partial(project_kernel, len(weights)),
        out_shape=[
            jax.ShapeDtypeStruct((rows, width), F32 if d == 0 else BF16) for d in range(owners)
        ],
        in_specs=[whole()] * (1 + len(weights)),
        out_specs=[whole()] * owners,
        cost_estimate=pl.CostEstimate(flops=flops, bytes_accessed=4 * x.size, transcendentals=0),
        name="project",
    )(x, *weights)


def spread_heads(ref, value, offset, stride, seqs, heads, steps, size, t):
    for h in range(heads):
        tile, lane = divmod(h * size, 128)
        part = value[:, tile * 128 : (tile + 1) * 128]
        if lane:
            part = pltpu.roll(part, 128 - lane, 1)
        ref[pl.ds(offset + h * steps + t, seqs, stride=stride), :] = part


def put_rows(ref, start, count, value, stride=None):
    for m in range(ref.shape[0]):
        ref[m, pl.ds(start, count, stride=stride), :] = value[:, m * 128 : (m + 1) * 128]


def get_rows(ref, start, count, stride=None):
    return jnp.concatenate(
        [ref[m, pl.ds(start, count, stride=stride), :] for m in range(ref.shape[0])], 1
    )


def own_heads(product, masks, group, steps):
    tile = group * steps
    total = None
    for m, mask in enumerate(masks):
        part = jnp.where(mask, product[m * tile : (m + 1) * tile], 0.0)
        total = part if total is None else total + part
    shift = steps
    acc = total
    for _ in range(group - 1):
        acc = acc + pltpu.roll(total, shift, 0)
        shift += steps
    return acc


def catch_kernel(
    steps, size, s0_ref, k_ref, v_ref, b_ref, d_ref, a_ref, out_ref, kscr, pscr, uscr, gscr
):
    seqs, _, width = s0_ref.shape
    heads = width // size
    group = 8 // steps
    ones = head_ones(width, size)
    masks = [head_mask(g * group, group, steps, width, size) for g in range(heads // group)]
    pick = jnp.where(
        lax.broadcasted_iota(jnp.int32, (heads, width), 0)
        == lax.broadcasted_iota(jnp.int32, (heads, width), 1) // size,
        1.0,
        0.0,
    )
    keys = [k_ref[:, t, :].astype(F32) for t in range(steps)]
    for t in range(steps):
        spread_heads(kscr, keys[t], 0, heads * steps, seqs, heads, steps, size, t)
    pairs = [(t, r) for t in range(steps) for r in range(t + 1)]
    sums = head_sum(jnp.concatenate([keys[t] * keys[r] for t, r in pairs], 0), ones)
    raw = {p: sums[i * seqs : (i + 1) * seqs] for i, p in enumerate(pairs)}
    inv = [lax.rsqrt(raw[t, t] + EPS) for t in range(steps)]

    def read(s, carry):
        kb = kscr[pl.ds(s * heads * steps, heads * steps), :][:, :size].astype(BF16)
        seen = own_heads(dot(kb, s0_ref[s].astype(BF16)), masks, group, steps)
        put_rows(pscr, s * 8, 8, seen)
        return carry

    lax.fori_loop(0, seqs, read, 0, unroll=8)
    live = [jnp.where(a_ref[...] > t, 1.0, 0.0) for t in range(steps)]
    highest = lax.Precision.HIGHEST
    cumul, solved = [], []
    for t in range(steps):
        log = dot(d_ref[:, t, :], pick, precision=highest) * live[t]
        strength = jax.nn.sigmoid(dot(b_ref[:, t, :], pick, precision=highest)) * live[t]
        cumul.append(log if t == 0 else cumul[-1] + log)
        seen = get_rows(pscr, t, seqs, 8) * inv[t]
        rest = v_ref[:, t, :].astype(F32) - jnp.exp(cumul[t]) * seen
        for r in range(t):
            rest = rest - jnp.exp(cumul[t] - cumul[r]) * (raw[t, r] * inv[t] * inv[r]) * solved[r]
        solved.append(strength * rest)
    for t in range(steps):
        add = jnp.exp(cumul[-1] - cumul[t]) * inv[t] * solved[t]
        for g in range(group):
            put_rows(uscr, g * steps + t, seqs, add, 8)
    gscr[...] = jnp.exp(cumul[-1])

    def write(s, carry):
        ub = get_rows(uscr, s * 8, 8)
        wide = jnp.concatenate([jnp.where(m, ub, 0.0) for m in masks], 0).astype(BF16)
        kb = kscr[pl.ds(s * heads * steps, heads * steps), :][:, :size].astype(BF16)
        out_ref[s] = gscr[pl.ds(s, 1), :] * s0_ref[s] + dot(kb, wide, ((0,), (0,)))
        return carry

    lax.fori_loop(0, seqs, write, 0, unroll=8)


def catch_up(state, prev_keys, prev_values, prev_beta, prev_decay, accepted):
    seqs, size, width = state.shape
    steps = prev_keys.shape[1]
    heads = width // size
    return pl.pallas_call(
        functools.partial(catch_kernel, steps, size),
        out_shape=jax.ShapeDtypeStruct(state.shape, F32),
        in_specs=[whole()] * 6,
        out_specs=whole(),
        scratch_shapes=[
            VMEM((seqs * heads * steps, 128), F32),
            VMEM((width // 128, seqs * 8, 128), F32),
            VMEM((width // 128, seqs * 8, 128), F32),
            VMEM((seqs, width), F32),
        ],
        cost_estimate=pl.CostEstimate(
            flops=seqs * 4000000, bytes_accessed=8 * state.size, transcendentals=0
        ),
        name="catch_up",
    )(state, prev_keys, prev_values, prev_beta, prev_decay, accepted.reshape(-1, 1))


def propose_kernel(
    dims, parts, blocks, place, stat_ref, base_ref, gain_ref, s_ref, *refs
):
    steps, size, features, heads_all = dims
    part_refs, refs = refs[:parts], refs[parts:]
    block_refs, refs = refs[: len(blocks)], refs[len(blocks) :]
    out_refs, refs = refs[:-4], refs[-4:]
    kscr, pscr, wo, sems = refs
    seqs, _, width = s_ref.shape
    heads = width // size
    group = 8 // steps
    kv, tp = place[1], place[2]

    copies = []
    for i, (place_of, ref) in enumerate(zip(blocks, block_refs)):
        target = place_of(place, wo)
        copies.append(pltpu.make_async_copy(ref, target, sems.at[i]))
        copies[-1].start()

    ones = head_ones(width, size)
    masks = [head_mask(g * group, group, steps, width, size) for g in range(heads // group)]
    rows = seqs * steps
    stat = stat_ref[...]
    count = stat.shape[0]
    src = lax.broadcasted_iota(jnp.int32, (count, width), 0)
    head = lax.broadcasted_iota(jnp.int32, (count, width), 1) // size + tp * heads
    highest = lax.Precision.HIGHEST
    flat = stat.T

    def take(row):
        return dot(flat, jnp.where(src == row, 1.0, 0.0), precision=highest)

    scale = lax.rsqrt(take(2 * heads_all) / features + EPS)
    strength = jax.nn.sigmoid(scale * take(head))
    rate = scale * take(heads_all + head)
    log = -base_ref[...] * (jnp.maximum(rate, 0.0) + jnp.log1p(jnp.exp(-jnp.abs(rate))))

    def column(w):
        lanes = slice(w * width, (w + 1) * width)
        total = part_refs[0][:, lanes].astype(F32)
        for ref in part_refs[1:]:
            total = total + ref[:, lanes].astype(F32)
        return total * scale

    query, key = column(0), column(1)
    squares = head_sum(jnp.concatenate([query * query, key * key], 0), ones)
    query = query * (lax.rsqrt(squares[:rows] + EPS) * size ** (-0.5))
    key = key * lax.rsqrt(squares[rows:] + EPS)

    def at(array, t):
        return array[t * seqs : (t + 1) * seqs]

    stride = 2 * heads * steps
    for t in range(steps):
        spread_heads(kscr, at(query, t), 0, stride, seqs, heads, steps, size, t)
        spread_heads(kscr, at(key, t), heads * steps, stride, seqs, heads, steps, size, t)
    below = [(t, r) for t in range(steps) for r in range(t)]
    inside = [(t, r) for t in range(steps) for r in range(t + 1)]
    products = [at(key, t) * at(key, r) for t, r in below]
    products += [at(query, t) * at(key, r) for t, r in inside]
    sums = head_sum(jnp.concatenate(products, 0), ones)
    k_k = {p: at(sums, i) for i, p in enumerate(below)}
    q_k = {p: at(sums, len(below) + i) for i, p in enumerate(inside)}
    upper = lax.broadcasted_iota(jnp.int32, (8, width), 0) < steps

    def read(s, carry):
        vectors = kscr[pl.ds(s * stride, stride), :][:, :size].astype(BF16)
        seen = dot(vectors, s_ref[s].astype(BF16))
        half = heads * steps
        from_query = own_heads(seen[:half], masks, group, steps)
        from_key = own_heads(seen[half:], masks, group, steps)
        put_rows(pscr, s * 8, 8, jnp.where(upper, from_query, from_key))
        return carry

    lax.fori_loop(0, seqs, read, 0, unroll=8)
    value, gate = column(2), column(3)
    cumul, solved, outs = [], [], []
    for t in range(steps):
        cumul.append(at(log, t) if t == 0 else cumul[-1] + at(log, t))
        grown = jnp.exp(cumul[t])
        rest = at(value, t) - grown * get_rows(pscr, steps + t, seqs, 8)
        out = grown * get_rows(pscr, t, seqs, 8)
        for r in range(t):
            decay = jnp.exp(cumul[t] - cumul[r])
            rest = rest - decay * k_k[t, r] * solved[r]
            out = out + decay * q_k[t, r] * solved[r]
        solved.append(at(strength, t) * rest)
        outs.append(out + q_k[t, t] * solved[t])
    output = jnp.concatenate(outs, 0)
    mean = head_sum(output * output, ones) * (1.0 / size)
    gated = output * lax.rsqrt(mean + EPS) * gain_ref[...] * (gate / (1.0 + jnp.exp(-gate)))
    gated = gated.astype(BF16)
    if not blocks:
        out_refs[0][...] = gated
        return
    for copy in copies:
        copy.wait()
    n = wo.shape[0]
    for s in list(range(1, n)) + [0]:
        out_refs[s][...] = dot(gated, wo[lax.rem(tp + s, n)]).astype(out_refs[s].dtype)


def propose(place, stat, base, gain, state, parts, blocks, block_arrays, n_tp, dims, seqs, first):
    steps, size = dims[0], dims[1]
    width = state.shape[2]
    heads = width // size
    rows = seqs * steps
    if blocks:
        share = dims[2] // n_tp
        shapes = [
            jax.ShapeDtypeStruct((rows, share), F32 if s == 0 else BF16) for s in range(n_tp)
        ]
        wo = VMEM((n_tp, width, share), BF16)
    else:
        shapes = [jax.ShapeDtypeStruct((rows, width), BF16)]
        wo = VMEM((8, 128), F32)
    grid = pltpu.PrefetchScalarGridSpec(
        num_scalar_prefetch=1,
        grid=(1,),
        in_specs=[
            pl.BlockSpec(stat.shape, lambda i, p: (0, 0)),
            pl.BlockSpec((1, width), lambda i, p: (0, 0)),
            pl.BlockSpec((1, width), lambda i, p: (0, 0)),
            pl.BlockSpec((seqs,) + state.shape[1:], lambda i, p: (first, 0, 0)),
        ]
        + [pl.BlockSpec(a.shape, lambda i, p: (0, 0)) for a in parts]
        + [whole(ANY)] * len(blocks),
        out_specs=[pl.BlockSpec(s.shape, lambda i, p: (0, 0)) for s in shapes],
        scratch_shapes=[
            VMEM((seqs * 2 * heads * steps, 128), F32),
            VMEM((width // 128, seqs * 8, 128), F32),
            wo,
            pltpu.SemaphoreType.DMA((max(1, len(blocks)),)),
        ],
    )
    return pl.pallas_call(
        functools.partial(propose_kernel, dims, len(parts), blocks),
        out_shape=shapes,
        grid_spec=grid,
        cost_estimate=pl.CostEstimate(
            flops=seqs * 4000000, bytes_accessed=4 * state.size, transcendentals=0
        ),
        name="propose",
    )(place, stat, base, gain, state, *parts, *block_arrays)


def finish_kernel(steps, chunks, *refs):
    ins, out_ref = refs[:-1], refs[-1]
    per = len(ins) // chunks
    each = out_ref.shape[0] // chunks
    for c in range(chunks):
        total = ins[c * per][...].astype(F32)
        for ref in ins[c * per + 1 : (c + 1) * per]:
            total = total + ref[...].astype(F32)
        for t in range(steps):
            out_ref[c * each : (c + 1) * each, t, :] = total[t * each : (t + 1) * each].astype(
                out_ref.dtype
            )


def finish(pieces, seqs, steps):
    chunks = len(pieces)
    flat = [a for piece in pieces for a in piece]
    return pl.pallas_call(
        functools.partial(finish_kernel, steps, chunks),
        out_shape=jax.ShapeDtypeStruct((seqs, steps, flat[0].shape[1]), BF16),
        in_specs=[whole()] * len(flat),
        out_specs=whole(),
        name="finish",
    )(*flat)


def body(
    sizes,
    tokens,
    in_gain,
    w_query,
    w_key,
    w_value,
    w_gate,
    w_beta,
    w_decay,
    decay_base,
    out_gain,
    w_out,
    state,
    prev_keys,
    prev_values,
    prev_beta,
    prev_decay,
    accepted,
):
    n_grp, n_kv, n_tp = sizes
    seqs, steps, local = tokens.shape
    heads = decay_base.shape[0]
    size = out_gain.shape[0]
    features = in_gain.shape[0]
    heads_all = w_beta.shape[1]
    dims = (steps, size, features, heads_all)
    square = n_kv == n_tp and n_grp == 2
    chunks = CHUNKS if square else 1
    each = seqs // chunks
    place = jnp.stack([lax.axis_index("grp"), lax.axis_index("kv"), lax.axis_index("tp")])
    place = place.astype(jnp.int32)
    base = jnp.repeat(decay_base, size).reshape(1, -1)
    gain = jnp.tile(out_gain, heads).reshape(1, -1)
    weights = (w_query, w_key, w_value, w_gate)

    scaled, stat = prepare(tokens, in_gain, w_beta, w_decay, place, n_tp, chunks)

    def ring(n, s):
        return [(i, (i + s) % n) for i in range(n)]

    if square:
        n = n_kv
        turn = [(k * n + t, t * n + (k - t) % n) for k in range(n) for t in range(n)]
        turned = [lax.ppermute(x, ("kv", "tp"), turn) for x in scaled]
        half = w_out.shape[0] // n_grp
        mine = lax.dynamic_slice_in_dim(w_out, place[0] * half, half, 0)
        blocks = [lambda p, wo: wo.at[p[1]]]
        arrays = [w_out]
        for s in range(1, n):
            got = lax.ppermute(mine, "kv", ring(n, s))
            other = lax.ppermute(got, "grp", ring(n_grp, 1))
            arrays += [got, other]
            for g in range(n_grp):

                def target(p, wo, s=s, g=g):
                    row = lax.rem(p[0] + g, n_grp) * half
                    return wo.at[lax.rem(p[1] - s + n, n), pl.ds(pl.multiple_of(row, half), half), :]

                blocks.append(target)
        stat_all = jnp.sum(lax.all_gather(stat, "tp"), 0)
        parts = []
        for x in turned:
            mine_parts = project(lax.all_gather(x, "tp"), weights)
            parts.append(
                [mine_parts[0]]
                + [lax.ppermute(mine_parts[d], "kv", ring(n, d)) for d in range(1, n)]
            )
    else:
        blocks, arrays = [], []
        stat_all = jnp.sum(lax.all_gather(stat, "tp"), 0)
        x = lax.all_gather(scaled[0], "tp", axis=1, tiled=True)
        parts = [
            [
                jnp.concatenate(
                    [
                        jnp.dot(
                            x,
                            lax.all_gather(w, "kv", axis=0, tiled=True),
                            preferred_element_type=F32,
                        )
                        for w in weights
                    ],
                    1,
                )
            ]
        ]

    new_state = catch_up(state, prev_keys, prev_values, prev_beta, prev_decay, accepted)
    by_step = stat_all.reshape(stat_all.shape[0], steps, seqs)
    pieces = []
    for c in range(chunks):
        own = by_step[:, :, c * each : (c + 1) * each].reshape(stat_all.shape[0], -1)
        out = propose(
            place, own, base, gain, new_state, parts[c], blocks, arrays, n_tp, dims, each, c
        )
        if square:
            pieces.append(
                [out[0]] + [lax.ppermute(out[s], "tp", ring(n_tp, s)) for s in range(1, n_tp)]
            )
        else:
            full = lax.all_gather(w_out, "kv", axis=1, tiled=True)
            terms = jnp.dot(out[0], full, preferred_element_type=F32).astype(BF16)
            pieces.append([lax.psum_scatter(terms, "tp", scatter_dimension=1, tiled=True)])
    return finish(pieces, seqs, steps), new_state


def solution(mesh):
    rows = P(("grp", "kv"), None, "tp")
    matrix = P("kv", "tp")
    placed = (
        rows,
        P(),
        matrix,
        matrix,
        matrix,
        matrix,
        P(),
        P(),
        P("tp"),
        P(),
        P("tp", "kv"),
        rows,
        rows,
        rows,
        rows,
        rows,
        P(("grp", "kv")),
    )
    sizes = (mesh.shape["grp"], mesh.shape["kv"], mesh.shape["tp"])
    return jax.shard_map(
        functools.partial(body, sizes),
        mesh=mesh,
        in_specs=placed,
        out_specs=(rows, rows),
        check_vma=False,
    )
```

time: 193 us -> 78.4 us (0.41); the launches traced: 190 us -> 78 us
  waiting for transfers between devices: 76.3 us -> 9.76 us
  matrix products: 41.6 us -> 0 us
  local copies, waits for them, and re-layouts: 40.1 us -> 5.78 us
  Pallas kernels: 0 us -> 19.1 us
  starting transfers between devices: 0.23 us -> 17.7 us
  blocking collectives: 7.9 us -> 22.2 us
  between operations: 14.7 us -> 0.83 us
  other arithmetic: 9.66 us -> 2.72 us
    all_gather x5 -> x0, waiting for transfers between devices: 64.4 us -> none  [the longest x1 26 us: body(): key_vec = add_rows(lax.all_gather(w_key, 'kv', axis=0, tiled=True))]
    dot_general x15 -> x0, matrix products: 41.6 us -> none  [the longest x2 13.7 us: delta_block(): jnp.einsum('bhpk,bhkv->bhpv', solution[..., value_size:], saved, precisio...]
    pallas_call x0 -> x5, Pallas kernels: none -> 19.1 us  [the longest x1 6.02 us: propose(): pl.pallas_call(functools.partial(propose_kernel, dims, len(parts), blocks...]
    ppermute x0 -> x13, starting transfers between devices: none -> 17.7 us  [the longest x3 5.59 us: body(): got = lax.ppermute(mine, 'kv', ring(n, s))]
    all_gather x1 -> x2, blocking collectives: 7.9 us -> 22.2 us  [the longest x1 15.2 us: body(): mine_parts = project(lax.all_gather(x, 'tp'), weights)]
    slice x15 -> x0, local copies, waits for them, and re-layouts: 10.7 us -> none  [the longest x14 10.5 us: delta_block(): lower_mat[:, :, row_index, col_index, None] * solved[col_index]]
    reshape x11 -> x1, local copies, waits for them, and re-layouts: 11.1 us -> 0.69 us  [catch_up(): accepted.reshape(-1, 1)]
    ppermute x0 -> x13, waiting for transfers between devices: none -> 9.76 us  [the longest x3 6.77 us: body(): lax.ppermute(out[s], 'tp', ring(n_tp, s))]
  transfers between devices with their start and end apart: 6 -> 13, of which waited for: 4 -> 4; matrix products, arithmetic and copies ran while one was open for 46% -> 6% of each run, Pallas kernels for 0% -> 11%
where the time goes in v1:
time: 78.4 us; the launch traced here: 78 us
  blocking collectives  22.2 us (28%)
  Pallas kernels  19.1 us (24%)
  starting transfers between devices  17.7 us (23%)
  waiting for transfers between devices  9.76 us (12%)
  local copies, waits for them, and re-layouts  5.78 us (7%)
  other arithmetic  2.72 us (3%)
  between operations  0.83 us (1%)
    all_gather x1, blocking collectives, body(): mine_parts = project(lax.all_gather(x, 'tp'), weights)  15.2 us
    all_gather x1, blocking collectives, body(): stat_all = jnp.sum(lax.all_gather(stat, 'tp'), 0)  6.94 us
    ppermute x3, waiting for transfers between devices, body(): lax.ppermute(out[s], 'tp', ring(n_tp, s))  6.77 us
    pallas_call x1, Pallas kernels, propose(): pl.pallas_call(functools.partial(propose_kernel, dims, len(parts), blocks...  6.02 us
    ppermute x3, starting transfers between devices, body(): got = lax.ppermute(mine, 'kv', ring(n, s))  5.59 us
    pallas_call x1, Pallas kernels, catch_up(): pl.pallas_call(functools.partial(catch_kernel, steps, size), out_shape=ja...  5.57 us
    ppermute x3, starting transfers between devices, body(): lax.ppermute(mine_parts[d], 'kv', ring(n, d))  4.75 us
    ppermute x3, waiting for transfers between devices, body(): lax.ppermute(mine_parts[d], 'kv', ring(n, d))  2.98 us
  transfers between devices with their start and end apart: 13, of which 4 were waited for; matrix products, arithmetic and copies ran while one was open for 6% of the time, Pallas kernels for 11%

profile of v1, /device:TPU:9, one launch (start us, length us, event | category | flops | bytes accessed | tf_op | source)
XLA Modules:
  0.0 78.0 jit_solution(10648662618658267589)
XLA Ops:
  0.6 0.0 copy-start.15
  0.6 0.0 copy-start.16
  0.7 0.0 copy-start.17
  0.7 0.0 copy-start.13
  0.7 0.0 copy-start.14
  0.7 1.6 %maximum_bitcast_fusion.wt_ref = bf16[32,2048]{1,0:T(8,128)(2,1)} fusion(bf16[2048,16]{0,1:T(8,128)(2,1)} %param.24, bf16[2048,16]{0,1:T(8,128)(2,1)} %param.23), kind=kLoop, calls=%fused_computation | loop fusion | flops 262144 | bytes 262144 | tf_op jit(solution)/shard_map/transpose | solution.py:70
  2.2 0.6 pad_add_fusion.place
  2.8 2.7 %prep.1 = (bf16[128,512]{1,0:T(8,128)(2,1)}, f32[40,128]{1,0:T(8,128)}) custom-call(s32[3]{0:T(128)} %pad_add_fusion.place, bf16[32,4,512]{2,1,0:T(4,128)(2,1)} %tok_ref.1, f32[1,2048]{1,0:T(1,128)} %bitcast.11, bf16[32,2048]{1,0:T(8,128)(2,1)} %maximum_bitcast_fusion.wt_ref), custom_call_target="tpu_custom_call" | custom-call | tf_op jit(solution)/shard_map/prep/pallas_call | solution.py:84
  5.5 2.7 %collective-permute-start = (bf16[128,512]{1,0:T(8,128)(2,1)}, bf16[128,512]{1,0:T(8,128)(2,1)S(1)}, u32[]{:S(2)}, u32[]{:S(2)}) collective-permute-start(bf16[128,512]{1,0:T(8,128)(2,1)} %get-tuple-element.13), channel_id=1, source_target_pairs={{0,0},{1,7},{2,10},{3,13},{4,1},{5,4},{6,11},{7,14},{8,2},{9,5},{1... | collective-permute-start | bytes 393224 | tf_op jit(solution)/shard_map/ppermute | solution.py:446
  8.2 0.9 %constant_dynamic-slice_fusion = bf16[128,512]{1,0:T(8,128)(2,1)S(1)} fusion(bf16[256,512]{1,0:T(8,128)(2,1)} %refs_4_.1, s32[]{:T(128)S(6)} %select_n.3), kind=kLoop, calls=%fused_computation.2 | loop fusion | bytes 262148 | tf_op jit(solution)/shard_map/dynamic_slice | solution.py:448
  9.1 1.8 %collective-permute-start.8 = (bf16[128,512]{1,0:T(8,128)(2,1)S(1)}, bf16[128,512]{1,0:T(8,128)(2,1)S(1)}, u32[]{:S(2)}, u32[]{:S(2)}) collective-permute-start(bf16[128,512]{1,0:T(8,128)(2,1)S(1)} %constant_dynamic-slice_fusion), channel_id=1, source_target_pairs={{0,12},{4,0},{8,4},{12,8},{1,13},{5,1},{9,5},{13,9},{2,14},{6,2},{... | collective-permute-start | bytes 393224 | tf_op jit(solution)/shard_map/ppermute | solution.py:452
  10.9 1.5 %collective-permute-start.6 = (bf16[128,512]{1,0:T(8,128)(2,1)S(1)}, bf16[128,512]{1,0:T(8,128)(2,1)S(1)}, u32[]{:S(2)}, u32[]{:S(2)}) collective-permute-start(bf16[128,512]{1,0:T(8,128)(2,1)S(1)} %constant_dynamic-slice_fusion), channel_id=1, source_target_pairs={{0,8},{4,12},{8,0},{12,4},{1,9},{5,13},{9,1},{13,5},{2,10},{6,14},... | collective-permute-start | bytes 393224 | tf_op jit(solution)/shard_map/ppermute | solution.py:452
  12.5 2.3 %collective-permute-start.4 = (bf16[128,512]{1,0:T(8,128)(2,1)S(1)}, bf16[128,512]{1,0:T(8,128)(2,1)S(1)}, u32[]{:S(2)}, u32[]{:S(2)}) collective-permute-start(bf16[128,512]{1,0:T(8,128)(2,1)S(1)} %constant_dynamic-slice_fusion), channel_id=1, source_target_pairs={{0,4},{4,8},{8,12},{12,0},{1,5},{5,9},{9,13},{13,1},{2,6},{6,10},{... | collective-permute-start | bytes 393224 | tf_op jit(solution)/shard_map/ppermute | solution.py:452
  14.7 0.0 collective-permute-done
  14.7 15.2 %all-gather.1 = bf16[512,512]{1,0:T(8,128)(2,1)} all-gather(bf16[128,512]{1,0:T(8,128)(2,1)S(1)} %collective-permute-done), channel_id=3, replica_groups=mesh['grp'=2,'kv'=4,'tp'=4] {'tp'}, dimensions={0}, use_global_device_ids=true | all-gather | bytes 655360 | tf_op jit(solution)/shard_map/all_gather | solution.py:465
  30.0 2.9 %project.1 = (f32[128,1024]{1,0:T(8,128)}, bf16[128,1024]{1,0:T(8,128)(2,1)}, bf16[128,1024]{1,0:T(8,128)(2,1)}, bf16[128,1024]{1,0:T(8,128)(2,1)}) custom-call(bf16[4,128,512]{2,1,0:T(8,128)(2,1)} %bitcast.9, bf16[512,256]{1,0:T(8,128)(2,1)} %refs_0_.1, bf16[512,256]{1,0:T(8,128)(2,1)} %refs_1_.1, bf16[512,256]{1,0:T(8,128)(2,1)} %refs_2_.1, ...), custom_call_target="tpu_custom_call" | custom-call | flops 536870912 | bytes 1048576 | tf_op jit(solution)/shard_map/project/pallas_call | solution.py:105
  32.8 0.0 collective-permute-start.1
  32.8 0.0 collective-permute-done.8.refs_9_
  32.8 0.0 copy-start.3
  32.9 1.3 %collective-permute-start.9 = (bf16[128,512]{1,0:T(8,128)(2,1)S(1)}, bf16[128,512]{1,0:T(8,128)(2,1)S(1)}, u32[]{:S(2)}, u32[]{:S(2)}) collective-permute-start(bf16[128,512]{1,0:T(8,128)(2,1)S(1)} %collective-permute-done.8.refs_9_), channel_id=1, source_target_pairs={{0,16},{16,0},{1,17},{17,1},{2,18},{18,2},{3,19},{19,3},{4,20},{20... | collective-permute-start | bytes 393224 | tf_op jit(solution)/shard_map/ppermute | solution.py:453
  34.2 3.4 %collective-permute-start.2 = (bf16[128,1024]{1,0:T(8,128)(2,1)}, bf16[128,1024]{1,0:T(8,128)(2,1)S(1)}, u32[]{:S(2)}, u32[]{:S(2)}) collective-permute-start(bf16[128,1024]{1,0:T(8,128)(2,1)} %get-tuple-element.16), channel_id=1, source_target_pairs={{0,8},{4,12},{8,0},{12,4},{1,9},{5,13},{9,1},{13,5},{2,10},{6,14},... | collective-permute-start | bytes 786440 | tf_op jit(solution)/shard_map/ppermute | solution.py:468
  37.5 0.0 collective-permute-done.6.refs_7_
  37.5 1.4 %collective-permute-start.3 = (bf16[128,1024]{1,0:T(8,128)(2,1)}, bf16[128,1024]{1,0:T(8,128)(2,1)S(1)}, u32[]{:S(2)}, u32[]{:S(2)}) collective-permute-start(bf16[128,1024]{1,0:T(8,128)(2,1)} %get-tuple-element.17), channel_id=1, source_target_pairs={{0,12},{4,0},{8,4},{12,8},{1,13},{5,1},{9,5},{13,9},{2,14},{6,2},{... | collective-permute-start | bytes 786440 | tf_op jit(solution)/shard_map/ppermute | solution.py:468
  38.9 0.0 collective-permute-done.4.refs_5_
  38.9 0.2 collective-permute-start.7
  39.2 0.0 collective-permute-done.9.refs_10_
  39.2 1.2 %collective-permute-start.5 = (bf16[128,512]{1,0:T(8,128)(2,1)S(1)}, bf16[128,512]{1,0:T(8,128)(2,1)S(1)}, u32[]{:S(2)}, u32[]{:S(2)}) collective-permute-start(bf16[128,512]{1,0:T(8,128)(2,1)S(1)} %collective-permute-done.4.refs_5_), channel_id=1, source_target_pairs={{0,16},{16,0},{1,17},{17,1},{2,18},{18,2},{3,19},{19,3},{4,20},{20... | collective-permute-start | bytes 393224 | tf_op jit(solution)/shard_map/ppermute | solution.py:453
  40.4 0.0 copy-done.15
  40.4 0.1 broadcast_in_dim.3
  40.5 0.7 reshape_reshape.3.base_ref
  41.1 0.0 copy-done.16
  41.1 0.6 reshape_tile.3.gain_ref
  41.7 0.0 copy-done.17
  41.8 0.7 copy.21.a_ref
  42.4 0.0 copy-done.13
  42.4 0.7 copy.19.b_ref
  43.2 0.0 copy-done.14
  43.2 0.7 copy.20.d_ref
  43.9 0.0 copy-done.12
  43.9 6.9 %all-gather = f32[160,128]{1,0:T(8,128)S(1)} all-gather(f32[40,128]{1,0:T(8,128)S(1)} %copy-done.12), channel_id=2, replica_groups=mesh['grp'=2,'kv'=4,'tp'=4] {'tp'}, dimensions={0}, use_global_device_ids=true | all-gather | bytes 102400 | tf_op jit(solution)/shard_map/all_gather | solution.py:462
  50.8 0.6 reduce_sum.9.stat_ref
  51.4 5.6 %catch_up.1.s_ref = f32[32,64,256]{2,1,0:T(8,128)} custom-call(f32[32,64,256]{2,1,0:T(8,128)} %s0_ref.1, bf16[32,4,256]{2,1,0:T(4,128)(2,1)} %k_ref.1, bf16[32,4,256]{2,1,0:T(4,128)(2,1)} %v_ref.1, f32[32,4,4]{2,1,0:T(4,128)} %copy.19.b_ref, f32[32,4,4]{2,1,0:T(4,128)} %copy.20.d_ref, s32[32,1]{1,0:T(8,128)} %copy.21.a_ref), custom_call_target="tpu_custom_call" | custom-call | flops 128000000 | bytes 4194304 | tf_op jit(solution)/shard_map/catch_up/pallas_call | solution.py:212
  57.0 0.0 copy-done.3
  57.0 0.0 copy-done.4
  57.0 0.0 copy-done.5
  57.0 0.0 copy-done.6
  57.0 0.0 collective-permute-done.7.refs_8_
  57.0 0.0 copy-start.7
  57.0 0.0 collective-permute-done.5.refs_6_
  57.1 0.0 collective-permute-done.1.refs_1_
  57.1 0.0 collective-permute-done.2.refs_2_
  57.1 3.0 %collective-permute-done.3.refs_3_ = bf16[128,1024]{1,0:T(8,128)(2,1)S(1)} collective-permute-done((bf16[128,1024]{1,0:T(8,128)(2,1)}, bf16[128,1024]{1,0:T(8,128)(2,1)S(1)}, u32[]{:S(2)}, u32[]{:S(2)}) %collective-permute-start.3) | collective-permute-done | bytes 262176 | tf_op jit(solution)/shard_map/ppermute | solution.py:468
  60.1 0.0 copy-done.8
  60.1 0.0 copy-done.1
  60.1 0.7 copy-done.2
  60.8 6.0 %propose.1 = (f32[128,512]{1,0:T(8,128)}, bf16[128,512]{1,0:T(8,128)(2,1)}, bf16[128,512]{1,0:T(8,128)(2,1)}, bf16[128,512]{1,0:T(8,128)(2,1)}) custom-call(s32[3]{0:T(128)} %pad_add_fusion.place, f32[40,128]{1,0:T(8,128)} %reduce_sum.9.stat_ref, f32[1,256]{1,0:T(1,128)} %reshape_reshape.3.base_ref, f32[1,256]{1,0:T(1,128)} %reshape_tile.3.gain_ref, ...), custom_call_target="tpu_custom_call" | custom-call | flops 128000000 | bytes 2097152 | tf_op jit(solution)/shard_map/propose/pallas_call | solution.py:365
  66.8 1.0 %collective-permute-start.10 = (bf16[128,512]{1,0:T(8,128)(2,1)}, bf16[128,512]{1,0:T(8,128)(2,1)S(1)}, u32[]{:S(2)}, u32[]{:S(2)}) collective-permute-start(bf16[128,512]{1,0:T(8,128)(2,1)} %get-tuple-element.19), channel_id=1, source_target_pairs={{0,1},{1,2},{2,3},{3,0},{4,5},{5,6},{6,7},{7,4},{8,9},{9,10},{10,1... | collective-permute-start | bytes 393224 | tf_op jit(solution)/shard_map/ppermute | solution.py:500
  67.8 0.9 %collective-permute-start.11 = (bf16[128,512]{1,0:T(8,128)(2,1)}, bf16[128,512]{1,0:T(8,128)(2,1)S(1)}, u32[]{:S(2)}, u32[]{:S(2)}) collective-permute-start(bf16[128,512]{1,0:T(8,128)(2,1)} %get-tuple-element.20), channel_id=1, source_target_pairs={{0,2},{1,3},{2,0},{3,1},{4,6},{5,7},{6,4},{7,5},{8,10},{9,11},{10,... | collective-permute-start | bytes 393224 | tf_op jit(solution)/shard_map/ppermute | solution.py:500
  68.7 0.0 collective-permute-start.12
  68.7 2.0 %collective-permute-done.10.refs_1_ = bf16[128,512]{1,0:T(8,128)(2,1)S(1)} collective-permute-done((bf16[128,512]{1,0:T(8,128)(2,1)}, bf16[128,512]{1,0:T(8,128)(2,1)S(1)}, u32[]{:S(2)}, u32[]{:S(2)}) %collective-permute-start.10) | collective-permute-done | bytes 131104 | tf_op jit(solution)/shard_map/ppermute | solution.py:500
  70.7 4.1 %collective-permute-done.11.refs_2_ = bf16[128,512]{1,0:T(8,128)(2,1)S(1)} collective-permute-done((bf16[128,512]{1,0:T(8,128)(2,1)}, bf16[128,512]{1,0:T(8,128)(2,1)S(1)}, u32[]{:S(2)}, u32[]{:S(2)}) %collective-permute-start.11) | collective-permute-done | bytes 131104 | tf_op jit(solution)/shard_map/ppermute | solution.py:500
  74.8 0.7 collective-permute-done.12.refs_3_
  75.5 0.6 copy-done.11
  76.1 1.9 %finish.1 = bf16[32,4,512]{2,1,0:T(4,128)(2,1)} custom-call(f32[128,512]{1,0:T(8,128)} %get-tuple-element.18.refs_0_, bf16[128,512]{1,0:T(8,128)(2,1)} %copy-done.9, bf16[128,512]{1,0:T(8,128)(2,1)} %copy-done.10, bf16[128,512]{1,0:T(8,128)(2,1)} %copy-done.11), custom_call_target="tpu_custom_call" | custom-call | tf_op jit(solution)/shard_map/finish/pallas_call | solution.py:393
  (16 shorter events, 0.0 us)
Async XLA Ops:
  0.6 39.8 %copy-start.15 = (f32[4]{0:T(128)S(1)}, f32[4]{0:T(128)}, u32[]{:S(2)}) copy-start(f32[4]{0:T(128)} %param.25) | copy-start | bytes 52
  0.6 40.5 %copy-start.16 = (f32[64]{0:T(128)S(1)}, f32[64]{0:T(128)}, u32[]{:S(2)}) copy-start(f32[64]{0:T(128)} %param.26) | copy-start | bytes 772
  0.7 41.1 %copy-start.17 = (s32[32]{0:T(128)S(1)}, s32[32]{0:T(128)}, u32[]{:S(2)}) copy-start(s32[32]{0:T(128)} %param.33) | copy-start | bytes 388
  0.7 41.8 %copy-start.13 = (f32[32,4,4]{0,2,1:T(4,128)S(1)}, f32[32,4,4]{0,2,1:T(4,128)}, u32[]{:S(2)}) copy-start(f32[32,4,4]{0,2,1:T(4,128)} %param.31) | copy-start | bytes 6148
  0.7 42.5 %copy-start.14 = (f32[32,4,4]{0,2,1:T(4,128)S(1)}, f32[32,4,4]{0,2,1:T(4,128)}, u32[]{:S(2)}) copy-start(f32[32,4,4]{0,2,1:T(4,128)} %param.32) | copy-start | bytes 6148
  5.5 38.4 %copy-start.12 = (f32[40,128]{1,0:T(8,128)S(1)}, f32[40,128]{1,0:T(8,128)}, u32[]{:S(2)}) copy-start(f32[40,128]{1,0:T(8,128)} %get-tuple-element.12) | copy-start | bytes 61444
  5.5 9.2 %collective-permute-start = (bf16[128,512]{1,0:T(8,128)(2,1)}, bf16[128,512]{1,0:T(8,128)(2,1)S(1)}, u32[]{:S(2)}, u32[]{:S(2)}) collective-permute-start(bf16[128,512]{1,0:T(8,128)(2,1)} %get-tuple-element.13), channel_id=1, source_target_pairs={{0,0},{1,7},{2,10},{3,13},{4,1},{5,4},{6,11},{7,14},{8,2},{9,5},{1... | collective-permute-start | bytes 393224 | tf_op jit(solution)/shard_map/ppermute | solution.py:446
  9.1 23.7 %collective-permute-start.8 = (bf16[128,512]{1,0:T(8,128)(2,1)S(1)}, bf16[128,512]{1,0:T(8,128)(2,1)S(1)}, u32[]{:S(2)}, u32[]{:S(2)}) collective-permute-start(bf16[128,512]{1,0:T(8,128)(2,1)S(1)} %constant_dynamic-slice_fusion), channel_id=1, source_target_pairs={{0,12},{4,0},{8,4},{12,8},{1,13},{5,1},{9,5},{13,9},{2,14},{6,2},{... | collective-permute-start | bytes 393224 | tf_op jit(solution)/shard_map/ppermute | solution.py:452
  10.9 26.6 %collective-permute-start.6 = (bf16[128,512]{1,0:T(8,128)(2,1)S(1)}, bf16[128,512]{1,0:T(8,128)(2,1)S(1)}, u32[]{:S(2)}, u32[]{:S(2)}) collective-permute-start(bf16[128,512]{1,0:T(8,128)(2,1)S(1)} %constant_dynamic-slice_fusion), channel_id=1, source_target_pairs={{0,8},{4,12},{8,0},{12,4},{1,9},{5,13},{9,1},{13,5},{2,10},{6,14},... | collective-permute-start | bytes 393224 | tf_op jit(solution)/shard_map/ppermute | solution.py:452
  12.5 26.5 %collective-permute-start.4 = (bf16[128,512]{1,0:T(8,128)(2,1)S(1)}, bf16[128,512]{1,0:T(8,128)(2,1)S(1)}, u32[]{:S(2)}, u32[]{:S(2)}) collective-permute-start(bf16[128,512]{1,0:T(8,128)(2,1)S(1)} %constant_dynamic-slice_fusion), channel_id=1, source_target_pairs={{0,4},{4,8},{8,12},{12,0},{1,5},{5,9},{9,13},{13,1},{2,6},{6,10},{... | collective-permute-start | bytes 393224 | tf_op jit(solution)/shard_map/ppermute | solution.py:452
  32.8 24.2 %collective-permute-start.1 = (bf16[128,1024]{1,0:T(8,128)(2,1)}, bf16[128,1024]{1,0:T(8,128)(2,1)S(1)}, u32[]{:S(2)}, u32[]{:S(2)}) collective-permute-start(bf16[128,1024]{1,0:T(8,128)(2,1)} %get-tuple-element.15), channel_id=1, source_target_pairs={{0,4},{4,8},{8,12},{12,0},{1,5},{5,9},{9,13},{13,1},{2,6},{6,10},{... | collective-permute-start | bytes 786440 | tf_op jit(solution)/shard_map/ppermute | solution.py:468
  32.8 24.2 %copy-start.3 = (bf16[128,512]{1,0:T(8,128)(2,1)}, bf16[128,512]{1,0:T(8,128)(2,1)S(1)}, u32[]{:S(2)}) copy-start(bf16[128,512]{1,0:T(8,128)(2,1)S(1)} %collective-permute-done.8.refs_9_) | copy-start | bytes 393220
  32.9 6.3 %collective-permute-start.9 = (bf16[128,512]{1,0:T(8,128)(2,1)S(1)}, bf16[128,512]{1,0:T(8,128)(2,1)S(1)}, u32[]{:S(2)}, u32[]{:S(2)}) collective-permute-start(bf16[128,512]{1,0:T(8,128)(2,1)S(1)} %collective-permute-done.8.refs_9_), channel_id=1, source_target_pairs={{0,16},{16,0},{1,17},{17,1},{2,18},{18,2},{3,19},{19,3},{4,20},{20... | collective-permute-start | bytes 393224 | tf_op jit(solution)/shard_map/ppermute | solution.py:453
  34.2 22.9 %collective-permute-start.2 = (bf16[128,1024]{1,0:T(8,128)(2,1)}, bf16[128,1024]{1,0:T(8,128)(2,1)S(1)}, u32[]{:S(2)}, u32[]{:S(2)}) collective-permute-start(bf16[128,1024]{1,0:T(8,128)(2,1)} %get-tuple-element.16), channel_id=1, source_target_pairs={{0,8},{4,12},{8,0},{12,4},{1,9},{5,13},{9,1},{13,5},{2,10},{6,14},... | collective-permute-start | bytes 786440 | tf_op jit(solution)/shard_map/ppermute | solution.py:468
  37.5 19.5 %copy-start.4 = (bf16[128,512]{1,0:T(8,128)(2,1)}, bf16[128,512]{1,0:T(8,128)(2,1)S(1)}, u32[]{:S(2)}) copy-start(bf16[128,512]{1,0:T(8,128)(2,1)S(1)} %collective-permute-done.6.refs_7_) | copy-start | bytes 393220
  37.5 22.6 %collective-permute-start.3 = (bf16[128,1024]{1,0:T(8,128)(2,1)}, bf16[128,1024]{1,0:T(8,128)(2,1)S(1)}, u32[]{:S(2)}, u32[]{:S(2)}) collective-permute-start(bf16[128,1024]{1,0:T(8,128)(2,1)} %get-tuple-element.17), channel_id=1, source_target_pairs={{0,12},{4,0},{8,4},{12,8},{1,13},{5,1},{9,5},{13,9},{2,14},{6,2},{... | collective-permute-start | bytes 786440 | tf_op jit(solution)/shard_map/ppermute | solution.py:468
  38.9 18.1 %copy-start.5 = (bf16[128,512]{1,0:T(8,128)(2,1)}, bf16[128,512]{1,0:T(8,128)(2,1)S(1)}, u32[]{:S(2)}) copy-start(bf16[128,512]{1,0:T(8,128)(2,1)S(1)} %collective-permute-done.4.refs_5_) | copy-start | bytes 393220
  38.9 18.1 %collective-permute-start.7 = (bf16[128,512]{1,0:T(8,128)(2,1)S(1)}, bf16[128,512]{1,0:T(8,128)(2,1)S(1)}, u32[]{:S(2)}, u32[]{:S(2)}) collective-permute-start(bf16[128,512]{1,0:T(8,128)(2,1)S(1)} %collective-permute-done.6.refs_7_), channel_id=1, source_target_pairs={{0,16},{16,0},{1,17},{17,1},{2,18},{18,2},{3,19},{19,3},{4,20},{20... | collective-permute-start | bytes 393224 | tf_op jit(solution)/shard_map/ppermute | solution.py:453
  39.2 17.9 %copy-start.6 = (bf16[128,512]{1,0:T(8,128)(2,1)}, bf16[128,512]{1,0:T(8,128)(2,1)S(1)}, u32[]{:S(2)}) copy-start(bf16[128,512]{1,0:T(8,128)(2,1)S(1)} %collective-permute-done.9.refs_10_) | copy-start | bytes 393220
  39.2 17.9 %collective-permute-start.5 = (bf16[128,512]{1,0:T(8,128)(2,1)S(1)}, bf16[128,512]{1,0:T(8,128)(2,1)S(1)}, u32[]{:S(2)}, u32[]{:S(2)}) collective-permute-start(bf16[128,512]{1,0:T(8,128)(2,1)S(1)} %collective-permute-done.4.refs_5_), channel_id=1, source_target_pairs={{0,16},{16,0},{1,17},{17,1},{2,18},{18,2},{3,19},{19,3},{4,20},{20... | collective-permute-start | bytes 393224 | tf_op jit(solution)/shard_map/ppermute | solution.py:453
  57.0 3.0 %copy-start.7 = (bf16[128,512]{1,0:T(8,128)(2,1)}, bf16[128,512]{1,0:T(8,128)(2,1)S(1)}, u32[]{:S(2)}) copy-start(bf16[128,512]{1,0:T(8,128)(2,1)S(1)} %collective-permute-done.7.refs_8_) | copy-start | bytes 393220
  57.1 3.0 %copy-start.8 = (bf16[128,512]{1,0:T(8,128)(2,1)}, bf16[128,512]{1,0:T(8,128)(2,1)S(1)}, u32[]{:S(2)}) copy-start(bf16[128,512]{1,0:T(8,128)(2,1)S(1)} %collective-permute-done.5.refs_6_) | copy-start | bytes 393220
  57.1 3.0 %copy-start = (bf16[128,1024]{1,0:T(8,128)(2,1)}, bf16[128,1024]{1,0:T(8,128)(2,1)S(1)}, u32[]{:S(2)}) copy-start(bf16[128,1024]{1,0:T(8,128)(2,1)S(1)} %collective-permute-done.1.refs_1_) | copy-start | bytes 786436
  57.1 3.0 %copy-start.1 = (bf16[128,1024]{1,0:T(8,128)(2,1)}, bf16[128,1024]{1,0:T(8,128)(2,1)S(1)}, u32[]{:S(2)}) copy-start(bf16[128,1024]{1,0:T(8,128)(2,1)S(1)} %collective-permute-done.2.refs_2_) | copy-start | bytes 786436
  60.1 0.7 copy-start.2
  66.8 3.9 %collective-permute-start.10 = (bf16[128,512]{1,0:T(8,128)(2,1)}, bf16[128,512]{1,0:T(8,128)(2,1)S(1)}, u32[]{:S(2)}, u32[]{:S(2)}) collective-permute-start(bf16[128,512]{1,0:T(8,128)(2,1)} %get-tuple-element.19), channel_id=1, source_target_pairs={{0,1},{1,2},{2,3},{3,0},{4,5},{5,6},{6,7},{7,4},{8,9},{9,10},{10,1... | collective-permute-start | bytes 393224 | tf_op jit(solution)/shard_map/ppermute | solution.py:500
  67.8 7.0 %collective-permute-start.11 = (bf16[128,512]{1,0:T(8,128)(2,1)}, bf16[128,512]{1,0:T(8,128)(2,1)S(1)}, u32[]{:S(2)}, u32[]{:S(2)}) collective-permute-start(bf16[128,512]{1,0:T(8,128)(2,1)} %get-tuple-element.20), channel_id=1, source_target_pairs={{0,2},{1,3},{2,0},{3,1},{4,6},{5,7},{6,4},{7,5},{8,10},{9,11},{10,... | collective-permute-start | bytes 393224 | tf_op jit(solution)/shard_map/ppermute | solution.py:500
  68.7 6.8 %collective-permute-start.12 = (bf16[128,512]{1,0:T(8,128)(2,1)}, bf16[128,512]{1,0:T(8,128)(2,1)S(1)}, u32[]{:S(2)}, u32[]{:S(2)}) collective-permute-start(bf16[128,512]{1,0:T(8,128)(2,1)} %get-tuple-element.21), channel_id=1, source_target_pairs={{0,3},{1,0},{2,1},{3,2},{4,7},{5,4},{6,5},{7,6},{8,11},{9,8},{10,9... | collective-permute-start | bytes 393224 | tf_op jit(solution)/shard_map/ppermute | solution.py:500
  70.7 4.7 %copy-start.9 = (bf16[128,512]{1,0:T(8,128)(2,1)}, bf16[128,512]{1,0:T(8,128)(2,1)S(1)}, u32[]{:S(2)}) copy-start(bf16[128,512]{1,0:T(8,128)(2,1)S(1)} %collective-permute-done.10.refs_1_) | copy-start | bytes 393220
  74.8 0.7 copy-start.10
  75.5 0.6 copy-start.11

commit v2 on v1

v2 whole, which is shorter than its diff:
```python
import functools

import jax
import jax.numpy as jnp
from jax import lax
from jax.experimental import pallas as pl
from jax.experimental.pallas import tpu as pltpu
from jax.sharding import PartitionSpec as P

EPS = 1e-06
CHUNKS = 1
F32 = jnp.float32
BF16 = jnp.bfloat16
VMEM = pltpu.VMEM
HBM = pltpu.HBM


def whole(space=VMEM):
    return pl.BlockSpec(memory_space=space)


def fetch(sources, targets, sems):
    copies = [
        pltpu.make_async_copy(source, target, sems.at[i])
        for i, (source, target) in enumerate(zip(sources, targets))
    ]
    for copy in copies:
        copy.start()
    return copies


def like(array):
    return VMEM(array.shape, array.dtype)


def limit(mebibytes):
    return pltpu.CompilerParams(vmem_limit_bytes=mebibytes << 20)


def dot(a, b, contract=((1,), (0,)), precision=None):
    return lax.dot_general(
        a, b, (contract, ((), ())), precision=precision, preferred_element_type=F32
    )


def head_ones(width, size):
    row = lax.broadcasted_iota(jnp.int32, (width, width), 0) // size
    col = lax.broadcasted_iota(jnp.int32, (width, width), 1) // size
    return jnp.where(row == col, 1.0, 0.0).astype(BF16)


def head_sum(values, ones):
    high = values.astype(BF16)
    low = (values - high.astype(F32)).astype(BF16)
    return dot(high, ones) + dot(low, ones)


def head_mask(first, group, steps, width, size):
    sub = lax.broadcasted_iota(jnp.int32, (group * steps, width), 0) // steps + first
    lane = lax.broadcasted_iota(jnp.int32, (group * steps, width), 1) // size
    return sub == lane


def block_of(axis, size):
    return pl.ds(pl.multiple_of(lax.axis_index(axis) * size, size), size)


def statistics(steps, tok_ref, gain_ref, beta_ref, decay_ref, stat_ref):
    raw = jnp.concatenate([tok_ref[:, t, :].astype(F32) for t in range(steps)], 0)
    scaled = (raw * gain_ref[...]).astype(BF16)
    count = beta_ref.shape[0]
    stat_ref[:count, :] = dot(beta_ref[...], scaled, ((1,), (1,)))
    stat_ref[count : 2 * count, :] = dot(decay_ref[...], scaled, ((1,), (1,)))
    ones = jnp.ones((8, raw.shape[1]), F32)
    total = dot(ones, raw * raw, ((1,), (1,)), lax.Precision.HIGHEST)
    stat_ref[2 * count : 2 * count + 8, :] = total


def project_kernel(chunks, x_ref, gain_ref, weight_ref, *outs):
    owners, seqs, steps, _ = x_ref.shape
    each = seqs // chunks
    gain = gain_ref[0:1, :]
    rows = []
    for d in range(owners):
        scaled = [(x_ref[d, :, t, :].astype(F32) * gain).astype(BF16) for t in range(steps)]
        for c in range(chunks):
            rows += [x[c * each : (c + 1) * each] for x in scaled]
    x = jnp.concatenate(rows, 0)
    size = each * steps
    width = weight_ref.shape[1]
    block = min(width, 256)
    for first in range(0, width, block):
        lanes = slice(first, first + block)
        product = dot(x, weight_ref[:, lanes])
        for i, out in enumerate(outs):
            c, d = divmod(i, owners)
            start = (d * chunks + c) * size
            out[:, lanes] = product[start : start + size].astype(out.dtype)


def project(x, gain, weight, chunks):
    owners, seqs, steps, _ = x.shape
    width = weight.shape[1]
    outs = pl.pallas_call(
        functools.partial(project_kernel, chunks),
        out_shape=[
            jax.ShapeDtypeStruct((seqs * steps // chunks, width), F32 if d == 0 else BF16)
            for _ in range(chunks)
            for d in range(owners)
        ],
        in_specs=[whole()] * 3,
        out_specs=[whole()] * (owners * chunks),
        compiler_params=limit(12),
        cost_estimate=pl.CostEstimate(
            flops=2 * x.size * width, bytes_accessed=4 * x.size, transcendentals=0
        ),
        name="project",
    )(x, gain, weight)
    return [outs[c * owners : (c + 1) * owners] for c in range(chunks)]


def spread_heads(ref, value, offset, stride, seqs, heads, steps, size, t):
    for h in range(heads):
        tile, lane = divmod(h * size, 128)
        part = value[:, tile * 128 : (tile + 1) * 128]
        if lane:
            part = pltpu.roll(part, 128 - lane, 1)
        ref[pl.ds(offset + h * steps + t, seqs, stride=stride), :] = part


def put_rows(ref, start, count, value, stride=None):
    for m in range(ref.shape[0]):
        ref[m, pl.ds(start, count, stride=stride), :] = value[:, m * 128 : (m + 1) * 128]


def get_rows(ref, start, count, stride=None):
    return jnp.concatenate(
        [ref[m, pl.ds(start, count, stride=stride), :] for m in range(ref.shape[0])], 1
    )


def own_heads(product, masks, group, steps):
    tile = group * steps
    total = None
    for m, mask in enumerate(masks):
        part = jnp.where(mask, product[m * tile : (m + 1) * tile], 0.0)
        total = part if total is None else total + part
    shift = steps
    acc = total
    for _ in range(group - 1):
        acc = acc + pltpu.roll(total, shift, 0)
        shift += steps
    return acc


def early_kernel(steps, size, axes, count, *refs):
    inputs = 12 + count
    sources, refs = refs[:inputs], refs[inputs:]
    outputs = 5 if count else 4
    outs, refs = refs[:outputs], refs[outputs:]
    out_ref, low_ref, stat_ref, const_ref = outs[:4]
    held, (kscr, pscr, uscr, gscr, sems) = refs[:12], refs[12:]
    k_ref, v_ref, b_ref, d_ref, a_ref, s0_ref = held[:6]
    tok_ref, gain_ref, beta_ref, decay_ref, base_ref, last_ref = held[6:]
    seqs, _, width = s0_ref.shape
    local = tok_ref.shape[2]
    part = block_of(axes[-1], local)
    views = list(sources[:7]) + [ref.at[:, part] for ref in sources[7:10]] + list(sources[10:12])
    copies = fetch(views, held, sems)
    if count:
        wide = sources[12].shape[1]
        targets = [outs[4].at[:, i * wide : (i + 1) * wide] for i in range(count)]
        copies += fetch(sources[12:], targets, sems.at[pl.ds(12, count)])
    for copy in copies[:5]:
        copy.wait()
    heads = width // size
    group = 8 // steps
    ones = head_ones(width, size)
    masks = [head_mask(g * group, group, steps, width, size) for g in range(heads // group)]
    pick = jnp.where(
        lax.broadcasted_iota(jnp.int32, (heads, width), 0)
        == lax.broadcasted_iota(jnp.int32, (heads, width), 1) // size,
        1.0,
        0.0,
    )
    keys = [k_ref[:, t, :].astype(F32) for t in range(steps)]
    for t in range(steps):
        spread_heads(kscr, keys[t], 0, heads * steps, seqs, heads, steps, size, t)
    pairs = [(t, r) for t in range(steps) for r in range(t + 1)]
    sums = head_sum(jnp.concatenate([keys[t] * keys[r] for t, r in pairs], 0), ones)
    raw = {p: sums[i * seqs : (i + 1) * seqs] for i, p in enumerate(pairs)}
    inv = [lax.rsqrt(raw[t, t] + EPS) for t in range(steps)]

    copies[5].wait()

    def read(s, carry):
        kb = kscr[pl.ds(s * heads * steps, heads * steps), :][:, :size].astype(BF16)
        seen = own_heads(dot(kb, s0_ref[s].astype(BF16)), masks, group, steps)
        put_rows(pscr, s * 8, 8, seen)
        return carry

    lax.fori_loop(0, seqs, read, 0, unroll=8)
    highest = lax.Precision.HIGHEST
    cumul, solved = [], []
    for t in range(steps):
        live = jnp.where(a_ref[...] > t, 1.0, 0.0)
        log = dot(d_ref[t] * live, pick, ((0,), (0,)), highest)
        strength = dot(jax.nn.sigmoid(b_ref[t]) * live, pick, ((0,), (0,)), highest)
        cumul.append(log if t == 0 else cumul[-1] + log)
        seen = get_rows(pscr, t, seqs, 8) * inv[t]
        rest = v_ref[:, t, :].astype(F32) - jnp.exp(cumul[t]) * seen
        for r in range(t):
            rest = rest - jnp.exp(cumul[t] - cumul[r]) * (raw[t, r] * inv[t] * inv[r]) * solved[r]
        solved.append(strength * rest)
    for t in range(steps):
        add = jnp.exp(cumul[-1] - cumul[t]) * inv[t] * solved[t]
        for g in range(group):
            put_rows(uscr, g * steps + t, seqs, add, 8)
    gscr[...] = jnp.exp(cumul[-1])

    def write(s, carry):
        ub = get_rows(uscr, s * 8, 8)
        wide = jnp.concatenate([jnp.where(m, ub, 0.0) for m in masks], 0).astype(BF16)
        kb = kscr[pl.ds(s * heads * steps, heads * steps), :][:, :size].astype(BF16)
        new = gscr[pl.ds(s, 1), :] * s0_ref[s] + dot(kb, wide, ((0,), (0,)))
        out_ref[s] = new
        low_ref[s] = new.astype(BF16)
        return carry

    lax.fori_loop(0, seqs, write, 0, unroll=8)
    for copy in copies[6:]:
        copy.wait()
    statistics(steps, tok_ref, gain_ref, beta_ref, decay_ref, stat_ref)
    entry = jnp.where(
        lax.broadcasted_iota(jnp.int32, (size, width), 0)
        == lax.broadcasted_iota(jnp.int32, (size, width), 1) % size,
        1.0,
        0.0,
    )
    const_ref[0:1, :] = dot(base_ref[...], pick, precision=highest)
    const_ref[1:2, :] = dot(last_ref[...], entry, precision=highest)


def early(axes, state, prev, tokens, in_gain, w_beta, w_decay, decay_base, out_gain, weights):
    prev_keys, prev_values, prev_beta, prev_decay, accepted = prev
    seqs, size, width = state.shape
    _, steps, local = tokens.shape
    heads = width // size
    heads_all = w_beta.shape[1]
    arrays = (
        prev_keys,
        prev_values,
        jnp.transpose(prev_beta, (1, 2, 0)),
        jnp.transpose(prev_decay, (1, 2, 0)),
        accepted.reshape(1, -1),
        state,
        tokens,
        in_gain.reshape(1, -1),
        w_beta.T,
        w_decay.T,
        decay_base.reshape(1, -1),
        out_gain.reshape(1, -1),
    )
    held = [like(a) for a in arrays]
    held[7] = VMEM((1, local), F32)
    held[8] = held[9] = VMEM((heads_all, local), BF16)
    shapes = [
        jax.ShapeDtypeStruct(state.shape, F32),
        jax.ShapeDtypeStruct(state.shape, BF16),
        jax.ShapeDtypeStruct((2 * heads_all + 8, seqs * steps), F32),
        jax.ShapeDtypeStruct((8, width), F32),
    ]
    if weights:
        rows, columns = weights[0].shape
        shapes.append(jax.ShapeDtypeStruct((rows, columns * len(weights)), BF16))
    return pl.pallas_call(
        functools.partial(early_kernel, steps, size, axes, len(weights)),
        out_shape=shapes,
        in_specs=[whole(HBM)] * (12 + len(weights)),
        out_specs=[whole()] * len(shapes),
        scratch_shapes=held
        + [
            VMEM((seqs * heads * steps, 128), F32),
            VMEM((width // 128, seqs * 8, 128), F32),
            VMEM((width // 128, seqs * 8, 128), F32),
            VMEM((seqs, width), F32),
            pltpu.SemaphoreType.DMA((12 + len(weights),)),
        ],
        cost_estimate=pl.CostEstimate(
            flops=seqs * 4000000, bytes_accessed=8 * state.size, transcendentals=0
        ),
        compiler_params=limit(20),
        name="early",
    )(*[pltpu.with_memory_space_constraint(a, HBM) for a in arrays + tuple(weights)])


def propose_kernel(dims, axes, parts, sources, blocks, first, stat_ref, const_ref, s_ref, *refs):
    steps, size, features, heads_all = dims
    part_refs, refs = refs[:parts], refs[parts:]
    block_refs, refs = refs[:sources], refs[sources:]
    out_refs, (kscr, pscr, wo, sems) = refs[:-4], refs[-4:]
    seqs = part_refs[0].shape[0] // steps
    width = s_ref.shape[2]
    heads = width // size
    group = 8 // steps
    place = [lax.axis_index(axis) for axis in axes]
    tp = place[-1]

    targets = [wo.at[lax.bitwise_xor(place[1], mark)] for mark in blocks]
    copies = fetch(block_refs, targets, sems)

    ones = head_ones(width, size)
    masks = [head_mask(g * group, group, steps, width, size) for g in range(heads // group)]
    rows = seqs * steps
    stat = stat_ref[...]
    count = stat.shape[0]
    src = lax.broadcasted_iota(jnp.int32, (count, width), 0)
    head = lax.broadcasted_iota(jnp.int32, (count, width), 1) // size + tp * heads
    highest = lax.Precision.HIGHEST
    flat = stat.T
    base, gain = const_ref[0:1, :], const_ref[1:2, :]

    def take(row):
        return dot(flat, jnp.where(src == row, 1.0, 0.0), precision=highest)

    scale = lax.rsqrt(take(2 * heads_all) / features + EPS)
    strength = jax.nn.sigmoid(scale * take(head))
    rate = scale * take(heads_all + head)
    log = -base * (jnp.maximum(rate, 0.0) + jnp.log1p(jnp.exp(-jnp.abs(rate))))

    def column(w):
        lanes = slice(w * width, (w + 1) * width)
        total = part_refs[0][:, lanes].astype(F32)
        for ref in part_refs[1:]:
            total = total + ref[:, lanes].astype(F32)
        return total * scale

    query, key = column(0), column(1)
    squares = head_sum(jnp.concatenate([query * query, key * key], 0), ones)
    query = query * (lax.rsqrt(squares[:rows] + EPS) * size ** (-0.5))
    key = key * lax.rsqrt(squares[rows:] + EPS)

    def at(array, t):
        return array[t * seqs : (t + 1) * seqs]

    stride = 2 * heads * steps
    for t in range(steps):
        spread_heads(kscr, at(query, t), 0, stride, seqs, heads, steps, size, t)
        spread_heads(kscr, at(key, t), heads * steps, stride, seqs, heads, steps, size, t)
    below = [(t, r) for t in range(steps) for r in range(t)]
    inside = [(t, r) for t in range(steps) for r in range(t + 1)]
    products = [at(key, t) * at(key, r) for t, r in below]
    products += [at(query, t) * at(key, r) for t, r in inside]
    sums = head_sum(jnp.concatenate(products, 0), ones)
    k_k = {p: at(sums, i) for i, p in enumerate(below)}
    q_k = {p: at(sums, len(below) + i) for i, p in enumerate(inside)}
    upper = lax.broadcasted_iota(jnp.int32, (8, width), 0) < steps

    def read(s, carry):
        vectors = kscr[pl.ds(s * stride, stride), :][:, :size].astype(BF16)
        seen = dot(vectors, s_ref[first * seqs + s])
        half = heads * steps
        from_query = own_heads(seen[:half], masks, group, steps)
        from_key = own_heads(seen[half:], masks, group, steps)
        put_rows(pscr, s * 8, 8, jnp.where(upper, from_query, from_key))
        return carry

    lax.fori_loop(0, seqs, read, 0, unroll=8)
    value, gate = column(2), column(3)
    cumul, solved, outs = [], [], []
    for t in range(steps):
        cumul.append(at(log, t) if t == 0 else cumul[-1] + at(log, t))
        grown = jnp.exp(cumul[t])
        rest = at(value, t) - grown * get_rows(pscr, steps + t, seqs, 8)
        out = grown * get_rows(pscr, t, seqs, 8)
        for r in range(t):
            decay = jnp.exp(cumul[t] - cumul[r])
            rest = rest - decay * k_k[t, r] * solved[r]
            out = out + decay * q_k[t, r] * solved[r]
        solved.append(at(strength, t) * rest)
        outs.append(out + q_k[t, t] * solved[t])
    output = jnp.concatenate(outs, 0)
    mean = head_sum(output * output, ones) * (1.0 / size)
    gated = output * lax.rsqrt(mean + EPS) * gain * (gate / (1.0 + jnp.exp(-gate)))
    gated = gated.astype(BF16)
    if not blocks:
        out_refs[0][...] = gated
        return
    for copy in copies:
        copy.wait()
    n = wo.shape[0]
    for s in list(range(1, n)) + [0]:
        out_refs[s][...] = dot(gated, wo[lax.rem(tp + s, n)]).astype(out_refs[s].dtype)


def propose(axes, stat, consts, state, parts, blocks, block_arrays, n_tp, dims, seqs, first):
    steps, size = dims[0], dims[1]
    width = state.shape[2]
    heads = width // size
    rows = seqs * steps
    if blocks:
        share = dims[2] // n_tp
        shapes = [
            jax.ShapeDtypeStruct((rows, share), F32 if s == 0 else BF16) for s in range(n_tp)
        ]
        wo = VMEM((n_tp, width, share), BF16)
    else:
        shapes = [jax.ShapeDtypeStruct((rows, width), BF16)]
        wo = VMEM((8, 128), F32)
    return pl.pallas_call(
        functools.partial(
            propose_kernel, dims, axes, len(parts), len(block_arrays), blocks, first
        ),
        out_shape=shapes,
        in_specs=[whole()] * (3 + len(parts)) + [whole(HBM)] * len(block_arrays),
        out_specs=[whole()] * len(shapes),
        scratch_shapes=[
            VMEM((seqs * 2 * heads * steps, 128), F32),
            VMEM((width // 128, seqs * 8, 128), F32),
            wo,
            pltpu.SemaphoreType.DMA((max(1, len(blocks)),)),
        ],
        compiler_params=limit(24),
        cost_estimate=pl.CostEstimate(
            flops=seqs * 4000000, bytes_accessed=4 * state.size, transcendentals=0
        ),
        name="propose",
    )(stat, consts, state, *parts, *block_arrays)


def finish_kernel(steps, chunks, *refs):
    ins, out_ref = refs[:-1], refs[-1]
    per = len(ins) // chunks
    each = out_ref.shape[0] // chunks
    for c in range(chunks):
        total = ins[c * per][...].astype(F32)
        for ref in ins[c * per + 1 : (c + 1) * per]:
            total = total + ref[...].astype(F32)
        for t in range(steps):
            out_ref[c * each : (c + 1) * each, t, :] = total[t * each : (t + 1) * each].astype(
                out_ref.dtype
            )


def finish(pieces, seqs, steps):
    chunks = len(pieces)
    flat = [a for piece in pieces for a in piece]
    return pl.pallas_call(
        functools.partial(finish_kernel, steps, chunks),
        out_shape=jax.ShapeDtypeStruct((seqs, steps, flat[0].shape[1]), BF16),
        in_specs=[whole()] * len(flat),
        out_specs=whole(),
        compiler_params=limit(8),
        name="finish",
    )(*flat)


def body(sizes, *args):
    return layer(sizes, *args)


def layer(
    sizes,
    tokens,
    in_gain,
    w_query,
    w_key,
    w_value,
    w_gate,
    w_beta,
    w_decay,
    decay_base,
    out_gain,
    w_out,
    state,
    prev_keys,
    prev_values,
    prev_beta,
    prev_decay,
    accepted,
):
    n_grp, n_kv, n_tp = sizes
    seqs, steps, local = tokens.shape
    size = out_gain.shape[0]
    features = in_gain.shape[0]
    heads_all = w_beta.shape[1]
    dims = (steps, size, features, heads_all)
    square = n_kv == n_tp and n_kv & (n_kv - 1) == 0 and n_grp == 2
    chunks = CHUNKS if square else 1
    each = seqs // chunks
    axes = ("grp", "kv", "tp")
    weights = (w_query, w_key, w_value, w_gate)
    prev = (prev_keys, prev_values, prev_beta, prev_decay, accepted)

    def ring(n, s):
        return [(i, (i + s) % n) for i in range(n)]

    if square:
        n = n_kv
        turn = [(k * n + t, t * n + (k - t) % n) for k in range(n) for t in range(n)]
        turned = lax.ppermute(tokens, ("kv", "tp"), turn)
    new_state, low, stat, consts, *staged = early(
        axes, state, prev, tokens, in_gain, w_beta, w_decay, decay_base, out_gain,
        weights if square else (),
    )
    if square:
        own_rows = lax.dynamic_slice_in_dim(
            in_gain.reshape(1, -1), lax.axis_index("kv") * local, local, 1
        )
        own_rows = jnp.broadcast_to(own_rows, (8, local))
        staged, later = lax.optimization_barrier((staged, w_out))
        turned, staged = lax.optimization_barrier((turned, staged))
        arrays, marks = [w_out], [0]
        bits = [n >> i for i in range(1, n.bit_length())]

        def swap(array, bit):
            return lax.ppermute(array, "kv", [(i, i ^ bit) for i in range(n)])

        for bit in bits:
            arrays.append(swap(later, bit))
            marks.append(bit)
        gathered = lax.all_gather(turned, "tp")
        parts = project(gathered, own_rows, staged[0], chunks)
        parts = [
            [piece[0]] + [lax.ppermute(piece[d], "kv", ring(n, d)) for d in range(1, n)]
            for piece in parts
        ]
        stat, arrays, parts[0][0] = lax.optimization_barrier((stat, arrays, parts[0][0]))
        for i, bit in enumerate(bits[1:], 1):
            for j in range(len(arrays)):
                mark = marks[j] ^ bit
                if mark not in marks:
                    arrays.append(swap(arrays[j], bit))
                    marks.append(mark)
    else:
        arrays, marks = [], []
        x = lax.all_gather(tokens, "tp", axis=2, tiled=True)
        x = jnp.transpose(x, (1, 0, 2)).reshape(seqs * steps, -1)
        x = (x.astype(F32) * in_gain).astype(BF16)
        full = [lax.all_gather(w, "kv", axis=0, tiled=True) for w in weights]
        products = [jnp.dot(x, w, preferred_element_type=F32) for w in full]
        parts = [[jnp.concatenate(products, 1)]]

    stat_all = jnp.sum(lax.all_gather(stat, "tp"), 0)
    by_step = stat_all.reshape(stat_all.shape[0], steps, seqs)
    pieces = []
    for c in range(chunks):
        own = by_step[:, :, c * each : (c + 1) * each].reshape(stat_all.shape[0], -1)
        out = propose(
            axes, own, consts, low, parts[c], marks, arrays, n_tp, dims, each, c
        )
        if square:
            pieces.append(
                [out[0]] + [lax.ppermute(out[s], "tp", ring(n_tp, s)) for s in range(1, n_tp)]
            )
        else:
            full = lax.all_gather(w_out, "kv", axis=1, tiled=True)
            terms = jnp.dot(out[0], full, preferred_element_type=F32).astype(BF16)
            pieces.append([lax.psum_scatter(terms, "tp", scatter_dimension=1, tiled=True)])
    return finish(pieces, seqs, steps), new_state


def solution(mesh):
    rows = P(("grp", "kv"), None, "tp")
    matrix = P("kv", "tp")
    placed = (
        rows,
        P(),
        matrix,
        matrix,
        matrix,
        matrix,
        P(),
        P(),
        P("tp"),
        P(),
        P("tp", "kv"),
        rows,
        rows,
        rows,
        rows,
        rows,
        P(("grp", "kv")),
    )
    sizes = (mesh.shape["grp"], mesh.shape["kv"], mesh.shape["tp"])
    return jax.shard_map(
        functools.partial(body, sizes),
        mesh=mesh,
        in_specs=placed,
        out_specs=(rows, rows),
        check_vma=False,
    )
```

time: 78.4 us -> 62.5 us (0.80)
  the two profiles are of different devices: /device:TPU:9 before, /device:TPU:1 now
where the time goes in v2:
time: 62.5 us; the launch traced here: 62.3 us
  waiting for transfers between devices  22.8 us (36%)
  starting transfers between devices  13.7 us (22%)
  blocking collectives  13.6 us (22%)
  Pallas kernels  10.7 us (17%)
  local copies, waits for them, and re-layouts  0.77 us (1%)
  between operations  0.7 us (1%)
    ppermute x3, waiting for transfers between devices, layer(): lax.ppermute(piece[d], 'kv', ring(n, d))  10 us
    all_gather x1, blocking collectives, layer(): gathered = lax.all_gather(turned, 'tp')  7.27 us
    ppermute x3, waiting for transfers between devices, layer(): lax.ppermute(out[s], 'tp', ring(n_tp, s))  6.56 us
    all_gather x1, blocking collectives, layer(): stat_all = jnp.sum(lax.all_gather(stat, 'tp'), 0)  6.38 us
    ppermute x3, waiting for transfers between devices, swap(): return lax.ppermute(array, 'kv', [(i, i ^ bit) for i in range(n)])  6.25 us
    pallas_call x1, Pallas kernels, early(): pl.pallas_call(functools.partial(early_kernel, steps, size, axes, len(wei...  5.39 us
    ppermute x1, starting transfers between devices, layer(): turned = lax.ppermute(tokens, ('kv', 'tp'), turn)  5.08 us
    ppermute x3, starting transfers between devices, layer(): lax.ppermute(piece[d], 'kv', ring(n, d))  3.51 us
  transfers between devices with their start and end apart: 10, of which 5 were waited for; matrix products, arithmetic and copies ran while one was open for 1% of the time, Pallas kernels for 12%

profile of v2, /device:TPU:1, one launch (start us, length us, event | category | flops | bytes accessed | tf_op | source)
XLA Modules:
  0.0 62.3 jit_solution(7724192930465256224)
XLA Ops:
  0.6 0.0 copy-start
  0.6 5.1 %collective-permute-start.2 = (bf16[32,4,512]{2,1,0:T(4,128)(2,1)}, bf16[32,4,512]{2,1,0:T(4,128)(2,1)S(1)}, u32[]{:S(2)}, u32[]{:S(2)}) collective-permute-start(bf16[32,4,512]{2,1,0:T(4,128)(2,1)} %refs_6_.1), channel_id=1, source_target_pairs={{0,0},{1,7},{2,10},{3,13},{4,1},{5,4},{6,11},{7,14},{8,2},{9,5},{1... | collective-permute-start | bytes 393224 | tf_op jit(solution)/shard_map/ppermute | solution.py:501
  5.7 5.4 %early.1 = (f32[32,64,256]{2,1,0:T(8,128)}, bf16[32,64,256]{2,1,0:T(8,128)(2,1)S(1)}, f32[40,128]{1,0:T(8,128)S(1)}, f32[8,256]{1,0:T(8,128)S(1)}, bf16[512,1024]{1,0:T(8,128)(2,1)S(1)}) custom-call(bf16[32,4,256]{2,1,0:T(4,128)(2,1)} %refs_0_.1, bf16[32,4,256]{2,1,0:T(4,128)(2,1)} %refs_1_.1, f32[4,4,32]{2,1,0:T(4,128)} %bitcast.15, f32[4,4,32]{2,1,0:T(4,128)} %bitcast.16, ...), custom_call_target="tpu_custom_call" | custom-call | flops 128000000 | bytes 4194304 | tf_op jit(solution)/shard_map/early/pallas_call | solution.py:276
  11.1 0.0 copy-done
  11.1 0.3 collective-permute-start
  11.5 2.7 %collective-permute-start.1 = (bf16[256,512]{1,0:T(8,128)(2,1)S(1)}, bf16[256,512]{1,0:T(8,128)(2,1)S(1)}, u32[]{:S(2)}, u32[]{:S(2)}) collective-permute-start(bf16[256,512]{1,0:T(8,128)(2,1)S(1)} %copy-done), channel_id=1, source_target_pairs={{0,4},{4,0},{8,12},{12,8},{1,5},{5,1},{9,13},{13,9},{2,6},{6,2},{1... | collective-permute-start | bytes 786440 | tf_op jit(solution)/shard_map/ppermute | solution.py:517
  14.1 0.8 %dynamic-slice.3 = f32[512]{0:T(512)S(1)} dynamic-slice(f32[2048]{0:T(1024)} %param.18, s32[]{:T(128)S(6)} %select_n.3), dynamic_slice_sizes={512} | dynamic-slice | bytes 4100 | tf_op jit(solution)/shard_map/dynamic-slice
  14.9 0.0 collective-permute-done.2
  14.9 7.3 %all-gather = bf16[128,4,512]{2,1,0:T(4,128)(2,1)S(1)} all-gather(bf16[32,4,512]{2,1,0:T(4,128)(2,1)S(1)} %collective-permute-done.2), channel_id=2, replica_groups=mesh['grp'=2,'kv'=4,'tp'=4] {'tp'}, dimensions={0}, use_global_device_ids=true | all-gather | bytes 655360 | tf_op jit(solution)/shard_map/all_gather | solution.py:522
  22.2 1.8 %project.1 = (f32[128,1024]{1,0:T(8,128)S(1)}, bf16[128,1024]{1,0:T(8,128)(2,1)}, bf16[128,1024]{1,0:T(8,128)(2,1)}, bf16[128,1024]{1,0:T(8,128)(2,1)}) custom-call(bf16[4,32,4,512]{3,2,1,0:T(4,128)(2,1)S(1)} %bitcast.10, f32[8,512]{1,0:T(8,128)S(1)} %broadcast_in_dim.2.gain_ref, bf16[512,1024]{1,0:T(8,128)(2,1)S(1)} %get-tuple-element.29.weight_ref), custom_call_target="tpu_custom_call" | custom-call | flops 536870912 | bytes 1048576 | tf_op jit(solution)/shard_map/project/pallas_call | solution.py:104
  24.0 0.2 collective-permute-start.3
  24.2 2.1 %collective-permute-start.4 = (bf16[128,1024]{1,0:T(8,128)(2,1)}, bf16[128,1024]{1,0:T(8,128)(2,1)S(1)}, u32[]{:S(2)}, u32[]{:S(2)}) collective-permute-start(bf16[128,1024]{1,0:T(8,128)(2,1)} %get-tuple-element.36), channel_id=1, source_target_pairs={{0,8},{4,12},{8,0},{12,4},{1,9},{5,13},{9,1},{13,5},{2,10},{6,14},... | collective-permute-start | bytes 786440 | tf_op jit(solution)/shard_map/ppermute | solution.py:525
  26.2 1.3 %collective-permute-start.5 = (bf16[128,1024]{1,0:T(8,128)(2,1)}, bf16[128,1024]{1,0:T(8,128)(2,1)S(1)}, u32[]{:S(2)}, u32[]{:S(2)}) collective-permute-start(bf16[128,1024]{1,0:T(8,128)(2,1)} %get-tuple-element.37), channel_id=1, source_target_pairs={{0,12},{4,0},{8,4},{12,8},{1,13},{5,1},{9,5},{13,9},{2,14},{6,2},{... | collective-permute-start | bytes 786440 | tf_op jit(solution)/shard_map/ppermute | solution.py:525
  27.5 0.0 collective-permute-done.refs_5_
  27.5 0.0 collective-permute-done.1.refs_6_
  27.5 0.2 collective-permute-start.6
  27.7 6.4 %all-gather.1 = f32[160,128]{1,0:T(8,128)S(1)} all-gather(f32[40,128]{1,0:T(8,128)S(1)} %get-tuple-element.31), channel_id=3, replica_groups=mesh['grp'=2,'kv'=4,'tp'=4] {'tp'}, dimensions={0}, use_global_device_ids=true | all-gather | bytes 102400 | tf_op jit(solution)/shard_map/all_gather | solution.py:544
  34.1 0.0 collective-permute-done.3.refs_1_
  34.1 10.0 %collective-permute-done.4.refs_2_ = bf16[128,1024]{1,0:T(8,128)(2,1)S(1)} collective-permute-done((bf16[128,1024]{1,0:T(8,128)(2,1)}, bf16[128,1024]{1,0:T(8,128)(2,1)S(1)}, u32[]{:S(2)}, u32[]{:S(2)}) %collective-permute-start.4) | collective-permute-done | bytes 262176 | tf_op jit(solution)/shard_map/ppermute | solution.py:525
  44.1 0.0 collective-permute-done.5.refs_3_
  44.1 6.2 %collective-permute-done.6.refs_7_ = bf16[256,512]{1,0:T(8,128)(2,1)S(1)} collective-permute-done((bf16[256,512]{1,0:T(8,128)(2,1)S(1)}, bf16[256,512]{1,0:T(8,128)(2,1)S(1)}, u32[]{:S(2)}, u32[]{:S(2)}) %collective-permute-start.6) | collective-permute-done | bytes 262176 | tf_op jit(solution)/shard_map/ppermute | solution.py:517
  50.4 2.7 %propose.1 = (f32[128,512]{1,0:T(8,128)S(1)}, bf16[128,512]{1,0:T(8,128)(2,1)S(1)}, bf16[128,512]{1,0:T(8,128)(2,1)S(1)}, bf16[128,512]{1,0:T(8,128)(2,1)S(1)}) custom-call(f32[40,128]{1,0:T(8,128)S(1)} %reduce_sum.9.stat_ref, f32[8,256]{1,0:T(8,128)S(1)} %get-tuple-element.32.const_ref, bf16[32,64,256]{2,1,0:T(8,128)(2,1)S(1)} %get-tuple-element.33.s_ref, ...), custom_call_target="tpu_custom_call" | custom-call | flops 128000000 | bytes 2097152 | tf_op jit(solution)/shard_map/propose/pallas_call | solution.py:410
  53.0 1.4 %collective-permute-start.7 = (bf16[128,512]{1,0:T(8,128)(2,1)S(1)}, bf16[128,512]{1,0:T(8,128)(2,1)S(1)}, u32[]{:S(2)}, u32[]{:S(2)}) collective-permute-start(bf16[128,512]{1,0:T(8,128)(2,1)S(1)} %get-tuple-element.42), channel_id=1, source_target_pairs={{0,1},{1,2},{2,3},{3,0},{4,5},{5,6},{6,7},{7,4},{8,9},{9,10},{10,1... | collective-permute-start | bytes 393224 | tf_op jit(solution)/shard_map/ppermute | solution.py:554
  54.4 0.5 collective-permute-start.8
  54.9 0.0 collective-permute-start.9
  54.9 2.1 %collective-permute-done.7.refs_1_ = bf16[128,512]{1,0:T(8,128)(2,1)S(1)} collective-permute-done((bf16[128,512]{1,0:T(8,128)(2,1)S(1)}, bf16[128,512]{1,0:T(8,128)(2,1)S(1)}, u32[]{:S(2)}, u32[]{:S(2)}) %collective-permute-start.7) | collective-permute-done | bytes 131104 | tf_op jit(solution)/shard_map/ppermute | solution.py:554
  57.1 3.8 %collective-permute-done.8.refs_2_ = bf16[128,512]{1,0:T(8,128)(2,1)S(1)} collective-permute-done((bf16[128,512]{1,0:T(8,128)(2,1)S(1)}, bf16[128,512]{1,0:T(8,128)(2,1)S(1)}, u32[]{:S(2)}, u32[]{:S(2)}) %collective-permute-start.8) | collective-permute-done | bytes 131104 | tf_op jit(solution)/shard_map/ppermute | solution.py:554
  60.8 0.7 %collective-permute-done.9.refs_3_ = bf16[128,512]{1,0:T(8,128)(2,1)S(1)} collective-permute-done((bf16[128,512]{1,0:T(8,128)(2,1)S(1)}, bf16[128,512]{1,0:T(8,128)(2,1)S(1)}, u32[]{:S(2)}, u32[]{:S(2)}) %collective-permute-start.9) | collective-permute-done | bytes 131104 | tf_op jit(solution)/shard_map/ppermute | solution.py:554
  61.5 0.8 %finish.1 = bf16[32,4,512]{2,1,0:T(4,128)(2,1)} custom-call(f32[128,512]{1,0:T(8,128)S(1)} %get-tuple-element.41.refs_0_, bf16[128,512]{1,0:T(8,128)(2,1)S(1)} %collective-permute-done.7.refs_1_, bf16[128,512]{1,0:T(8,128)(2,1)S(1)} %collective-permute-done.8.refs_2_, bf16[128,512]{1,0:T(8,128)(2,1)S(1)} %collective-permute-done.9.refs_3_), custom_call_target="tpu_custom_call" | custom-call | tf_op jit(solution)/shard_map/finish/pallas_call | solution.py:448
  (2 shorter events, 0.0 us)
Async XLA Ops:
  0.6 10.5 %copy-start = (bf16[256,512]{1,0:T(8,128)(2,1)S(1)}, bf16[256,512]{1,0:T(8,128)(2,1)}, u32[]{:S(2)}) copy-start(bf16[256,512]{1,0:T(8,128)(2,1)} %refs_4_) | copy-start | bytes 786436
  0.6 14.3 %collective-permute-start.2 = (bf16[32,4,512]{2,1,0:T(4,128)(2,1)}, bf16[32,4,512]{2,1,0:T(4,128)(2,1)S(1)}, u32[]{:S(2)}, u32[]{:S(2)}) collective-permute-start(bf16[32,4,512]{2,1,0:T(4,128)(2,1)} %refs_6_.1), channel_id=1, source_target_pairs={{0,0},{1,7},{2,10},{3,13},{4,1},{5,4},{6,11},{7,14},{8,2},{9,5},{1... | collective-permute-start | bytes 393224 | tf_op jit(solution)/shard_map/ppermute | solution.py:501
  11.1 16.4 %collective-permute-start = (bf16[256,512]{1,0:T(8,128)(2,1)S(1)}, bf16[256,512]{1,0:T(8,128)(2,1)S(1)}, u32[]{:S(2)}, u32[]{:S(2)}) collective-permute-start(bf16[256,512]{1,0:T(8,128)(2,1)S(1)} %copy-done), channel_id=1, source_target_pairs={{0,8},{4,12},{8,0},{12,4},{1,9},{5,13},{9,1},{13,5},{2,10},{6,14},... | collective-permute-start | bytes 786440 | tf_op jit(solution)/shard_map/ppermute | solution.py:517
  11.5 16.0 %collective-permute-start.1 = (bf16[256,512]{1,0:T(8,128)(2,1)S(1)}, bf16[256,512]{1,0:T(8,128)(2,1)S(1)}, u32[]{:S(2)}, u32[]{:S(2)}) collective-permute-start(bf16[256,512]{1,0:T(8,128)(2,1)S(1)} %copy-done), channel_id=1, source_target_pairs={{0,4},{4,0},{8,12},{12,8},{1,5},{5,1},{9,13},{13,9},{2,6},{6,2},{1... | collective-permute-start | bytes 786440 | tf_op jit(solution)/shard_map/ppermute | solution.py:517
  24.0 10.1 %collective-permute-start.3 = (bf16[128,1024]{1,0:T(8,128)(2,1)}, bf16[128,1024]{1,0:T(8,128)(2,1)S(1)}, u32[]{:S(2)}, u32[]{:S(2)}) collective-permute-start(bf16[128,1024]{1,0:T(8,128)(2,1)} %get-tuple-element.35), channel_id=1, source_target_pairs={{0,4},{4,8},{8,12},{12,0},{1,5},{5,9},{9,13},{13,1},{2,6},{6,10},{... | collective-permute-start | bytes 786440 | tf_op jit(solution)/shard_map/ppermute | solution.py:525
  24.2 19.9 %collective-permute-start.4 = (bf16[128,1024]{1,0:T(8,128)(2,1)}, bf16[128,1024]{1,0:T(8,128)(2,1)S(1)}, u32[]{:S(2)}, u32[]{:S(2)}) collective-permute-start(bf16[128,1024]{1,0:T(8,128)(2,1)} %get-tuple-element.36), channel_id=1, source_target_pairs={{0,8},{4,12},{8,0},{12,4},{1,9},{5,13},{9,1},{13,5},{2,10},{6,14},... | collective-permute-start | bytes 786440 | tf_op jit(solution)/shard_map/ppermute | solution.py:525
  26.2 17.9 %collective-permute-start.5 = (bf16[128,1024]{1,0:T(8,128)(2,1)}, bf16[128,1024]{1,0:T(8,128)(2,1)S(1)}, u32[]{:S(2)}, u32[]{:S(2)}) collective-permute-start(bf16[128,1024]{1,0:T(8,128)(2,1)} %get-tuple-element.37), channel_id=1, source_target_pairs={{0,12},{4,0},{8,4},{12,8},{1,13},{5,1},{9,5},{13,9},{2,14},{6,2},{... | collective-permute-start | bytes 786440 | tf_op jit(solution)/shard_map/ppermute | solution.py:525
  27.5 22.9 %collective-permute-start.6 = (bf16[256,512]{1,0:T(8,128)(2,1)S(1)}, bf16[256,512]{1,0:T(8,128)(2,1)S(1)}, u32[]{:S(2)}, u32[]{:S(2)}) collective-permute-start(bf16[256,512]{1,0:T(8,128)(2,1)S(1)} %collective-permute-done.refs_5_), channel_id=1, source_target_pairs={{0,4},{4,0},{8,12},{12,8},{1,5},{5,1},{9,13},{13,9},{2,6},{6,2},{1... | collective-permute-start | bytes 786440 | tf_op jit(solution)/shard_map/ppermute | solution.py:517
  53.0 4.0 %collective-permute-start.7 = (bf16[128,512]{1,0:T(8,128)(2,1)S(1)}, bf16[128,512]{1,0:T(8,128)(2,1)S(1)}, u32[]{:S(2)}, u32[]{:S(2)}) collective-permute-start(bf16[128,512]{1,0:T(8,128)(2,1)S(1)} %get-tuple-element.42), channel_id=1, source_target_pairs={{0,1},{1,2},{2,3},{3,0},{4,5},{5,6},{6,7},{7,4},{8,9},{9,10},{10,1... | collective-permute-start | bytes 393224 | tf_op jit(solution)/shard_map/ppermute | solution.py:554
  54.4 6.4 %collective-permute-start.8 = (bf16[128,512]{1,0:T(8,128)(2,1)S(1)}, bf16[128,512]{1,0:T(8,128)(2,1)S(1)}, u32[]{:S(2)}, u32[]{:S(2)}) collective-permute-start(bf16[128,512]{1,0:T(8,128)(2,1)S(1)} %get-tuple-element.43), channel_id=1, source_target_pairs={{0,2},{1,3},{2,0},{3,1},{4,6},{5,7},{6,4},{7,5},{8,10},{9,11},{10,... | collective-permute-start | bytes 393224 | tf_op jit(solution)/shard_map/ppermute | solution.py:554
  54.9 6.6 %collective-permute-start.9 = (bf16[128,512]{1,0:T(8,128)(2,1)S(1)}, bf16[128,512]{1,0:T(8,128)(2,1)S(1)}, u32[]{:S(2)}, u32[]{:S(2)}) collective-permute-start(bf16[128,512]{1,0:T(8,128)(2,1)S(1)} %get-tuple-element.44), channel_id=1, source_target_pairs={{0,3},{1,0},{2,1},{3,2},{4,7},{5,4},{6,5},{7,6},{8,11},{9,8},{10,9... | collective-permute-start | bytes 393224 | tf_op jit(solution)/shard_map/ppermute | solution.py:554

commit v3 on v2

v3 whole, which is shorter than its diff:
```python
import functools

import jax
import jax.numpy as jnp
from jax import lax
from jax.experimental import pallas as pl
from jax.experimental.pallas import tpu as pltpu
from jax.sharding import PartitionSpec as P

EPS = 1e-06
F32 = jnp.float32
BF16 = jnp.bfloat16
VMEM = pltpu.VMEM
HBM = pltpu.HBM


def whole(space=VMEM):
    return pl.BlockSpec(memory_space=space)


def fetch(sources, targets, sems):
    copies = [
        pltpu.make_async_copy(source, target, sems.at[i])
        for i, (source, target) in enumerate(zip(sources, targets))
    ]
    for copy in copies:
        copy.start()
    return copies


def like(array):
    return VMEM(array.shape, array.dtype)


def limit(mebibytes):
    return pltpu.CompilerParams(vmem_limit_bytes=mebibytes << 20)


def dot(a, b, contract=((1,), (0,)), precision=None):
    return lax.dot_general(
        a, b, (contract, ((), ())), precision=precision, preferred_element_type=F32
    )


def head_ones(width, size):
    row = lax.broadcasted_iota(jnp.int32, (width, width), 0) // size
    col = lax.broadcasted_iota(jnp.int32, (width, width), 1) // size
    return jnp.where(row == col, 1.0, 0.0).astype(BF16)


def head_sum(values, ones):
    high = values.astype(BF16)
    low = (values - high.astype(F32)).astype(BF16)
    return dot(high, ones) + dot(low, ones)


def head_mask(first, group, steps, width, size):
    sub = lax.broadcasted_iota(jnp.int32, (group * steps, width), 0) // steps + first
    lane = lax.broadcasted_iota(jnp.int32, (group * steps, width), 1) // size
    return sub == lane


def block_of(axis, size):
    return pl.ds(pl.multiple_of(lax.axis_index(axis) * size, size), size)


def stat_rows(values):
    high = values.astype(BF16).astype(F32)
    return high, values - high


def project_kernel(chunks, x_ref, gain_ref, weight_ref, small_ref, *outs):
    owners, _, steps, local = x_ref.shape
    gain = gain_ref[0:1, :]
    raw, spans, start = [], [], 0
    tokens = [[x_ref[d, :, t, :].astype(F32) for t in range(steps)] for d in range(owners)]
    for first, each in chunks:
        for d in range(owners):
            raw += [x[first : first + each] for x in tokens[d]]
            spans.append(slice(start, start + each * steps))
            start += each * steps
    raw = jnp.concatenate(raw, 0)
    x = (raw * gain).astype(BF16)
    square = raw * raw
    high = square.astype(BF16)
    low = (square - high.astype(F32)).astype(BF16)
    count = small_ref.shape[0]
    unit = (lax.broadcasted_iota(jnp.int32, (128, local), 0) == count).astype(F32).astype(BF16)
    small = jnp.concatenate([small_ref[...], jnp.zeros((128 - count, local), BF16)], 0)
    sums = dot(x, small, ((1,), (1,))) + dot(high, unit, ((1,), (1,))) + dot(low, unit, ((1,), (1,)))
    for out, span in zip(outs, spans):
        rows = span.stop - span.start
        part = sums[span]
        if rows < 128:
            part = jnp.concatenate([part, jnp.zeros((128 - rows, 128), F32)], 0)
        part = part.T
        extra = []
        for first in range(0, 2 * count, count):
            extra += stat_rows(part[first : first + count])
        extra.append(jnp.zeros((count, out.shape[1] - 128 * len(extra)), F32))
        out[rows : rows + count, :] = jnp.concatenate(extra, 1).astype(out.dtype)
    width = weight_ref.shape[1]
    block = min(width, 256)
    for first in range(0, width, block):
        lanes = slice(first, first + block)
        product = dot(x, weight_ref[:, lanes])
        for out, span in zip(outs, spans):
            rows = span.stop - span.start
            out[:rows, lanes] = product[span].astype(out.dtype)


def project(x, gain, weight, small, chunks):
    owners, _, steps, _ = x.shape
    width = weight.shape[1]
    extra = small.shape[0]
    outs = pl.pallas_call(
        functools.partial(project_kernel, chunks),
        out_shape=[
            jax.ShapeDtypeStruct((each * steps + extra, width), F32 if d == 0 else BF16)
            for _, each in chunks
            for d in range(owners)
        ],
        in_specs=[whole()] * 4,
        out_specs=[whole()] * (owners * len(chunks)),
        compiler_params=limit(16),
        cost_estimate=pl.CostEstimate(
            flops=2 * x.size * width, bytes_accessed=4 * x.size, transcendentals=0
        ),
        name="project",
    )(x, gain, weight, small)
    return [list(outs[c * owners : (c + 1) * owners]) for c in range(len(chunks))]


def assemble_kernel(axes, blocks, *refs):
    sources, out_ref, sems = refs[:-2], refs[-2], refs[-1]
    place = [lax.axis_index(axis) for axis in axes]
    targets = []
    for ref, (mark, flip) in zip(sources, blocks):
        target = out_ref.at[lax.bitwise_xor(place[1], mark)]
        if flip is not None:
            count = ref.shape[0]
            row = lax.bitwise_xor(place[0], flip) * count
            target = target.at[pl.ds(pl.multiple_of(row, count), count)]
        targets.append(target)
    for copy in fetch(sources, targets, sems):
        copy.wait()


def assemble(axes, arrays, blocks, n):
    return pl.pallas_call(
        functools.partial(assemble_kernel, axes, blocks),
        out_shape=jax.ShapeDtypeStruct((n,) + arrays[0].shape, arrays[0].dtype),
        in_specs=[whole(HBM)] * len(arrays),
        out_specs=whole(),
        scratch_shapes=[pltpu.SemaphoreType.DMA((len(arrays),))],
        compiler_params=limit(4),
        cost_estimate=pl.CostEstimate(
            flops=4000000, bytes_accessed=8 * arrays[0].size, transcendentals=0
        ),
        name="assemble",
    )(*arrays)


def spread_heads(ref, value, offset, stride, seqs, heads, steps, size, t):
    for h in range(heads):
        tile, lane = divmod(h * size, 128)
        part = value[:, tile * 128 : (tile + 1) * 128]
        if lane:
            part = pltpu.roll(part, 128 - lane, 1)
        ref[pl.ds(offset + h * steps + t, seqs, stride=stride), :] = part


def put_rows(ref, start, count, value, stride=None):
    for m in range(ref.shape[0]):
        ref[m, pl.ds(start, count, stride=stride), :] = value[:, m * 128 : (m + 1) * 128]


def get_rows(ref, start, count, stride=None):
    return jnp.concatenate(
        [ref[m, pl.ds(start, count, stride=stride), :] for m in range(ref.shape[0])], 1
    )


def own_heads(product, masks, group, steps):
    tile = group * steps
    total = None
    for m, mask in enumerate(masks):
        part = jnp.where(mask, product[m * tile : (m + 1) * tile], 0.0)
        total = part if total is None else total + part
    shift = steps
    acc = total
    for _ in range(group - 1):
        acc = acc + pltpu.roll(total, shift, 0)
        shift += steps
    return acc


def early_kernel(steps, size, axes, count, *refs):
    inputs = 12 + count if count else 8
    own = 11 if count else 8
    sources, refs = refs[:inputs], refs[inputs:]
    outputs = 7 if count else 3
    outs, refs = refs[:outputs], refs[outputs:]
    out_ref, low_ref, const_ref = outs[:3]
    held, (kscr, pscr, uscr, gscr, sems) = refs[:own], refs[own:]
    k_ref, v_ref, b_ref, d_ref, a_ref, s0_ref = held[:6]
    base_ref, last_ref = held[6:8]
    seqs, _, width = s0_ref.shape
    views = list(sources[:8])
    if count:
        part = block_of(axes[1], held[8].shape[1])
        views += [ref.at[:, part] for ref in sources[8:11]]
    copies = fetch(views, held, sems)
    if count:
        half = sources[-1].at[block_of(axes[0], outs[6].shape[0])]
        wide = sources[11].shape[1]
        targets = [outs[3].at[:, i * wide : (i + 1) * wide] for i in range(count)]
        copies += fetch(
            [half] + list(sources[11:-1]), [outs[6]] + targets, sems.at[pl.ds(11, count + 1)]
        )
    for copy in copies[:5]:
        copy.wait()
    heads = width // size
    group = 8 // steps
    ones = head_ones(width, size)
    masks = [head_mask(g * group, group, steps, width, size) for g in range(heads // group)]
    pick = jnp.where(
        lax.broadcasted_iota(jnp.int32, (heads, width), 0)
        == lax.broadcasted_iota(jnp.int32, (heads, width), 1) // size,
        1.0,
        0.0,
    )
    keys = [k_ref[:, t, :].astype(F32) for t in range(steps)]
    for t in range(steps):
        spread_heads(kscr, keys[t], 0, heads * steps, seqs, heads, steps, size, t)
    pairs = [(t, r) for t in range(steps) for r in range(t + 1)]
    sums = head_sum(jnp.concatenate([keys[t] * keys[r] for t, r in pairs], 0), ones)
    raw = {p: sums[i * seqs : (i + 1) * seqs] for i, p in enumerate(pairs)}
    inv = [lax.rsqrt(raw[t, t] + EPS) for t in range(steps)]

    copies[5].wait()

    def read(s, carry):
        kb = kscr[pl.ds(s * heads * steps, heads * steps), :][:, :size].astype(BF16)
        seen = own_heads(dot(kb, s0_ref[s].astype(BF16)), masks, group, steps)
        put_rows(pscr, s * 8, 8, seen)
        return carry

    lax.fori_loop(0, seqs, read, 0, unroll=8)
    highest = lax.Precision.HIGHEST
    cumul, solved = [], []
    for t in range(steps):
        live = jnp.where(a_ref[...] > t, 1.0, 0.0)
        log = dot(d_ref[t] * live, pick, ((0,), (0,)), highest)
        strength = dot(jax.nn.sigmoid(b_ref[t]) * live, pick, ((0,), (0,)), highest)
        cumul.append(log if t == 0 else cumul[-1] + log)
        seen = get_rows(pscr, t, seqs, 8) * inv[t]
        rest = v_ref[:, t, :].astype(F32) - jnp.exp(cumul[t]) * seen
        for r in range(t):
            rest = rest - jnp.exp(cumul[t] - cumul[r]) * (raw[t, r] * inv[t] * inv[r]) * solved[r]
        solved.append(strength * rest)
    for t in range(steps):
        add = jnp.exp(cumul[-1] - cumul[t]) * inv[t] * solved[t]
        for g in range(group):
            put_rows(uscr, g * steps + t, seqs, add, 8)
    gscr[...] = jnp.exp(cumul[-1])

    def write(s, carry):
        ub = get_rows(uscr, s * 8, 8)
        wide = jnp.concatenate([jnp.where(m, ub, 0.0) for m in masks], 0).astype(BF16)
        kb = kscr[pl.ds(s * heads * steps, heads * steps), :][:, :size].astype(BF16)
        new = gscr[pl.ds(s, 1), :] * s0_ref[s] + dot(kb, wide, ((0,), (0,)))
        out_ref[s] = new
        low_ref[s] = new.astype(BF16)
        return carry

    lax.fori_loop(0, seqs, write, 0, unroll=8)
    for copy in copies[6:]:
        copy.wait()
    if count:
        outs[4][0:1, :] = held[8][...]
        total = None
        for i, ref in enumerate(held[9:11]):
            rows, every = outs[5].shape[0], ref.shape[0]
            row = lax.broadcasted_iota(jnp.int32, (rows, every), 0) - i * heads
            col = lax.broadcasted_iota(jnp.int32, (rows, every), 1)
            chosen = (row >= 0) & (row < heads) & (col == row + lax.axis_index(axes[2]) * heads)
            term = dot(chosen.astype(F32).astype(BF16), ref[...])
            total = term if total is None else total + term
        outs[5][...] = total.astype(BF16)
    entry = jnp.where(
        lax.broadcasted_iota(jnp.int32, (size, width), 0)
        == lax.broadcasted_iota(jnp.int32, (size, width), 1) % size,
        1.0,
        0.0,
    )
    const_ref[0:1, :] = dot(base_ref[...], pick, precision=highest)
    const_ref[1:2, :] = dot(last_ref[...], entry, precision=highest)


def early(axes, state, prev, decay_base, out_gain, shared):
    prev_keys, prev_values, prev_beta, prev_decay, accepted = prev
    seqs, size, width = state.shape
    steps = prev_keys.shape[1]
    heads = width // size
    arrays = (
        prev_keys,
        prev_values,
        jnp.transpose(prev_beta, (1, 2, 0)),
        jnp.transpose(prev_decay, (1, 2, 0)),
        accepted.reshape(1, -1),
        state,
        decay_base.reshape(1, -1),
        out_gain.reshape(1, -1),
    )
    held = [like(a) for a in arrays]
    shapes = [
        jax.ShapeDtypeStruct(state.shape, F32),
        jax.ShapeDtypeStruct(state.shape, BF16),
        jax.ShapeDtypeStruct((8, width), F32),
    ]
    count = 0
    if shared:
        in_gain, w_beta, w_decay, weights, w_out = shared
        count = len(weights)
        rows, columns = weights[0].shape
        arrays += (in_gain.reshape(1, -1), w_beta.T, w_decay.T) + weights + (w_out,)
        small = VMEM((w_beta.shape[1], rows), BF16)
        held += [VMEM((1, rows), F32), small, small]
        shapes += [
            jax.ShapeDtypeStruct((rows, columns * count), BF16),
            jax.ShapeDtypeStruct((8, rows), F32),
            jax.ShapeDtypeStruct((-(-2 * heads // 8) * 8, rows), BF16),
            jax.ShapeDtypeStruct((w_out.shape[0] // 2, w_out.shape[1]), BF16),
        ]
    return pl.pallas_call(
        functools.partial(early_kernel, steps, size, axes, count),
        out_shape=shapes,
        in_specs=[whole(HBM)] * len(arrays),
        out_specs=[whole()] * len(shapes),
        scratch_shapes=held
        + [
            VMEM((seqs * heads * steps, 128), F32),
            VMEM((width // 128, seqs * 8, 128), F32),
            VMEM((width // 128, seqs * 8, 128), F32),
            VMEM((seqs, width), F32),
            pltpu.SemaphoreType.DMA((len(arrays),)),
        ],
        cost_estimate=pl.CostEstimate(
            flops=seqs * 4000000, bytes_accessed=8 * state.size, transcendentals=0
        ),
        compiler_params=limit(20),
        name="early",
    )(*[pltpu.with_memory_space_constraint(a, HBM) for a in arrays])


def propose_kernel(dims, axis, parts, first, const_ref, s_ref, *refs):
    steps, size, features = dims
    part_refs, wo, refs = refs[:parts], refs[parts], refs[parts + 1 :]
    out_refs, (kscr, pscr) = refs[:-2], refs[-2:]
    width = s_ref.shape[2]
    extra = -(-2 * (width // size) // 8) * 8
    seqs = (part_refs[0].shape[0] - extra) // steps
    heads = width // size
    group = 8 // steps
    ones = head_ones(width, size)
    masks = [head_mask(g * group, group, steps, width, size) for g in range(heads // group)]
    rows = seqs * steps

    def gathered(rows_of, lanes):
        total = part_refs[0][rows_of, lanes].astype(F32)
        for ref in part_refs[1:]:
            total = total + ref[rows_of, lanes].astype(F32)
        return total

    stat = gathered(slice(rows, rows + extra), slice(0, 512))
    logits = stat[:, :128] + stat[:, 128:256]
    total = stat[:, 256:384] + stat[:, 384:]
    flat = jnp.concatenate([logits, total], 0).T[:rows]
    src = lax.broadcasted_iota(jnp.int32, (2 * extra, width), 0)
    head = lax.broadcasted_iota(jnp.int32, (2 * extra, width), 1) // size
    highest = lax.Precision.HIGHEST
    base, gain = const_ref[0:1, :], const_ref[1:2, :]

    def take(row):
        return dot(flat, jnp.where(src == row, 1.0, 0.0), precision=highest)

    scale = lax.rsqrt(take(extra) / features + EPS)
    strength = jax.nn.sigmoid(scale * take(head))
    rate = scale * take(heads + head)
    log = -base * (jnp.maximum(rate, 0.0) + jnp.log1p(jnp.exp(-jnp.abs(rate))))

    def column(w):
        return gathered(slice(0, rows), slice(w * width, (w + 1) * width)) * scale

    query, key = column(0), column(1)
    squares = head_sum(jnp.concatenate([query * query, key * key], 0), ones)
    query = query * (lax.rsqrt(squares[:rows] + EPS) * size ** (-0.5))
    key = key * lax.rsqrt(squares[rows:] + EPS)

    def at(array, t):
        return array[t * seqs : (t + 1) * seqs]

    stride = 2 * heads * steps
    for t in range(steps):
        spread_heads(kscr, at(query, t), 0, stride, seqs, heads, steps, size, t)
        spread_heads(kscr, at(key, t), heads * steps, stride, seqs, heads, steps, size, t)
    below = [(t, r) for t in range(steps) for r in range(t)]
    inside = [(t, r) for t in range(steps) for r in range(t + 1)]
    products = [at(key, t) * at(key, r) for t, r in below]
    products += [at(query, t) * at(key, r) for t, r in inside]
    sums = head_sum(jnp.concatenate(products, 0), ones)
    k_k = {p: at(sums, i) for i, p in enumerate(below)}
    q_k = {p: at(sums, len(below) + i) for i, p in enumerate(inside)}
    upper = lax.broadcasted_iota(jnp.int32, (8, width), 0) < steps

    def read(s, carry):
        vectors = kscr[pl.ds(s * stride, stride), :][:, :size].astype(BF16)
        seen = dot(vectors, s_ref[first + s])
        half = heads * steps
        from_query = own_heads(seen[:half], masks, group, steps)
        from_key = own_heads(seen[half:], masks, group, steps)
        put_rows(pscr, s * 8, 8, jnp.where(upper, from_query, from_key))
        return carry

    lax.fori_loop(0, seqs, read, 0, unroll=8)
    value, gate = column(2), column(3)
    cumul, solved, outs = [], [], []
    for t in range(steps):
        cumul.append(at(log, t) if t == 0 else cumul[-1] + at(log, t))
        grown = jnp.exp(cumul[t])
        rest = at(value, t) - grown * get_rows(pscr, steps + t, seqs, 8)
        out = grown * get_rows(pscr, t, seqs, 8)
        for r in range(t):
            decay = jnp.exp(cumul[t] - cumul[r])
            rest = rest - decay * k_k[t, r] * solved[r]
            out = out + decay * q_k[t, r] * solved[r]
        solved.append(at(strength, t) * rest)
        outs.append(out + q_k[t, t] * solved[t])
    output = jnp.concatenate(outs, 0)
    mean = head_sum(output * output, ones) * (1.0 / size)
    gated = output * lax.rsqrt(mean + EPS) * gain * (gate / (1.0 + jnp.exp(-gate)))
    gated = gated.astype(BF16)
    n = wo.shape[0]
    tp = lax.axis_index(axis)
    for s in list(range(1, len(out_refs))) + [0]:
        block = wo[lax.rem(tp + s, n)] if n > 1 else wo[0]
        out_refs[s][...] = dot(gated, block).astype(out_refs[s].dtype)


def propose(axis, consts, state, parts, wo, dims, first, seqs):
    steps, size = dims[0], dims[1]
    width = state.shape[2]
    heads = width // size
    rows = seqs * steps
    shapes = [
        jax.ShapeDtypeStruct((rows, wo.shape[2]), F32 if s == 0 and wo.shape[0] > 1 else BF16)
        for s in range(wo.shape[0])
    ]
    return pl.pallas_call(
        functools.partial(propose_kernel, dims, axis, len(parts), first),
        out_shape=shapes,
        in_specs=[whole()] * (3 + len(parts)),
        out_specs=[whole()] * len(shapes),
        scratch_shapes=[
            VMEM((seqs * 2 * heads * steps, 128), F32),
            VMEM((width // 128, seqs * 8, 128), F32),
        ],
        compiler_params=limit(12),
        cost_estimate=pl.CostEstimate(
            flops=seqs * 4000000, bytes_accessed=4 * state.size, transcendentals=0
        ),
        name="propose",
    )(consts, state, *parts, wo)


def finish_kernel(steps, chunks, *refs):
    ins, out_ref = refs[:-1], refs[-1]
    per = len(ins) // len(chunks)
    for c, (first, each) in enumerate(chunks):
        total = ins[c * per][...].astype(F32)
        for ref in ins[c * per + 1 : (c + 1) * per]:
            total = total + ref[...].astype(F32)
        for t in range(steps):
            out_ref[first : first + each, t, :] = total[t * each : (t + 1) * each].astype(
                out_ref.dtype
            )


def finish(pieces, chunks, seqs, steps):
    flat = [a for piece in pieces for a in piece]
    return pl.pallas_call(
        functools.partial(finish_kernel, steps, chunks),
        out_shape=jax.ShapeDtypeStruct((seqs, steps, flat[0].shape[1]), BF16),
        in_specs=[whole()] * len(flat),
        out_specs=whole(),
        compiler_params=limit(8),
        name="finish",
    )(*flat)


def split(seqs):
    last = max(8, seqs // 4)
    return ((0, seqs - last), (seqs - last, last)) if seqs % 8 == 0 and seqs > 8 else ((0, seqs),)


def body(sizes, *args):
    return layer(sizes, *args)


def layer(
    sizes,
    tokens,
    in_gain,
    w_query,
    w_key,
    w_value,
    w_gate,
    w_beta,
    w_decay,
    decay_base,
    out_gain,
    w_out,
    state,
    prev_keys,
    prev_values,
    prev_beta,
    prev_decay,
    accepted,
):
    n_grp, n_kv, n_tp = sizes
    seqs, steps, _ = tokens.shape
    heads = decay_base.shape[0]
    size = out_gain.shape[0]
    features = in_gain.shape[0]
    dims = (steps, size, features)
    square = n_kv == n_tp and n_kv & (n_kv - 1) == 0 and n_grp == 2
    chunks = split(seqs) if square else ((0, seqs),)
    axes = ("grp", "kv", "tp")
    weights = (w_query, w_key, w_value, w_gate)
    prev = (prev_keys, prev_values, prev_beta, prev_decay, accepted)

    def ring(n, s):
        return [(i, (i + s) % n) for i in range(n)]

    if square:
        n = n_kv
        turn = [(k * n + t, t * n + (k - t) % n) for k in range(n) for t in range(n)]
        turned = lax.ppermute(tokens, ("kv", "tp"), turn)
    shared = (in_gain, w_beta, w_decay, weights, w_out) if square else None
    new_state, low, consts, *staged = early(axes, state, prev, decay_base, out_gain, shared)
    if square:
        weight, own_gain, small, mine = staged
        turned, weight = lax.optimization_barrier((turned, weight))
        halves, marks = [mine], [0]
        bits = [n >> i for i in range(1, n.bit_length())]

        def swap(array, bit):
            return lax.ppermute(array, "kv", [(i, i ^ bit) for i in range(n)])

        for bit in bits:
            halves.append(swap(mine, bit))
            marks.append(bit)
        gathered = lax.all_gather(turned, "tp")
        parts = project(gathered, own_gain, weight, small, chunks)
        for piece in parts:
            for d in range(1, n):
                piece[d] = lax.ppermute(piece[d], "kv", ring(n, d))
        halves, parts[0][0] = lax.optimization_barrier((halves, parts[0][0]))
        for bit in bits[1:]:
            for j in range(len(halves)):
                if marks[j] ^ bit not in marks:
                    halves.append(swap(halves[j], bit))
                    marks.append(marks[j] ^ bit)
        arrays, blocks = [w_out], [(0, None)]
        for i in range(1, len(halves)):
            other = lax.ppermute(halves[i], "grp", ring(n_grp, 1))
            arrays += [halves[i], other]
            blocks += [(marks[i], 0), (marks[i], 1)]
        wo = assemble(axes, arrays, blocks, n)
    else:
        x = lax.all_gather(tokens, "tp", axis=2, tiled=True)
        x = jnp.transpose(x, (1, 0, 2)).reshape(seqs * steps, -1).astype(F32)
        square_sum = jnp.sum(x * x, -1)
        x = (x * in_gain).astype(BF16)
        full = [lax.all_gather(w, "kv", axis=0, tiled=True) for w in weights]
        products = [jnp.dot(x, w, preferred_element_type=F32) for w in full]
        start = lax.axis_index("tp") * heads
        chosen = [lax.dynamic_slice_in_dim(w, start, heads, 1) for w in (w_beta, w_decay)]
        logits = jnp.dot(x, jnp.concatenate(chosen, 1), preferred_element_type=F32).T
        extra = -(-2 * heads // 8) * 8
        sums = jnp.zeros((extra, sum(p.shape[1] for p in products)), F32)
        sums = sums.at[: 2 * heads, : seqs * steps].set(logits)
        sums = sums.at[0, 256 : 256 + seqs * steps].set(square_sum)
        parts = [[jnp.concatenate([jnp.concatenate(products, 1), sums], 0)]]
        wo = lax.all_gather(w_out, "kv", axis=1, tiled=True)[None]

    pieces = []
    for (first, each), part in zip(chunks, parts):
        out = propose("tp", consts, low, part, wo, dims, first, each)
        if square:
            pieces.append(
                [out[0]] + [lax.ppermute(out[s], "tp", ring(n_tp, s)) for s in range(1, n_tp)]
            )
        else:
            pieces.append([lax.psum_scatter(out[0], "tp", scatter_dimension=1, tiled=True)])
    return finish(pieces, chunks, seqs, steps), new_state


def solution(mesh):
    rows = P(("grp", "kv"), None, "tp")
    matrix = P("kv", "tp")
    placed = (
        rows,
        P(),
        matrix,
        matrix,
        matrix,
        matrix,
        P(),
        P(),
        P("tp"),
        P(),
        P("tp", "kv"),
        rows,
        rows,
        rows,
        rows,
        rows,
        P(("grp", "kv")),
    )
    sizes = (mesh.shape["grp"], mesh.shape["kv"], mesh.shape["tp"])
    return jax.shard_map(
        functools.partial(body, sizes),
        mesh=mesh,
        in_specs=placed,
        out_specs=(rows, rows),
        check_vma=False,
    )
```

time: 62.5 us -> 62.7 us (level)
  the two profiles are of different devices: /device:TPU:1 before, /device:TPU:9 now
where the time goes in v3:
time: 62.7 us; the launch traced here: 62.5 us
  starting transfers between devices  24.3 us (39%)
  waiting for transfers between devices  18 us (29%)
  Pallas kernels  12.1 us (19%)
  blocking collectives  7.45 us (12%)
  between operations  0.72 us (1%)
    ppermute x6, waiting for transfers between devices, layer(): piece[d] = lax.ppermute(piece[d], 'kv', ring(n, d))  13.3 us
    all_gather x1, blocking collectives, layer(): gathered = lax.all_gather(turned, 'tp')  7.45 us
    ppermute x6, starting transfers between devices, layer(): lax.ppermute(out[s], 'tp', ring(n_tp, s))  7.18 us
    ppermute x6, starting transfers between devices, layer(): piece[d] = lax.ppermute(piece[d], 'kv', ring(n, d))  6.69 us
    pallas_call x1, Pallas kernels, early(): pl.pallas_call(functools.partial(early_kernel, steps, size, axes, count),...  5.4 us
    ppermute x3, starting transfers between devices, swap(): return lax.ppermute(array, 'kv', [(i, i ^ bit) for i in range(n)])  4.58 us
    ppermute x3, starting transfers between devices, layer(): other = lax.ppermute(halves[i], 'grp', ring(n_grp, 1))  3.24 us
    pallas_call x2, Pallas kernels, propose(): pl.pallas_call(functools.partial(propose_kernel, dims, axis, len(parts),...  3.24 us
  transfers between devices with their start and end apart: 19, of which 6 were waited for; matrix products, arithmetic and copies ran while one was open for 0% of the time, Pallas kernels for 18%

profile of v3, /device:TPU:9, one launch (start us, length us, event | category | flops | bytes accessed | tf_op | source)
XLA Modules:
  0.0 62.5 jit_solution(13662859360440483799)
XLA Ops:
  0.6 2.6 %collective-permute-start.2 = (bf16[32,4,512]{2,1,0:T(4,128)(2,1)}, bf16[32,4,512]{2,1,0:T(4,128)(2,1)S(1)}, u32[]{:S(2)}, u32[]{:S(2)}) collective-permute-start(bf16[32,4,512]{2,1,0:T(4,128)(2,1)} %param.17), channel_id=1, source_target_pairs={{0,0},{1,7},{2,10},{3,13},{4,1},{5,4},{6,11},{7,14},{8,2},{9,5},{1... | collective-permute-start | bytes 393224 | tf_op jit(solution)/shard_map/ppermute | solution.py:549
  3.2 5.4 %early.1 = (f32[32,64,256]{2,1,0:T(8,128)}, bf16[32,64,256]{2,1,0:T(8,128)(2,1)S(1)}, f32[8,256]{1,0:T(8,128)S(1)}, bf16[512,1024]{1,0:T(8,128)(2,1)S(1)}, f32[8...) custom-call(bf16[32,4,256]{2,1,0:T(4,128)(2,1)} %refs_0_.2, ...), custom_call_target="tpu_custom_call" | custom-call | flops 128000000 | bytes 4194304 | tf_op jit(solution)/shard_map/early/pallas_call | solution.py:336
  8.6 0.0 copy-start
  8.6 3.2 %collective-permute-start = (bf16[128,512]{1,0:T(8,128)(2,1)S(1)}, bf16[128,512]{1,0:T(8,128)(2,1)S(1)}, u32[]{:S(2)}, u32[]{:S(2)}) collective-permute-start(bf16[128,512]{1,0:T(8,128)(2,1)S(1)} %get-tuple-element.32), channel_id=1, source_target_pairs={{0,8},{4,12},{8,0},{12,4},{1,9},{5,13},{9,1},{13,5},{2,10},{6,14},... | collective-permute-start | bytes 393224 | tf_op jit(solution)/shard_map/ppermute | solution.py:559
  11.9 0.0 collective-permute-start.1
  11.9 0.0 collective-permute-done.2
  11.9 7.4 %all-gather = bf16[128,4,512]{2,1,0:T(4,128)(2,1)S(1)} all-gather(bf16[32,4,512]{2,1,0:T(4,128)(2,1)S(1)} %collective-permute-done.2), channel_id=2, replica_groups=mesh['grp'=2,'kv'=4,'tp'=4] {'tp'}, dimensions={0}, use_global_device_ids=true | all-gather | bytes 655360 | tf_op jit(solution)/shard_map/all_gather | solution.py:564
  19.3 1.5 %project.1 = (f32[104,1024]{1,0:T(8,128)S(1)}, bf16[104,1024]{1,0:T(8,128)(2,1)S(1)}, bf16[104,1024]{1,0:T(8,128)(2,1)S(1)}, bf16[104,1024]{1,0:T(8,128)(2,1)S(1...) custom-call(bf16[4,32,4,512]{3,2,1,0:T(4,128)(2,1)S(1)} %bitcast.9, ...), custom_call_target="tpu_custom_call" | custom-call | flops 536870912 | bytes 1048576 | tf_op jit(solution)/shard_map/project/pallas_call | solution.py:116
  20.8 0.0 collective-permute-done.refs_1_
  20.8 0.0 collective-permute-done.1.refs_3_
  20.8 1.3 %collective-permute-start.8 = (bf16[128,512]{1,0:T(8,128)(2,1)S(1)}, bf16[128,512]{1,0:T(8,128)(2,1)S(1)}, u32[]{:S(2)}, u32[]{:S(2)}) collective-permute-start(bf16[128,512]{1,0:T(8,128)(2,1)S(1)} %collective-permute-done.refs_1_), channel_id=1, source_target_pairs={{0,4},{4,0},{8,12},{12,8},{1,5},{5,1},{9,13},{13,9},{2,6},{6,2},{1... | collective-permute-start | bytes 393224 | tf_op jit(solution)/shard_map/ppermute | solution.py:559
  22.2 1.2 %collective-permute-start.6 = (bf16[128,512]{1,0:T(8,128)(2,1)S(1)}, bf16[128,512]{1,0:T(8,128)(2,1)S(1)}, u32[]{:S(2)}, u32[]{:S(2)}) collective-permute-start(bf16[128,512]{1,0:T(8,128)(2,1)S(1)} %collective-permute-done.refs_1_), channel_id=1, source_target_pairs={{0,16},{16,0},{1,17},{17,1},{2,18},{18,2},{3,19},{19,3},{4,20},{20... | collective-permute-start | bytes 393224 | tf_op jit(solution)/shard_map/ppermute | solution.py:577
  23.4 1.1 %collective-permute-start.3 = (bf16[104,1024]{1,0:T(8,128)(2,1)S(1)}, bf16[104,1024]{1,0:T(8,128)(2,1)S(1)}, u32[]{:S(2)}, u32[]{:S(2)}) collective-permute-start(bf16[104,1024]{1,0:T(8,128)(2,1)S(1)} %get-tuple-element.40), channel_id=1, source_target_pairs={{0,4},{4,8},{8,12},{12,0},{1,5},{5,9},{9,13},{13,1},{2,6},{6,10},{... | collective-permute-start | bytes 638984 | tf_op jit(solution)/shard_map/ppermute | solution.py:568
  24.5 1.2 %collective-permute-start.4 = (bf16[104,1024]{1,0:T(8,128)(2,1)S(1)}, bf16[104,1024]{1,0:T(8,128)(2,1)S(1)}, u32[]{:S(2)}, u32[]{:S(2)}) collective-permute-start(bf16[104,1024]{1,0:T(8,128)(2,1)S(1)} %get-tuple-element.41), channel_id=1, source_target_pairs={{0,8},{4,12},{8,0},{12,4},{1,9},{5,13},{9,1},{13,5},{2,10},{6,14},... | collective-permute-start | bytes 638984 | tf_op jit(solution)/shard_map/ppermute | solution.py:568
  25.7 0.3 collective-permute-start.5
  26.0 0.0 collective-permute-done.8.refs_5_
  26.1 1.0 %collective-permute-start.7 = (bf16[128,512]{1,0:T(8,128)(2,1)S(1)}, bf16[128,512]{1,0:T(8,128)(2,1)S(1)}, u32[]{:S(2)}, u32[]{:S(2)}) collective-permute-start(bf16[128,512]{1,0:T(8,128)(2,1)S(1)} %collective-permute-done.1.refs_3_), channel_id=1, source_target_pairs={{0,16},{16,0},{1,17},{17,1},{2,18},{18,2},{3,19},{19,3},{4,20},{20... | collective-permute-start | bytes 393224 | tf_op jit(solution)/shard_map/ppermute | solution.py:577
  27.0 0.0 collective-permute-done.6.refs_2_
  27.0 1.0 %collective-permute-start.9 = (bf16[128,512]{1,0:T(8,128)(2,1)S(1)}, bf16[128,512]{1,0:T(8,128)(2,1)S(1)}, u32[]{:S(2)}, u32[]{:S(2)}) collective-permute-start(bf16[128,512]{1,0:T(8,128)(2,1)S(1)} %collective-permute-done.8.refs_5_), channel_id=1, source_target_pairs={{0,16},{16,0},{1,17},{17,1},{2,18},{18,2},{3,19},{19,3},{4,20},{20... | collective-permute-start | bytes 393224 | tf_op jit(solution)/shard_map/ppermute | solution.py:577
  28.0 2.1 %collective-permute-done.7.refs_4_ = bf16[128,512]{1,0:T(8,128)(2,1)S(1)} collective-permute-done((bf16[128,512]{1,0:T(8,128)(2,1)S(1)}, bf16[128,512]{1,0:T(8,128)(2,1)S(1)}, u32[]{:S(2)}, u32[]{:S(2)}) %collective-permute-start.7) | collective-permute-done | bytes 131104 | tf_op jit(solution)/shard_map/ppermute | solution.py:577
  30.2 1.1 %collective-permute-start.13 = (bf16[40,1024]{1,0:T(8,128)(2,1)S(1)}, bf16[40,1024]{1,0:T(8,128)(2,1)S(1)}, u32[]{:S(2)}, u32[]{:S(2)}) collective-permute-start(bf16[40,1024]{1,0:T(8,128)(2,1)S(1)} %get-tuple-element.50), channel_id=1, source_target_pairs={{0,4},{4,8},{8,12},{12,0},{1,5},{5,9},{9,13},{13,1},{2,6},{6,10},{... | collective-permute-start | bytes 245768 | tf_op jit(solution)/shard_map/ppermute | solution.py:568
  31.3 0.0 collective-permute-done.3.refs_1_
  31.3 3.0 %collective-permute-start.14 = (bf16[40,1024]{1,0:T(8,128)(2,1)S(1)}, bf16[40,1024]{1,0:T(8,128)(2,1)S(1)}, u32[]{:S(2)}, u32[]{:S(2)}) collective-permute-start(bf16[40,1024]{1,0:T(8,128)(2,1)S(1)} %get-tuple-element.51), channel_id=1, source_target_pairs={{0,8},{4,12},{8,0},{12,4},{1,9},{5,13},{9,1},{13,5},{2,10},{6,14},... | collective-permute-start | bytes 245768 | tf_op jit(solution)/shard_map/ppermute | solution.py:568
  34.2 0.0 collective-permute-done.9.refs_6_
  34.2 0.0 collective-permute-start.15
  34.2 0.0 copy-done
  34.3 1.1 %assemble.1.refs_4_ = bf16[4,256,512]{2,1,0:T(8,128)(2,1)S(1)} custom-call(bf16[256,512]{1,0:T(8,128)(2,1)S(1)} %copy-done, bf16[128,512]{1,0:T(8,128)(2,1)S(1)} %collective-permute-done.refs_1_, bf16[128,512]{1,0:T(8,128)(2,1)S(1)} %collective-permute-done.6.refs_2_, bf16[128,512]{1,0:T(8,128)(2,1)S(1)} %collective-permute-done.1.refs_3_, ...), custom_call_target="tpu_custom_call" | custom-call | flops 4000000 | bytes 1048576 | tf_op jit(solution)/shard_map/assemble/pallas_call | solution.py:150
  35.4 8.5 %collective-permute-done.4.refs_2_ = bf16[104,1024]{1,0:T(8,128)(2,1)S(1)} collective-permute-done((bf16[104,1024]{1,0:T(8,128)(2,1)S(1)}, bf16[104,1024]{1,0:T(8,128)(2,1)S(1)}, u32[]{:S(2)}, u32[]{:S(2)}) %collective-permute-start.4) | collective-permute-done | bytes 213024 | tf_op jit(solution)/shard_map/ppermute | solution.py:568
  43.9 4.8 %collective-permute-done.5.refs_3_ = bf16[104,1024]{1,0:T(8,128)(2,1)S(1)} collective-permute-done((bf16[104,1024]{1,0:T(8,128)(2,1)S(1)}, bf16[104,1024]{1,0:T(8,128)(2,1)S(1)}, u32[]{:S(2)}, u32[]{:S(2)}) %collective-permute-start.5) | collective-permute-done | bytes 213024 | tf_op jit(solution)/shard_map/ppermute | solution.py:568
  48.6 2.0 %propose.2 = (f32[96,512]{1,0:T(8,128)S(1)}, bf16[96,512]{1,0:T(8,128)(2,1)S(1)}, bf16[96,512]{1,0:T(8,128)(2,1)S(1)}, bf16[96,512]{1,0:T(8,128)(2,1)S(1)}) custom-call(f32[8,256]{1,0:T(8,128)S(1)} %get-tuple-element.30.const_ref, bf16[32,64,256]{2,1,0:T(8,128)(2,1)S(1)} %get-tuple-element.31.s_ref, f32[104,1024]{1,0:T(8,128)S(1)} %get-tuple-element.39.refs_0_, ...), custom_call_target="tpu_custom_call" | custom-call | flops 96000000 | bytes 2097152 | tf_op jit(solution)/shard_map/propose/pallas_call | solution.py:460
  50.7 2.2 %collective-permute-start.10 = (bf16[96,512]{1,0:T(8,128)(2,1)S(1)}, bf16[96,512]{1,0:T(8,128)(2,1)S(1)}, u32[]{:S(2)}, u32[]{:S(2)}) collective-permute-start(bf16[96,512]{1,0:T(8,128)(2,1)S(1)} %get-tuple-element.46), channel_id=1, source_target_pairs={{0,1},{1,2},{2,3},{3,0},{4,5},{5,6},{6,7},{7,4},{8,9},{9,10},{10,1... | collective-permute-start | bytes 294920 | tf_op jit(solution)/shard_map/ppermute | solution.py:603
  52.8 0.3 collective-permute-start.11
  53.2 0.0 collective-permute-done.13.refs_1_
  53.2 0.1 collective-permute-start.12
  53.3 0.0 collective-permute-done.14.refs_2_
  53.3 0.0 collective-permute-done.15.refs_3_
  53.3 1.2 %propose.3 = (f32[32,512]{1,0:T(8,128)S(1)}, bf16[32,512]{1,0:T(8,128)(2,1)S(1)}, bf16[32,512]{1,0:T(8,128)(2,1)S(1)}, bf16[32,512]{1,0:T(8,128)(2,1)S(1)}) custom-call(f32[8,256]{1,0:T(8,128)S(1)} %get-tuple-element.30.const_ref, bf16[32,64,256]{2,1,0:T(8,128)(2,1)S(1)} %get-tuple-element.31.s_ref, f32[40,1024]{1,0:T(8,128)S(1)} %get-tuple-element.49.refs_0_, ...), custom_call_target="tpu_custom_call" | custom-call | flops 32000000 | bytes 2097152 | tf_op jit(solution)/shard_map/propose/pallas_call | solution.py:460
  54.5 1.6 %collective-permute-start.16 = (bf16[32,512]{1,0:T(8,128)(2,1)S(1)}, bf16[32,512]{1,0:T(8,128)(2,1)S(1)}, u32[]{:S(2)}, u32[]{:S(2)}) collective-permute-start(bf16[32,512]{1,0:T(8,128)(2,1)S(1)} %get-tuple-element.54), channel_id=1, source_target_pairs={{0,1},{1,2},{2,3},{3,0},{4,5},{5,6},{6,7},{7,4},{8,9},{9,10},{10,1... | collective-permute-start | bytes 98312 | tf_op jit(solution)/shard_map/ppermute | solution.py:603
  56.2 1.1 %collective-permute-start.17 = (bf16[32,512]{1,0:T(8,128)(2,1)S(1)}, bf16[32,512]{1,0:T(8,128)(2,1)S(1)}, u32[]{:S(2)}, u32[]{:S(2)}) collective-permute-start(bf16[32,512]{1,0:T(8,128)(2,1)S(1)} %get-tuple-element.55), channel_id=1, source_target_pairs={{0,2},{1,3},{2,0},{3,1},{4,6},{5,7},{6,4},{7,5},{8,10},{9,11},{10,... | collective-permute-start | bytes 98312 | tf_op jit(solution)/shard_map/ppermute | solution.py:603
  57.3 0.3 collective-permute-done.16.refs_5_
  57.6 1.8 %collective-permute-start.18 = (bf16[32,512]{1,0:T(8,128)(2,1)S(1)}, bf16[32,512]{1,0:T(8,128)(2,1)S(1)}, u32[]{:S(2)}, u32[]{:S(2)}) collective-permute-start(bf16[32,512]{1,0:T(8,128)(2,1)S(1)} %get-tuple-element.56), channel_id=1, source_target_pairs={{0,3},{1,0},{2,1},{3,2},{4,7},{5,4},{6,5},{7,6},{8,11},{9,8},{10,9... | collective-permute-start | bytes 98312 | tf_op jit(solution)/shard_map/ppermute | solution.py:603
  59.4 0.1 collective-permute-done.17.refs_6_
  59.5 2.2 %collective-permute-done.18.refs_7_ = bf16[32,512]{1,0:T(8,128)(2,1)S(1)} collective-permute-done((bf16[32,512]{1,0:T(8,128)(2,1)S(1)}, bf16[32,512]{1,0:T(8,128)(2,1)S(1)}, u32[]{:S(2)}, u32[]{:S(2)}) %collective-permute-start.18) | collective-permute-done | bytes 32800 | tf_op jit(solution)/shard_map/ppermute | solution.py:603
  61.7 0.0 collective-permute-done.10.refs_1_
  61.7 0.0 collective-permute-done.11.refs_2_
  61.7 0.0 collective-permute-done.12.refs_3_
  61.7 0.8 %finish.1 = bf16[32,4,512]{2,1,0:T(4,128)(2,1)} custom-call(f32[96,512]{1,0:T(8,128)S(1)} %get-tuple-element.45.refs_0_, bf16[96,512]{1,0:T(8,128)(2,1)S(1)} %collective-permute-done.10.refs_1_, bf16[96,512]{1,0:T(8,128)(2,1)S(1)} %collective-permute-done.11.refs_2_, bf16[96,512]{1,0:T(8,128)(2,1)S(1)} %collective-permute-done.12.refs_3_, ...), custom_call_target="tpu_custom_call" | custom-call | tf_op jit(solution)/shard_map/finish/pallas_call | solution.py:492
Async XLA Ops:
  0.6 11.3 %collective-permute-start.2 = (bf16[32,4,512]{2,1,0:T(4,128)(2,1)}, bf16[32,4,512]{2,1,0:T(4,128)(2,1)S(1)}, u32[]{:S(2)}, u32[]{:S(2)}) collective-permute-start(bf16[32,4,512]{2,1,0:T(4,128)(2,1)} %param.17), channel_id=1, source_target_pairs={{0,0},{1,7},{2,10},{3,13},{4,1},{5,4},{6,11},{7,14},{8,2},{9,5},{1... | collective-permute-start | bytes 393224 | tf_op jit(solution)/shard_map/ppermute | solution.py:549
  8.6 25.6 %copy-start = (bf16[256,512]{1,0:T(8,128)(2,1)S(1)}, bf16[256,512]{1,0:T(8,128)(2,1)}, u32[]{:S(2)}) copy-start(bf16[256,512]{1,0:T(8,128)(2,1)} %refs_0_.3) | copy-start | bytes 786436
  8.6 12.2 %collective-permute-start = (bf16[128,512]{1,0:T(8,128)(2,1)S(1)}, bf16[128,512]{1,0:T(8,128)(2,1)S(1)}, u32[]{:S(2)}, u32[]{:S(2)}) collective-permute-start(bf16[128,512]{1,0:T(8,128)(2,1)S(1)} %get-tuple-element.32), channel_id=1, source_target_pairs={{0,8},{4,12},{8,0},{12,4},{1,9},{5,13},{9,1},{13,5},{2,10},{6,14},... | collective-permute-start | bytes 393224 | tf_op jit(solution)/shard_map/ppermute | solution.py:559
  11.9 9.0 %collective-permute-start.1 = (bf16[128,512]{1,0:T(8,128)(2,1)S(1)}, bf16[128,512]{1,0:T(8,128)(2,1)S(1)}, u32[]{:S(2)}, u32[]{:S(2)}) collective-permute-start(bf16[128,512]{1,0:T(8,128)(2,1)S(1)} %get-tuple-element.32), channel_id=1, source_target_pairs={{0,4},{4,0},{8,12},{12,8},{1,5},{5,1},{9,13},{13,9},{2,6},{6,2},{1... | collective-permute-start | bytes 393224 | tf_op jit(solution)/shard_map/ppermute | solution.py:559
  20.8 5.2 %collective-permute-start.8 = (bf16[128,512]{1,0:T(8,128)(2,1)S(1)}, bf16[128,512]{1,0:T(8,128)(2,1)S(1)}, u32[]{:S(2)}, u32[]{:S(2)}) collective-permute-start(bf16[128,512]{1,0:T(8,128)(2,1)S(1)} %collective-permute-done.refs_1_), channel_id=1, source_target_pairs={{0,4},{4,0},{8,12},{12,8},{1,5},{5,1},{9,13},{13,9},{2,6},{6,2},{1... | collective-permute-start | bytes 393224 | tf_op jit(solution)/shard_map/ppermute | solution.py:559
  22.2 4.9 %collective-permute-start.6 = (bf16[128,512]{1,0:T(8,128)(2,1)S(1)}, bf16[128,512]{1,0:T(8,128)(2,1)S(1)}, u32[]{:S(2)}, u32[]{:S(2)}) collective-permute-start(bf16[128,512]{1,0:T(8,128)(2,1)S(1)} %collective-permute-done.refs_1_), channel_id=1, source_target_pairs={{0,16},{16,0},{1,17},{17,1},{2,18},{18,2},{3,19},{19,3},{4,20},{20... | collective-permute-start | bytes 393224 | tf_op jit(solution)/shard_map/ppermute | solution.py:577
  23.4 7.9 %collective-permute-start.3 = (bf16[104,1024]{1,0:T(8,128)(2,1)S(1)}, bf16[104,1024]{1,0:T(8,128)(2,1)S(1)}, u32[]{:S(2)}, u32[]{:S(2)}) collective-permute-start(bf16[104,1024]{1,0:T(8,128)(2,1)S(1)} %get-tuple-element.40), channel_id=1, source_target_pairs={{0,4},{4,8},{8,12},{12,0},{1,5},{5,9},{9,13},{13,1},{2,6},{6,10},{... | collective-permute-start | bytes 638984 | tf_op jit(solution)/shard_map/ppermute | solution.py:568
  24.5 19.4 %collective-permute-start.4 = (bf16[104,1024]{1,0:T(8,128)(2,1)S(1)}, bf16[104,1024]{1,0:T(8,128)(2,1)S(1)}, u32[]{:S(2)}, u32[]{:S(2)}) collective-permute-start(bf16[104,1024]{1,0:T(8,128)(2,1)S(1)} %get-tuple-element.41), channel_id=1, source_target_pairs={{0,8},{4,12},{8,0},{12,4},{1,9},{5,13},{9,1},{13,5},{2,10},{6,14},... | collective-permute-start | bytes 638984 | tf_op jit(solution)/shard_map/ppermute | solution.py:568
  25.7 22.9 %collective-permute-start.5 = (bf16[104,1024]{1,0:T(8,128)(2,1)S(1)}, bf16[104,1024]{1,0:T(8,128)(2,1)S(1)}, u32[]{:S(2)}, u32[]{:S(2)}) collective-permute-start(bf16[104,1024]{1,0:T(8,128)(2,1)S(1)} %get-tuple-element.42), channel_id=1, source_target_pairs={{0,12},{4,0},{8,4},{12,8},{1,13},{5,1},{9,5},{13,9},{2,14},{6,2},{... | collective-permute-start | bytes 638984 | tf_op jit(solution)/shard_map/ppermute | solution.py:568
  26.1 4.1 %collective-permute-start.7 = (bf16[128,512]{1,0:T(8,128)(2,1)S(1)}, bf16[128,512]{1,0:T(8,128)(2,1)S(1)}, u32[]{:S(2)}, u32[]{:S(2)}) collective-permute-start(bf16[128,512]{1,0:T(8,128)(2,1)S(1)} %collective-permute-done.1.refs_3_), channel_id=1, source_target_pairs={{0,16},{16,0},{1,17},{17,1},{2,18},{18,2},{3,19},{19,3},{4,20},{20... | collective-permute-start | bytes 393224 | tf_op jit(solution)/shard_map/ppermute | solution.py:577
  27.0 7.2 %collective-permute-start.9 = (bf16[128,512]{1,0:T(8,128)(2,1)S(1)}, bf16[128,512]{1,0:T(8,128)(2,1)S(1)}, u32[]{:S(2)}, u32[]{:S(2)}) collective-permute-start(bf16[128,512]{1,0:T(8,128)(2,1)S(1)} %collective-permute-done.8.refs_5_), channel_id=1, source_target_pairs={{0,16},{16,0},{1,17},{17,1},{2,18},{18,2},{3,19},{19,3},{4,20},{20... | collective-permute-start | bytes 393224 | tf_op jit(solution)/shard_map/ppermute | solution.py:577
  30.2 23.0 %collective-permute-start.13 = (bf16[40,1024]{1,0:T(8,128)(2,1)S(1)}, bf16[40,1024]{1,0:T(8,128)(2,1)S(1)}, u32[]{:S(2)}, u32[]{:S(2)}) collective-permute-start(bf16[40,1024]{1,0:T(8,128)(2,1)S(1)} %get-tuple-element.50), channel_id=1, source_target_pairs={{0,4},{4,8},{8,12},{12,0},{1,5},{5,9},{9,13},{13,1},{2,6},{6,10},{... | collective-permute-start | bytes 245768 | tf_op jit(solution)/shard_map/ppermute | solution.py:568
  31.3 22.0 %collective-permute-start.14 = (bf16[40,1024]{1,0:T(8,128)(2,1)S(1)}, bf16[40,1024]{1,0:T(8,128)(2,1)S(1)}, u32[]{:S(2)}, u32[]{:S(2)}) collective-permute-start(bf16[40,1024]{1,0:T(8,128)(2,1)S(1)} %get-tuple-element.51), channel_id=1, source_target_pairs={{0,8},{4,12},{8,0},{12,4},{1,9},{5,13},{9,1},{13,5},{2,10},{6,14},... | collective-permute-start | bytes 245768 | tf_op jit(solution)/shard_map/ppermute | solution.py:568
  34.2 19.1 %collective-permute-start.15 = (bf16[40,1024]{1,0:T(8,128)(2,1)S(1)}, bf16[40,1024]{1,0:T(8,128)(2,1)S(1)}, u32[]{:S(2)}, u32[]{:S(2)}) collective-permute-start(bf16[40,1024]{1,0:T(8,128)(2,1)S(1)} %get-tuple-element.52), channel_id=1, source_target_pairs={{0,12},{4,0},{8,4},{12,8},{1,13},{5,1},{9,5},{13,9},{2,14},{6,2},{... | collective-permute-start | bytes 245768 | tf_op jit(solution)/shard_map/ppermute | solution.py:568
  50.7 11.0 %collective-permute-start.10 = (bf16[96,512]{1,0:T(8,128)(2,1)S(1)}, bf16[96,512]{1,0:T(8,128)(2,1)S(1)}, u32[]{:S(2)}, u32[]{:S(2)}) collective-permute-start(bf16[96,512]{1,0:T(8,128)(2,1)S(1)} %get-tuple-element.46), channel_id=1, source_target_pairs={{0,1},{1,2},{2,3},{3,0},{4,5},{5,6},{6,7},{7,4},{8,9},{9,10},{10,1... | collective-permute-start | bytes 294920 | tf_op jit(solution)/shard_map/ppermute | solution.py:603
  52.8 8.8 %collective-permute-start.11 = (bf16[96,512]{1,0:T(8,128)(2,1)S(1)}, bf16[96,512]{1,0:T(8,128)(2,1)S(1)}, u32[]{:S(2)}, u32[]{:S(2)}) collective-permute-start(bf16[96,512]{1,0:T(8,128)(2,1)S(1)} %get-tuple-element.47), channel_id=1, source_target_pairs={{0,2},{1,3},{2,0},{3,1},{4,6},{5,7},{6,4},{7,5},{8,10},{9,11},{10,... | collective-permute-start | bytes 294920 | tf_op jit(solution)/shard_map/ppermute | solution.py:603
  53.2 8.5 %collective-permute-start.12 = (bf16[96,512]{1,0:T(8,128)(2,1)S(1)}, bf16[96,512]{1,0:T(8,128)(2,1)S(1)}, u32[]{:S(2)}, u32[]{:S(2)}) collective-permute-start(bf16[96,512]{1,0:T(8,128)(2,1)S(1)} %get-tuple-element.48), channel_id=1, source_target_pairs={{0,3},{1,0},{2,1},{3,2},{4,7},{5,4},{6,5},{7,6},{8,11},{9,8},{10,9... | collective-permute-start | bytes 294920 | tf_op jit(solution)/shard_map/ppermute | solution.py:603
  54.5 3.1 %collective-permute-start.16 = (bf16[32,512]{1,0:T(8,128)(2,1)S(1)}, bf16[32,512]{1,0:T(8,128)(2,1)S(1)}, u32[]{:S(2)}, u32[]{:S(2)}) collective-permute-start(bf16[32,512]{1,0:T(8,128)(2,1)S(1)} %get-tuple-element.54), channel_id=1, source_target_pairs={{0,1},{1,2},{2,3},{3,0},{4,5},{5,6},{6,7},{7,4},{8,9},{9,10},{10,1... | collective-permute-start | bytes 98312 | tf_op jit(solution)/shard_map/ppermute | solution.py:603
  56.2 3.3 %collective-permute-start.17 = (bf16[32,512]{1,0:T(8,128)(2,1)S(1)}, bf16[32,512]{1,0:T(8,128)(2,1)S(1)}, u32[]{:S(2)}, u32[]{:S(2)}) collective-permute-start(bf16[32,512]{1,0:T(8,128)(2,1)S(1)} %get-tuple-element.55), channel_id=1, source_target_pairs={{0,2},{1,3},{2,0},{3,1},{4,6},{5,7},{6,4},{7,5},{8,10},{9,11},{10,... | collective-permute-start | bytes 98312 | tf_op jit(solution)/shard_map/ppermute | solution.py:603
  57.6 4.1 %collective-permute-start.18 = (bf16[32,512]{1,0:T(8,128)(2,1)S(1)}, bf16[32,512]{1,0:T(8,128)(2,1)S(1)}, u32[]{:S(2)}, u32[]{:S(2)}) collective-permute-start(bf16[32,512]{1,0:T(8,128)(2,1)S(1)} %get-tuple-element.56), channel_id=1, source_target_pairs={{0,3},{1,0},{2,1},{3,2},{4,7},{5,4},{6,5},{7,6},{8,11},{9,8},{10,9... | collective-permute-start | bytes 98312 | tf_op jit(solution)/shard_map/ppermute | solution.py:603

commit v4 on v3

--- a/solution.py
+++ b/solution.py
@@ -69,15 +69,15 @@
     return high, values - high
 
 
-def project_kernel(chunks, x_ref, gain_ref, weight_ref, small_ref, *outs):
+def project_kernel(chunks, layout, x_ref, gain_ref, weight_ref, small_ref, *outs):
     owners, _, steps, local = x_ref.shape
     gain = gain_ref[0:1, :]
-    raw, spans, start = [], [], 0
-    tokens = [[x_ref[d, :, t, :].astype(F32) for t in range(steps)] for d in range(owners)]
-    for first, each in chunks:
-        for d in range(owners):
-            raw += [x[first : first + each] for x in tokens[d]]
-            spans.append(slice(start, start + each * steps))
+    raw, spans, start = [], {}, 0
+    for d in range(owners):
+        tokens = [x_ref[d, :, t, :].astype(F32) for t in range(steps)]
+        for c, (first, each) in enumerate(chunks):
+            raw += [x[first : first + each] for x in tokens]
+            spans[d, c] = slice(start, start + each * steps)
             start += each * steps
     raw = jnp.concatenate(raw, 0)
     x = (raw * gain).astype(BF16)
@@ -88,47 +88,51 @@
     unit = (lax.broadcasted_iota(jnp.int32, (128, local), 0) == count).astype(F32).astype(BF16)
     small = jnp.concatenate([small_ref[...], jnp.zeros((128 - count, local), BF16)], 0)
     sums = dot(x, small, ((1,), (1,))) + dot(high, unit, ((1,), (1,))) + dot(low, unit, ((1,), (1,)))
-    for out, span in zip(outs, spans):
-        rows = span.stop - span.start
-        part = sums[span]
-        if rows < 128:
-            part = jnp.concatenate([part, jnp.zeros((128 - rows, 128), F32)], 0)
-        part = part.T
+    width = weight_ref.shape[1]
+    for out, (d, parts, with_sums) in zip(outs, layout):
+        if not with_sums:
+            continue
         extra = []
-        for first in range(0, 2 * count, count):
-            extra += stat_rows(part[first : first + count])
-        extra.append(jnp.zeros((count, out.shape[1] - 128 * len(extra)), F32))
-        out[rows : rows + count, :] = jnp.concatenate(extra, 1).astype(out.dtype)
-    width = weight_ref.shape[1]
+        for c in range(len(chunks)):
+            part = sums[spans[d, c]]
+            if part.shape[0] < 128:
+                part = jnp.concatenate([part, jnp.zeros((128 - part.shape[0], 128), F32)], 0)
+            part = part.T
+            for first in range(0, 2 * count, count):
+                extra += stat_rows(part[first : first + count])
+        if width > 128 * len(extra):
+            extra.append(jnp.zeros((count, width - 128 * len(extra)), F32))
+        out[out.shape[0] - count :, :] = jnp.concatenate(extra, 1).astype(out.dtype)
     block = min(width, 256)
     for first in range(0, width, block):
         lanes = slice(first, first + block)
         product = dot(x, weight_ref[:, lanes])
-        for out, span in zip(outs, spans):
-            rows = span.stop - span.start
-            out[:rows, lanes] = product[span].astype(out.dtype)
-
-
-def project(x, gain, weight, small, chunks):
-    owners, _, steps, _ = x.shape
+        for out, (d, parts, _) in zip(outs, layout):
+            start = 0
+            for c in parts:
+                piece = product[spans[d, c]]
+                out[start : start + piece.shape[0], lanes] = piece.astype(out.dtype)
+                start += piece.shape[0]
+
+
+def project(x, gain, weight, small, chunks, layout):
+    _, _, steps, _ = x.shape
     width = weight.shape[1]
-    extra = small.shape[0]
-    outs = pl.pallas_call(
-        functools.partial(project_kernel, chunks),
-        out_shape=[
-            jax.ShapeDtypeStruct((each * steps + extra, width), F32 if d == 0 else BF16)
-            for _, each in chunks
-            for d in range(owners)
-        ],
+
+    def shape(d, parts, with_sums, dtype):
+        rows = sum(chunks[c][1] for c in parts) * steps
+        return jax.ShapeDtypeStruct((rows + small.shape[0] * with_sums, width), dtype)
+
+    return pl.pallas_call(
+        functools.partial(project_kernel, chunks, [entry[:3] for entry in layout]),
+        out_shape=[shape(*entry) for entry in layout],
         in_specs=[whole()] * 4,
-        out_specs=[whole()] * (owners * len(chunks)),
+        out_specs=[whole()] * len(layout),
         compiler_params=limit(16),
         cost_estimate=pl.CostEstimate(
             flops=2 * x.size * width, bytes_accessed=4 * x.size, transcendentals=0
         ),
-        name="project",
     )(x, gain, weight, small)
-    return [list(outs[c * owners : (c + 1) * owners]) for c in range(len(chunks))]
 
 
 def assemble_kernel(axes, blocks, *refs):
@@ -354,26 +358,38 @@
     )(*[pltpu.with_memory_space_constraint(a, HBM) for a in arrays])
 
 
-def propose_kernel(dims, axis, parts, first, const_ref, s_ref, *refs):
+def propose_kernel(dims, axis, spans, first, seqs, slot, const_ref, s_ref, *refs):
     steps, size, features = dims
+    parts = len(spans)
     part_refs, wo, refs = refs[:parts], refs[parts], refs[parts + 1 :]
-    out_refs, (kscr, pscr) = refs[:-2], refs[-2:]
+    stat_in = None if any(sums is not None for _, sums in spans) else refs[0]
+    out_refs, (kscr, pscr) = refs[0 if stat_in is None else 1 : -2], refs[-2:]
     width = s_ref.shape[2]
     extra = -(-2 * (width // size) // 8) * 8
-    seqs = (part_refs[0].shape[0] - extra) // steps
     heads = width // size
     group = 8 // steps
     ones = head_ones(width, size)
     masks = [head_mask(g * group, group, steps, width, size) for g in range(heads // group)]
     rows = seqs * steps
 
-    def gathered(rows_of, lanes):
-        total = part_refs[0][rows_of, lanes].astype(F32)
-        for ref in part_refs[1:]:
-            total = total + ref[rows_of, lanes].astype(F32)
+    def gathered(starts, count, lanes):
+        total = None
+        for ref, start in zip(part_refs, starts):
+            if start is not None:
+                piece = ref[start : start + count, lanes].astype(F32)
+                total = piece if total is None else total + piece
         return total
 
-    stat = gathered(slice(rows, rows + extra), slice(0, 512))
+    starts = [start for start, _ in spans]
+    if stat_in is None:
+        stat = gathered([sums for _, sums in spans], extra, slice(None))
+        if slot is not None:
+            out_refs[-1][...] = stat
+            out_refs = out_refs[:-1]
+    else:
+        stat = stat_in[...]
+    at_slot = 512 * (slot or 0)
+    stat = stat[:, at_slot : at_slot + 512]
     logits = stat[:, :128] + stat[:, 128:256]
     total = stat[:, 256:384] + stat[:, 384:]
     flat = jnp.concatenate([logits, total], 0).T[:rows]
@@ -391,7 +407,7 @@
     log = -base * (jnp.maximum(rate, 0.0) + jnp.log1p(jnp.exp(-jnp.abs(rate))))
 
     def column(w):
-        return gathered(slice(0, rows), slice(w * width, (w + 1) * width)) * scale
+        return gathered(starts, rows, slice(w * width, (w + 1) * width)) * scale
 
     query, key = column(0), column(1)
     squares = head_sum(jnp.concatenate([query * query, key * key], 0), ones)
@@ -444,11 +460,11 @@
     n = wo.shape[0]
     tp = lax.axis_index(axis)
     for s in list(range(1, len(out_refs))) + [0]:
-        block = wo[lax.rem(tp + s, n)] if n > 1 else wo[0]
+        block = wo[lax.bitwise_xor(tp, s)] if n > 1 else wo[0]
         out_refs[s][...] = dot(gated, block).astype(out_refs[s].dtype)
 
 
-def propose(axis, consts, state, parts, wo, dims, first, seqs):
+def propose(axis, consts, state, parts, spans, wo, dims, first, seqs, slot, stat):
     steps, size = dims[0], dims[1]
     width = state.shape[2]
     heads = width // size
@@ -457,10 +473,16 @@
         jax.ShapeDtypeStruct((rows, wo.shape[2]), F32 if s == 0 and wo.shape[0] > 1 else BF16)
         for s in range(wo.shape[0])
     ]
+    inputs = [consts, state, *parts, wo]
+    if stat is not None:
+        inputs.append(stat)
+    elif slot is not None:
+        extra = -(-2 * heads // 8) * 8
+        shapes.append(jax.ShapeDtypeStruct((extra, parts[0].shape[1]), F32))
     return pl.pallas_call(
-        functools.partial(propose_kernel, dims, axis, len(parts), first),
+        functools.partial(propose_kernel, dims, axis, spans, first, seqs, slot),
         out_shape=shapes,
-        in_specs=[whole()] * (3 + len(parts)),
+        in_specs=[whole()] * len(inputs),
         out_specs=[whole()] * len(shapes),
         scratch_shapes=[
             VMEM((seqs * 2 * heads * steps, 128), F32),
@@ -471,7 +493,7 @@
             flops=seqs * 4000000, bytes_accessed=4 * state.size, transcendentals=0
         ),
         name="propose",
-    )(consts, state, *parts, wo)
+    )(*inputs)
 
 
 def finish_kernel(steps, chunks, *refs):
@@ -545,7 +567,8 @@
 
     if square:
         n = n_kv
-        turn = [(k * n + t, t * n + (k - t) % n) for k in range(n) for t in range(n)]
+        bits = [n >> i for i in range(1, n.bit_length())]
+        turn = [(k * n + t, t * n + (k ^ t)) for k in range(n) for t in range(n)]
         turned = lax.ppermute(tokens, ("kv", "tp"), turn)
     shared = (in_gain, w_beta, w_decay, weights, w_out) if square else None
     new_state, low, consts, *staged = early(axes, state, prev, decay_base, out_gain, shared)
@@ -553,19 +576,25 @@
         weight, own_gain, small, mine = staged
         turned, weight = lax.optimization_barrier((turned, weight))
         halves, marks = [mine], [0]
-        bits = [n >> i for i in range(1, n.bit_length())]
 
         def swap(array, bit):
             return lax.ppermute(array, "kv", [(i, i ^ bit) for i in range(n)])
 
-        for bit in bits:
-            halves.append(swap(mine, bit))
-            marks.append(bit)
+        halves.append(swap(mine, bits[0]))
+        marks.append(bits[0])
+        halves.append(swap(mine, bits[1]))
+        marks.append(bits[1])
         gathered = lax.all_gather(turned, "tp")
-        parts = project(gathered, own_gain, weight, small, chunks)
-        for piece in parts:
-            for d in range(1, n):
-                piece[d] = lax.ppermute(piece[d], "kv", ring(n, d))
+        layout = [
+            (i, (c,), c == 0, F32 if i == 0 else BF16) for c in range(len(chunks)) for i in range(n)
+        ]
+        products = project(gathered, own_gain, weight, small, chunks, layout)
+        parts = [list(products[c * n : (c + 1) * n]) for c in range(len(chunks))]
+        spans = []
+        for c, (first, each) in enumerate(chunks):
+            for i in range(1, n):
+                parts[c][i] = swap(parts[c][i], i)
+            spans.append([(0, each * steps if c == 0 else None)] * n)
         halves, parts[0][0] = lax.optimization_barrier((halves, parts[0][0]))
         for bit in bits[1:]:
             for j in range(len(halves)):
@@ -593,14 +622,24 @@
         sums = sums.at[: 2 * heads, : seqs * steps].set(logits)
         sums = sums.at[0, 256 : 256 + seqs * steps].set(square_sum)
         parts = [[jnp.concatenate([jnp.concatenate(products, 1), sums], 0)]]
+        spans = [[(0, seqs * steps)]]
         wo = lax.all_gather(w_out, "kv", axis=1, tiled=True)[None]
 
-    pieces = []
-    for (first, each), part in zip(chunks, parts):
-        out = propose("tp", consts, low, part, wo, dims, first, each)
+    pieces, stat = [], None
+    for c, (first, each) in enumerate(chunks):
+        slot = c if len(chunks) > 1 else None
+        out = propose(
+            "tp", consts, low, parts[c], spans[c], wo, dims, first, each, slot, stat
+        )
+        if slot == 0:
+            stat = out[-1]
         if square:
             pieces.append(
-                [out[0]] + [lax.ppermute(out[s], "tp", ring(n_tp, s)) for s in range(1, n_tp)]
+                [out[0]]
+                + [
+                    lax.ppermute(out[s], "tp", [(i, i ^ s) for i in range(n_tp)])
+                    for s in range(1, n_tp)
+                ]
             )
         else:
             pieces.append([lax.psum_scatter(out[0], "tp", scatter_dimension=1, tiled=True)])

time: 62.7 us -> 61.3 us (0.978)
  waiting for transfers between devices: 18 us -> 16.8 us
    ppermute x12 -> x6, waiting for transfers between devices: 15.9 us -> 3.42 us  [layer(): lax.ppermute(out[s], 'tp', [(i, i ^ s) for i in range(n_tp)])]
    ppermute x3 -> x9, waiting for transfers between devices: 0.01 us -> 11.2 us  [swap(): return lax.ppermute(array, 'kv', [(i, i ^ bit) for i in range(n)])]
    ppermute x12 -> x6, starting transfers between devices: 13.9 us -> 6.69 us  [layer(): lax.ppermute(out[s], 'tp', [(i, i ^ s) for i in range(n_tp)])]
    ppermute x3 -> x9, starting transfers between devices: 4.58 us -> 11.7 us  [swap(): return lax.ppermute(array, 'kv', [(i, i ^ bit) for i in range(n)])]
where the time goes in v4:
time: 61.3 us; the launch traced here: 61.2 us
  starting transfers between devices  24.2 us (39%)
  waiting for transfers between devices  16.8 us (27%)
  Pallas kernels  12 us (20%)
  blocking collectives  7.45 us (12%)
  between operations  0.72 us (1%)
    ppermute x9, starting transfers between devices, swap(): return lax.ppermute(array, 'kv', [(i, i ^ bit) for i in range(n)])  11.7 us
    ppermute x9, waiting for transfers between devices, swap(): return lax.ppermute(array, 'kv', [(i, i ^ bit) for i in range(n)])  11.2 us
    all_gather x1, blocking collectives, layer(): gathered = lax.all_gather(turned, 'tp')  7.45 us
    ppermute x6, starting transfers between devices, layer(): lax.ppermute(out[s], 'tp', [(i, i ^ s) for i in range(n_tp)])  6.69 us
    pallas_call x1, Pallas kernels, early(): pl.pallas_call(functools.partial(early_kernel, steps, size, axes, count),...  5.4 us
    ppermute x6, waiting for transfers between devices, layer(): lax.ppermute(out[s], 'tp', [(i, i ^ s) for i in range(n_tp)])  3.42 us
    pallas_call x2, Pallas kernels, propose(): pl.pallas_call(functools.partial(propose_kernel, dims, axis, spans, first...  3.24 us
    ppermute x3, starting transfers between devices, layer(): other = lax.ppermute(halves[i], 'grp', ring(n_grp, 1))  3.2 us
  transfers between devices with their start and end apart: 19, of which 6 were waited for; matrix products, arithmetic and copies ran while one was open for 0% of the time, Pallas kernels for 18%

profile of v4, /device:TPU:9, one launch (start us, length us, event | category | flops | bytes accessed | tf_op | source)
XLA Modules:
  0.0 61.2 jit_solution(10546681172006213410)
XLA Ops:
  0.6 2.6 %collective-permute-start.2 = (bf16[32,4,512]{2,1,0:T(4,128)(2,1)}, bf16[32,4,512]{2,1,0:T(4,128)(2,1)S(1)}, u32[]{:S(2)}, u32[]{:S(2)}) collective-permute-start(bf16[32,4,512]{2,1,0:T(4,128)(2,1)} %param.17), channel_id=1, source_target_pairs={{0,0},{1,5},{2,10},{3,15},{4,1},{5,4},{6,11},{7,14},{8,2},{9,7},{1... | collective-permute-start | bytes 393224 | tf_op jit(solution)/shard_map/ppermute | solution.py:572
  3.2 5.4 %early.1 = (f32[32,64,256]{2,1,0:T(8,128)}, bf16[32,64,256]{2,1,0:T(8,128)(2,1)S(1)}, f32[8,256]{1,0:T(8,128)S(1)}, bf16[512,1024]{1,0:T(8,128)(2,1)S(1)}, f32[8...) custom-call(bf16[32,4,256]{2,1,0:T(4,128)(2,1)} %refs_0_.2, ...), custom_call_target="tpu_custom_call" | custom-call | flops 128000000 | bytes 4194304 | tf_op jit(solution)/shard_map/early/pallas_call | solution.py:340
  8.6 0.0 copy-start
  8.6 3.2 %collective-permute-start = (bf16[128,512]{1,0:T(8,128)(2,1)S(1)}, bf16[128,512]{1,0:T(8,128)(2,1)S(1)}, u32[]{:S(2)}, u32[]{:S(2)}) collective-permute-start(bf16[128,512]{1,0:T(8,128)(2,1)S(1)} %get-tuple-element.33), channel_id=1, source_target_pairs={{0,8},{4,12},{8,0},{12,4},{1,9},{5,13},{9,1},{13,5},{2,10},{6,14},... | collective-permute-start | bytes 393224 | tf_op jit(solution)/shard_map/ppermute | solution.py:581
  11.9 0.0 collective-permute-start.1
  11.9 0.0 collective-permute-done.2
  11.9 7.4 %all-gather = bf16[128,4,512]{2,1,0:T(4,128)(2,1)S(1)} all-gather(bf16[32,4,512]{2,1,0:T(4,128)(2,1)S(1)} %collective-permute-done.2), channel_id=2, replica_groups=mesh['grp'=2,'kv'=4,'tp'=4] {'tp'}, dimensions={0}, use_global_device_ids=true | all-gather | bytes 655360 | tf_op jit(solution)/shard_map/all_gather | solution.py:587
  19.3 1.5 %shard_map.176 = (f32[104,1024]{1,0:T(8,128)S(1)}, bf16[104,1024]{1,0:T(8,128)(2,1)S(1)}, bf16[104,1024]{1,0:T(8,128)(2,1)S(1)}, bf16[104,1024]{1,0:T(8,128)(2,1...) custom-call(bf16[4,32,4,512]{3,2,1,0:T(4,128)(2,1)S(1)} %bitcast.9, ...), custom_call_target="tpu_custom_call" | custom-call | flops 536870912 | bytes 1048576 | tf_op jit(solution)/shard_map/pallas_call | solution.py:126
  20.8 0.0 collective-permute-done.refs_1_
  20.8 0.0 collective-permute-done.1.refs_3_
  20.8 1.3 %collective-permute-start.8 = (bf16[128,512]{1,0:T(8,128)(2,1)S(1)}, bf16[128,512]{1,0:T(8,128)(2,1)S(1)}, u32[]{:S(2)}, u32[]{:S(2)}) collective-permute-start(bf16[128,512]{1,0:T(8,128)(2,1)S(1)} %collective-permute-done.refs_1_), channel_id=1, source_target_pairs={{0,4},{4,0},{8,12},{12,8},{1,5},{5,1},{9,13},{13,9},{2,6},{6,2},{1... | collective-permute-start | bytes 393224 | tf_op jit(solution)/shard_map/ppermute | solution.py:581
  22.2 1.2 %collective-permute-start.6 = (bf16[128,512]{1,0:T(8,128)(2,1)S(1)}, bf16[128,512]{1,0:T(8,128)(2,1)S(1)}, u32[]{:S(2)}, u32[]{:S(2)}) collective-permute-start(bf16[128,512]{1,0:T(8,128)(2,1)S(1)} %collective-permute-done.refs_1_), channel_id=1, source_target_pairs={{0,16},{16,0},{1,17},{17,1},{2,18},{18,2},{3,19},{19,3},{4,20},{20... | collective-permute-start | bytes 393224 | tf_op jit(solution)/shard_map/ppermute | solution.py:606
  23.4 0.2 collective-permute-start.3
  23.6 2.1 %collective-permute-start.4 = (bf16[104,1024]{1,0:T(8,128)(2,1)S(1)}, bf16[104,1024]{1,0:T(8,128)(2,1)S(1)}, u32[]{:S(2)}, u32[]{:S(2)}) collective-permute-start(bf16[104,1024]{1,0:T(8,128)(2,1)S(1)} %get-tuple-element.42), channel_id=1, source_target_pairs={{0,8},{4,12},{8,0},{12,4},{1,9},{5,13},{9,1},{13,5},{2,10},{6,14},... | collective-permute-start | bytes 638984 | tf_op jit(solution)/shard_map/ppermute | solution.py:581
  25.7 0.4 collective-permute-start.5
  26.1 0.0 collective-permute-done.8.refs_5_
  26.1 1.0 %collective-permute-start.7 = (bf16[128,512]{1,0:T(8,128)(2,1)S(1)}, bf16[128,512]{1,0:T(8,128)(2,1)S(1)}, u32[]{:S(2)}, u32[]{:S(2)}) collective-permute-start(bf16[128,512]{1,0:T(8,128)(2,1)S(1)} %collective-permute-done.1.refs_3_), channel_id=1, source_target_pairs={{0,16},{16,0},{1,17},{17,1},{2,18},{18,2},{3,19},{19,3},{4,20},{20... | collective-permute-start | bytes 393224 | tf_op jit(solution)/shard_map/ppermute | solution.py:606
  27.0 0.0 collective-permute-done.6.refs_2_
  27.0 1.0 %collective-permute-start.9 = (bf16[128,512]{1,0:T(8,128)(2,1)S(1)}, bf16[128,512]{1,0:T(8,128)(2,1)S(1)}, u32[]{:S(2)}, u32[]{:S(2)}) collective-permute-start(bf16[128,512]{1,0:T(8,128)(2,1)S(1)} %collective-permute-done.8.refs_5_), channel_id=1, source_target_pairs={{0,16},{16,0},{1,17},{17,1},{2,18},{18,2},{3,19},{19,3},{4,20},{20... | collective-permute-start | bytes 393224 | tf_op jit(solution)/shard_map/ppermute | solution.py:606
  28.0 2.2 %collective-permute-done.7.refs_4_ = bf16[128,512]{1,0:T(8,128)(2,1)S(1)} collective-permute-done((bf16[128,512]{1,0:T(8,128)(2,1)S(1)}, bf16[128,512]{1,0:T(8,128)(2,1)S(1)}, u32[]{:S(2)}, u32[]{:S(2)}) %collective-permute-start.7) | collective-permute-done | bytes 131104 | tf_op jit(solution)/shard_map/ppermute | solution.py:606
  30.2 1.1 %collective-permute-start.13 = (bf16[32,1024]{1,0:T(8,128)(2,1)S(1)}, bf16[32,1024]{1,0:T(8,128)(2,1)S(1)}, u32[]{:S(2)}, u32[]{:S(2)}) collective-permute-start(bf16[32,1024]{1,0:T(8,128)(2,1)S(1)} %get-tuple-element.51), channel_id=1, source_target_pairs={{0,4},{4,0},{8,12},{12,8},{1,5},{5,1},{9,13},{13,9},{2,6},{6,2},{1... | collective-permute-start | bytes 196616 | tf_op jit(solution)/shard_map/ppermute | solution.py:581
  31.3 2.1 %collective-permute-done.3.refs_1_ = bf16[104,1024]{1,0:T(8,128)(2,1)S(1)} collective-permute-done((bf16[104,1024]{1,0:T(8,128)(2,1)S(1)}, bf16[104,1024]{1,0:T(8,128)(2,1)S(1)}, u32[]{:S(2)}, u32[]{:S(2)}) %collective-permute-start.3) | collective-permute-done | bytes 213024 | tf_op jit(solution)/shard_map/ppermute | solution.py:581
  33.3 2.6 %collective-permute-start.14 = (bf16[32,1024]{1,0:T(8,128)(2,1)S(1)}, bf16[32,1024]{1,0:T(8,128)(2,1)S(1)}, u32[]{:S(2)}, u32[]{:S(2)}) collective-permute-start(bf16[32,1024]{1,0:T(8,128)(2,1)S(1)} %get-tuple-element.52), channel_id=1, source_target_pairs={{0,8},{4,12},{8,0},{12,4},{1,9},{5,13},{9,1},{13,5},{2,10},{6,14},... | collective-permute-start | bytes 196616 | tf_op jit(solution)/shard_map/ppermute | solution.py:581
  35.9 0.0 collective-permute-done.9.refs_6_
  35.9 0.8 %collective-permute-start.15 = (bf16[32,1024]{1,0:T(8,128)(2,1)S(1)}, bf16[32,1024]{1,0:T(8,128)(2,1)S(1)}, u32[]{:S(2)}, u32[]{:S(2)}) collective-permute-start(bf16[32,1024]{1,0:T(8,128)(2,1)S(1)} %get-tuple-element.53), channel_id=1, source_target_pairs={{0,12},{4,8},{8,4},{12,0},{1,13},{5,9},{9,5},{13,1},{2,14},{6,10},... | collective-permute-start | bytes 196616 | tf_op jit(solution)/shard_map/ppermute | solution.py:581
  36.7 0.0 copy-done
  36.7 1.1 %assemble.1.refs_4_ = bf16[4,256,512]{2,1,0:T(8,128)(2,1)S(1)} custom-call(bf16[256,512]{1,0:T(8,128)(2,1)S(1)} %copy-done, bf16[128,512]{1,0:T(8,128)(2,1)S(1)} %collective-permute-done.refs_1_, bf16[128,512]{1,0:T(8,128)(2,1)S(1)} %collective-permute-done.6.refs_2_, bf16[128,512]{1,0:T(8,128)(2,1)S(1)} %collective-permute-done.1.refs_3_, ...), custom_call_target="tpu_custom_call" | custom-call | flops 4000000 | bytes 1048576 | tf_op jit(solution)/shard_map/assemble/pallas_call | solution.py:154
  37.8 0.0 collective-permute-done.4.refs_2_
  37.9 9.2 %collective-permute-done.5.refs_3_ = bf16[104,1024]{1,0:T(8,128)(2,1)S(1)} collective-permute-done((bf16[104,1024]{1,0:T(8,128)(2,1)S(1)}, bf16[104,1024]{1,0:T(8,128)(2,1)S(1)}, u32[]{:S(2)}, u32[]{:S(2)}) %collective-permute-start.5) | collective-permute-done | bytes 213024 | tf_op jit(solution)/shard_map/ppermute | solution.py:581
  47.0 2.0 %propose.2 = (f32[96,512]{1,0:T(8,128)S(1)}, bf16[96,512]{1,0:T(8,128)(2,1)S(1)}, bf16[96,512]{1,0:T(8,128)(2,1)S(1)}, bf16[96,512]{1,0:T(8,128)(2,1)S(1)}, f32[8,1024]{1,0:T(8,128)S(1)}) custom-call(f32[8,256]{1,0:T(8,128)S(1)} %get-tuple-element.31.const_ref, bf16[32,64,256]{2,1,0:T(8,128)(2,1)S(1)} %get-tuple-element.32.s_ref, ...), custom_call_target="tpu_custom_call" | custom-call | flops 96000000 | bytes 2097152 | tf_op jit(solution)/shard_map/propose/pallas_call | solution.py:482
  49.0 3.3 %collective-permute-start.10 = (bf16[96,512]{1,0:T(8,128)(2,1)S(1)}, bf16[96,512]{1,0:T(8,128)(2,1)S(1)}, u32[]{:S(2)}, u32[]{:S(2)}) collective-permute-start(bf16[96,512]{1,0:T(8,128)(2,1)S(1)} %get-tuple-element.47), channel_id=1, source_target_pairs={{0,1},{1,0},{2,3},{3,2},{4,5},{5,4},{6,7},{7,6},{8,9},{9,8},{10,11... | collective-permute-start | bytes 294920 | tf_op jit(solution)/shard_map/ppermute | solution.py:640
  52.3 0.6 collective-permute-start.11
  52.9 0.0 collective-permute-done.13.refs_1_
  52.9 1.2 %collective-permute-start.12 = (bf16[96,512]{1,0:T(8,128)(2,1)S(1)}, bf16[96,512]{1,0:T(8,128)(2,1)S(1)}, u32[]{:S(2)}, u32[]{:S(2)}) collective-permute-start(bf16[96,512]{1,0:T(8,128)(2,1)S(1)} %get-tuple-element.49), channel_id=1, source_target_pairs={{0,3},{1,2},{2,1},{3,0},{4,7},{5,6},{6,5},{7,4},{8,11},{9,10},{10,... | collective-permute-start | bytes 294920 | tf_op jit(solution)/shard_map/ppermute | solution.py:640
  54.0 0.0 collective-permute-done.14.refs_2_
  54.1 0.0 collective-permute-done.15.refs_3_
  54.1 1.2 %propose.3 = (f32[32,512]{1,0:T(8,128)S(1)}, bf16[32,512]{1,0:T(8,128)(2,1)S(1)}, bf16[32,512]{1,0:T(8,128)(2,1)S(1)}, bf16[32,512]{1,0:T(8,128)(2,1)S(1)}) custom-call(f32[8,256]{1,0:T(8,128)S(1)} %get-tuple-element.31.const_ref, bf16[32,64,256]{2,1,0:T(8,128)(2,1)S(1)} %get-tuple-element.32.s_ref, f32[32,1024]{1,0:T(8,128)S(1)} %get-tuple-element.50.refs_0_, ...), custom_call_target="tpu_custom_call" | custom-call | flops 32000000 | bytes 2097152 | tf_op jit(solution)/shard_map/propose/pallas_call | solution.py:482
  55.3 0.2 collective-permute-start.16
  55.5 0.6 collective-permute-start.17
  56.0 0.5 collective-permute-done.16.refs_5_
  56.5 0.9 %collective-permute-start.18 = (bf16[32,512]{1,0:T(8,128)(2,1)S(1)}, bf16[32,512]{1,0:T(8,128)(2,1)S(1)}, u32[]{:S(2)}, u32[]{:S(2)}) collective-permute-start(bf16[32,512]{1,0:T(8,128)(2,1)S(1)} %get-tuple-element.58), channel_id=1, source_target_pairs={{0,3},{1,2},{2,1},{3,0},{4,7},{5,6},{6,5},{7,4},{8,11},{9,10},{10,... | collective-permute-start | bytes 98312 | tf_op jit(solution)/shard_map/ppermute | solution.py:640
  57.5 1.7 %collective-permute-done.17.refs_6_ = bf16[32,512]{1,0:T(8,128)(2,1)S(1)} collective-permute-done((bf16[32,512]{1,0:T(8,128)(2,1)S(1)}, bf16[32,512]{1,0:T(8,128)(2,1)S(1)}, u32[]{:S(2)}, u32[]{:S(2)}) %collective-permute-start.17) | collective-permute-done | bytes 32800 | tf_op jit(solution)/shard_map/ppermute | solution.py:640
  59.1 1.2 %collective-permute-done.18.refs_7_ = bf16[32,512]{1,0:T(8,128)(2,1)S(1)} collective-permute-done((bf16[32,512]{1,0:T(8,128)(2,1)S(1)}, bf16[32,512]{1,0:T(8,128)(2,1)S(1)}, u32[]{:S(2)}, u32[]{:S(2)}) %collective-permute-start.18) | collective-permute-done | bytes 32800 | tf_op jit(solution)/shard_map/ppermute | solution.py:640
  60.4 0.0 collective-permute-done.10.refs_1_
  60.4 0.0 collective-permute-done.11.refs_2_
  60.4 0.0 collective-permute-done.12.refs_3_
  60.4 0.8 %finish.1 = bf16[32,4,512]{2,1,0:T(4,128)(2,1)} custom-call(f32[96,512]{1,0:T(8,128)S(1)} %get-tuple-element.46.refs_0_, bf16[96,512]{1,0:T(8,128)(2,1)S(1)} %collective-permute-done.10.refs_1_, bf16[96,512]{1,0:T(8,128)(2,1)S(1)} %collective-permute-done.11.refs_2_, bf16[96,512]{1,0:T(8,128)(2,1)S(1)} %collective-permute-done.12.refs_3_, ...), custom_call_target="tpu_custom_call" | custom-call | tf_op jit(solution)/shard_map/finish/pallas_call | solution.py:514
Async XLA Ops:
  0.6 11.3 %collective-permute-start.2 = (bf16[32,4,512]{2,1,0:T(4,128)(2,1)}, bf16[32,4,512]{2,1,0:T(4,128)(2,1)S(1)}, u32[]{:S(2)}, u32[]{:S(2)}) collective-permute-start(bf16[32,4,512]{2,1,0:T(4,128)(2,1)} %param.17), channel_id=1, source_target_pairs={{0,0},{1,5},{2,10},{3,15},{4,1},{5,4},{6,11},{7,14},{8,2},{9,7},{1... | collective-permute-start | bytes 393224 | tf_op jit(solution)/shard_map/ppermute | solution.py:572
  8.6 28.1 %copy-start = (bf16[256,512]{1,0:T(8,128)(2,1)S(1)}, bf16[256,512]{1,0:T(8,128)(2,1)}, u32[]{:S(2)}) copy-start(bf16[256,512]{1,0:T(8,128)(2,1)} %refs_0_.3) | copy-start | bytes 786436
  8.6 12.2 %collective-permute-start = (bf16[128,512]{1,0:T(8,128)(2,1)S(1)}, bf16[128,512]{1,0:T(8,128)(2,1)S(1)}, u32[]{:S(2)}, u32[]{:S(2)}) collective-permute-start(bf16[128,512]{1,0:T(8,128)(2,1)S(1)} %get-tuple-element.33), channel_id=1, source_target_pairs={{0,8},{4,12},{8,0},{12,4},{1,9},{5,13},{9,1},{13,5},{2,10},{6,14},... | collective-permute-start | bytes 393224 | tf_op jit(solution)/shard_map/ppermute | solution.py:581
  11.9 8.9 %collective-permute-start.1 = (bf16[128,512]{1,0:T(8,128)(2,1)S(1)}, bf16[128,512]{1,0:T(8,128)(2,1)S(1)}, u32[]{:S(2)}, u32[]{:S(2)}) collective-permute-start(bf16[128,512]{1,0:T(8,128)(2,1)S(1)} %get-tuple-element.33), channel_id=1, source_target_pairs={{0,4},{4,0},{8,12},{12,8},{1,5},{5,1},{9,13},{13,9},{2,6},{6,2},{1... | collective-permute-start | bytes 393224 | tf_op jit(solution)/shard_map/ppermute | solution.py:581
  20.8 5.2 %collective-permute-start.8 = (bf16[128,512]{1,0:T(8,128)(2,1)S(1)}, bf16[128,512]{1,0:T(8,128)(2,1)S(1)}, u32[]{:S(2)}, u32[]{:S(2)}) collective-permute-start(bf16[128,512]{1,0:T(8,128)(2,1)S(1)} %collective-permute-done.refs_1_), channel_id=1, source_target_pairs={{0,4},{4,0},{8,12},{12,8},{1,5},{5,1},{9,13},{13,9},{2,6},{6,2},{1... | collective-permute-start | bytes 393224 | tf_op jit(solution)/shard_map/ppermute | solution.py:581
  22.2 4.9 %collective-permute-start.6 = (bf16[128,512]{1,0:T(8,128)(2,1)S(1)}, bf16[128,512]{1,0:T(8,128)(2,1)S(1)}, u32[]{:S(2)}, u32[]{:S(2)}) collective-permute-start(bf16[128,512]{1,0:T(8,128)(2,1)S(1)} %collective-permute-done.refs_1_), channel_id=1, source_target_pairs={{0,16},{16,0},{1,17},{17,1},{2,18},{18,2},{3,19},{19,3},{4,20},{20... | collective-permute-start | bytes 393224 | tf_op jit(solution)/shard_map/ppermute | solution.py:606
  23.4 9.9 %collective-permute-start.3 = (bf16[104,1024]{1,0:T(8,128)(2,1)S(1)}, bf16[104,1024]{1,0:T(8,128)(2,1)S(1)}, u32[]{:S(2)}, u32[]{:S(2)}) collective-permute-start(bf16[104,1024]{1,0:T(8,128)(2,1)S(1)} %get-tuple-element.41), channel_id=1, source_target_pairs={{0,4},{4,0},{8,12},{12,8},{1,5},{5,1},{9,13},{13,9},{2,6},{6,2},{1... | collective-permute-start | bytes 638984 | tf_op jit(solution)/shard_map/ppermute | solution.py:581
  23.6 14.2 %collective-permute-start.4 = (bf16[104,1024]{1,0:T(8,128)(2,1)S(1)}, bf16[104,1024]{1,0:T(8,128)(2,1)S(1)}, u32[]{:S(2)}, u32[]{:S(2)}) collective-permute-start(bf16[104,1024]{1,0:T(8,128)(2,1)S(1)} %get-tuple-element.42), channel_id=1, source_target_pairs={{0,8},{4,12},{8,0},{12,4},{1,9},{5,13},{9,1},{13,5},{2,10},{6,14},... | collective-permute-start | bytes 638984 | tf_op jit(solution)/shard_map/ppermute | solution.py:581
  25.7 21.3 %collective-permute-start.5 = (bf16[104,1024]{1,0:T(8,128)(2,1)S(1)}, bf16[104,1024]{1,0:T(8,128)(2,1)S(1)}, u32[]{:S(2)}, u32[]{:S(2)}) collective-permute-start(bf16[104,1024]{1,0:T(8,128)(2,1)S(1)} %get-tuple-element.43), channel_id=1, source_target_pairs={{0,12},{4,8},{8,4},{12,0},{1,13},{5,9},{9,5},{13,1},{2,14},{6,10},... | collective-permute-start | bytes 638984 | tf_op jit(solution)/shard_map/ppermute | solution.py:581
  26.1 4.1 %collective-permute-start.7 = (bf16[128,512]{1,0:T(8,128)(2,1)S(1)}, bf16[128,512]{1,0:T(8,128)(2,1)S(1)}, u32[]{:S(2)}, u32[]{:S(2)}) collective-permute-start(bf16[128,512]{1,0:T(8,128)(2,1)S(1)} %collective-permute-done.1.refs_3_), channel_id=1, source_target_pairs={{0,16},{16,0},{1,17},{17,1},{2,18},{18,2},{3,19},{19,3},{4,20},{20... | collective-permute-start | bytes 393224 | tf_op jit(solution)/shard_map/ppermute | solution.py:606
  27.0 8.9 %collective-permute-start.9 = (bf16[128,512]{1,0:T(8,128)(2,1)S(1)}, bf16[128,512]{1,0:T(8,128)(2,1)S(1)}, u32[]{:S(2)}, u32[]{:S(2)}) collective-permute-start(bf16[128,512]{1,0:T(8,128)(2,1)S(1)} %collective-permute-done.8.refs_5_), channel_id=1, source_target_pairs={{0,16},{16,0},{1,17},{17,1},{2,18},{18,2},{3,19},{19,3},{4,20},{20... | collective-permute-start | bytes 393224 | tf_op jit(solution)/shard_map/ppermute | solution.py:606
  30.2 22.7 %collective-permute-start.13 = (bf16[32,1024]{1,0:T(8,128)(2,1)S(1)}, bf16[32,1024]{1,0:T(8,128)(2,1)S(1)}, u32[]{:S(2)}, u32[]{:S(2)}) collective-permute-start(bf16[32,1024]{1,0:T(8,128)(2,1)S(1)} %get-tuple-element.51), channel_id=1, source_target_pairs={{0,4},{4,0},{8,12},{12,8},{1,5},{5,1},{9,13},{13,9},{2,6},{6,2},{1... | collective-permute-start | bytes 196616 | tf_op jit(solution)/shard_map/ppermute | solution.py:581
  33.3 20.7 %collective-permute-start.14 = (bf16[32,1024]{1,0:T(8,128)(2,1)S(1)}, bf16[32,1024]{1,0:T(8,128)(2,1)S(1)}, u32[]{:S(2)}, u32[]{:S(2)}) collective-permute-start(bf16[32,1024]{1,0:T(8,128)(2,1)S(1)} %get-tuple-element.52), channel_id=1, source_target_pairs={{0,8},{4,12},{8,0},{12,4},{1,9},{5,13},{9,1},{13,5},{2,10},{6,14},... | collective-permute-start | bytes 196616 | tf_op jit(solution)/shard_map/ppermute | solution.py:581
  35.9 18.2 %collective-permute-start.15 = (bf16[32,1024]{1,0:T(8,128)(2,1)S(1)}, bf16[32,1024]{1,0:T(8,128)(2,1)S(1)}, u32[]{:S(2)}, u32[]{:S(2)}) collective-permute-start(bf16[32,1024]{1,0:T(8,128)(2,1)S(1)} %get-tuple-element.53), channel_id=1, source_target_pairs={{0,12},{4,8},{8,4},{12,0},{1,13},{5,9},{9,5},{13,1},{2,14},{6,10},... | collective-permute-start | bytes 196616 | tf_op jit(solution)/shard_map/ppermute | solution.py:581
  49.0 11.3 %collective-permute-start.10 = (bf16[96,512]{1,0:T(8,128)(2,1)S(1)}, bf16[96,512]{1,0:T(8,128)(2,1)S(1)}, u32[]{:S(2)}, u32[]{:S(2)}) collective-permute-start(bf16[96,512]{1,0:T(8,128)(2,1)S(1)} %get-tuple-element.47), channel_id=1, source_target_pairs={{0,1},{1,0},{2,3},{3,2},{4,5},{5,4},{6,7},{7,6},{8,9},{9,8},{10,11... | collective-permute-start | bytes 294920 | tf_op jit(solution)/shard_map/ppermute | solution.py:640
  52.3 8.0 %collective-permute-start.11 = (bf16[96,512]{1,0:T(8,128)(2,1)S(1)}, bf16[96,512]{1,0:T(8,128)(2,1)S(1)}, u32[]{:S(2)}, u32[]{:S(2)}) collective-permute-start(bf16[96,512]{1,0:T(8,128)(2,1)S(1)} %get-tuple-element.48), channel_id=1, source_target_pairs={{0,2},{1,3},{2,0},{3,1},{4,6},{5,7},{6,4},{7,5},{8,10},{9,11},{10,... | collective-permute-start | bytes 294920 | tf_op jit(solution)/shard_map/ppermute | solution.py:640
  52.9 7.5 %collective-permute-start.12 = (bf16[96,512]{1,0:T(8,128)(2,1)S(1)}, bf16[96,512]{1,0:T(8,128)(2,1)S(1)}, u32[]{:S(2)}, u32[]{:S(2)}) collective-permute-start(bf16[96,512]{1,0:T(8,128)(2,1)S(1)} %get-tuple-element.49), channel_id=1, source_target_pairs={{0,3},{1,2},{2,1},{3,0},{4,7},{5,6},{6,5},{7,4},{8,11},{9,10},{10,... | collective-permute-start | bytes 294920 | tf_op jit(solution)/shard_map/ppermute | solution.py:640
  55.3 1.3 %collective-permute-start.16 = (bf16[32,512]{1,0:T(8,128)(2,1)S(1)}, bf16[32,512]{1,0:T(8,128)(2,1)S(1)}, u32[]{:S(2)}, u32[]{:S(2)}) collective-permute-start(bf16[32,512]{1,0:T(8,128)(2,1)S(1)} %get-tuple-element.56), channel_id=1, source_target_pairs={{0,1},{1,0},{2,3},{3,2},{4,5},{5,4},{6,7},{7,6},{8,9},{9,8},{10,11... | collective-permute-start | bytes 98312 | tf_op jit(solution)/shard_map/ppermute | solution.py:640
  55.5 3.7 %collective-permute-start.17 = (bf16[32,512]{1,0:T(8,128)(2,1)S(1)}, bf16[32,512]{1,0:T(8,128)(2,1)S(1)}, u32[]{:S(2)}, u32[]{:S(2)}) collective-permute-start(bf16[32,512]{1,0:T(8,128)(2,1)S(1)} %get-tuple-element.57), channel_id=1, source_target_pairs={{0,2},{1,3},{2,0},{3,1},{4,6},{5,7},{6,4},{7,5},{8,10},{9,11},{10,... | collective-permute-start | bytes 98312 | tf_op jit(solution)/shard_map/ppermute | solution.py:640
  56.5 3.9 %collective-permute-start.18 = (bf16[32,512]{1,0:T(8,128)(2,1)S(1)}, bf16[32,512]{1,0:T(8,128)(2,1)S(1)}, u32[]{:S(2)}, u32[]{:S(2)}) collective-permute-start(bf16[32,512]{1,0:T(8,128)(2,1)S(1)} %get-tuple-element.58), channel_id=1, source_target_pairs={{0,3},{1,2},{2,1},{3,0},{4,7},{5,6},{6,5},{7,4},{8,11},{9,10},{10,... | collective-permute-start | bytes 98312 | tf_op jit(solution)/shard_map/ppermute | solution.py:640

commit v5 on v4

--- a/solution.py
+++ b/solution.py
@@ -70,10 +70,10 @@
 
 
 def project_kernel(chunks, layout, x_ref, gain_ref, weight_ref, small_ref, *outs):
-    owners, _, steps, local = x_ref.shape
+    _, _, steps, local = x_ref.shape
     gain = gain_ref[0:1, :]
     raw, spans, start = [], {}, 0
-    for d in range(owners):
+    for d in sorted({d for d, _, _ in layout}):
         tokens = [x_ref[d, :, t, :].astype(F32) for t in range(steps)]
         for c, (first, each) in enumerate(chunks):
             raw += [x[first : first + each] for x in tokens]
@@ -585,11 +585,17 @@
         halves.append(swap(mine, bits[1]))
         marks.append(bits[1])
         gathered = lax.all_gather(turned, "tp")
-        layout = [
-            (i, (c,), c == 0, F32 if i == 0 else BF16) for c in range(len(chunks)) for i in range(n)
-        ]
-        products = project(gathered, own_gain, weight, small, chunks, layout)
-        parts = [list(products[c * n : (c + 1) * n]) for c in range(len(chunks))]
+        parts = [[None] * n for _ in chunks]
+        rest = [i for i in range(n) if i != bits[0]]
+        for owners in ([bits[0]], rest):
+            layout = [
+                (i, (c,), c == 0, F32 if i == 0 else BF16)
+                for c in range(len(chunks))
+                for i in owners
+            ]
+            products = project(gathered, own_gain, weight, small, chunks, layout)
+            for (i, (c,), _, _), product in zip(layout, products):
+                parts[c][i] = product
         spans = []
         for c, (first, each) in enumerate(chunks):
             for i in range(1, n):

time: 61.3 us -> 61.6 us (level)
    pallas_call x1 -> x2, Pallas kernels: 1.46 us -> 1.63 us  [project(): pl.pallas_call(functools.partial(project_kernel, chunks, [entry[:3] for e...]
where the time goes in v5:
time: 61.6 us; the launch traced here: 61.5 us
  starting transfers between devices  23.7 us (38%)
  waiting for transfers between devices  17.4 us (28%)
  Pallas kernels  12.2 us (20%)
  blocking collectives  7.45 us (12%)
  between operations  0.72 us (1%)
    ppermute x9, starting transfers between devices, swap(): return lax.ppermute(array, 'kv', [(i, i ^ bit) for i in range(n)])  11.7 us
    ppermute x9, waiting for transfers between devices, swap(): return lax.ppermute(array, 'kv', [(i, i ^ bit) for i in range(n)])  11.3 us
    all_gather x1, blocking collectives, layer(): gathered = lax.all_gather(turned, 'tp')  7.45 us
    ppermute x6, starting transfers between devices, layer(): lax.ppermute(out[s], 'tp', [(i, i ^ s) for i in range(n_tp)])  6.63 us
    pallas_call x1, Pallas kernels, early(): pl.pallas_call(functools.partial(early_kernel, steps, size, axes, count),...  5.4 us
    ppermute x6, waiting for transfers between devices, layer(): lax.ppermute(out[s], 'tp', [(i, i ^ s) for i in range(n_tp)])  3.48 us
    pallas_call x2, Pallas kernels, propose(): pl.pallas_call(functools.partial(propose_kernel, dims, axis, spans, first...  3.24 us
    ppermute x3, starting transfers between devices, layer(): other = lax.ppermute(halves[i], 'grp', ring(n_grp, 1))  2.78 us
  transfers between devices with their start and end apart: 19, of which 6 were waited for; matrix products, arithmetic and copies ran while one was open for 0% of the time, Pallas kernels for 18%

profile of v5, /device:TPU:9, one launch (start us, length us, event | category | flops | bytes accessed | tf_op | source)
XLA Modules:
  0.0 61.5 jit_solution(11226504658906754312)
XLA Ops:
  0.6 2.6 %collective-permute-start.2 = (bf16[32,4,512]{2,1,0:T(4,128)(2,1)}, bf16[32,4,512]{2,1,0:T(4,128)(2,1)S(1)}, u32[]{:S(2)}, u32[]{:S(2)}) collective-permute-start(bf16[32,4,512]{2,1,0:T(4,128)(2,1)} %param.17), channel_id=1, source_target_pairs={{0,0},{1,5},{2,10},{3,15},{4,1},{5,4},{6,11},{7,14},{8,2},{9,7},{1... | collective-permute-start | bytes 393224 | tf_op jit(solution)/shard_map/ppermute | solution.py:572
  3.2 5.4 %early.1 = (f32[32,64,256]{2,1,0:T(8,128)}, bf16[32,64,256]{2,1,0:T(8,128)(2,1)S(1)}, f32[8,256]{1,0:T(8,128)S(1)}, bf16[512,1024]{1,0:T(8,128)(2,1)S(1)}, f32[8...) custom-call(bf16[32,4,256]{2,1,0:T(4,128)(2,1)} %refs_0_.2, ...), custom_call_target="tpu_custom_call" | custom-call | flops 128000000 | bytes 4194304 | tf_op jit(solution)/shard_map/early/pallas_call | solution.py:340
  8.6 3.2 %collective-permute-start = (bf16[128,512]{1,0:T(8,128)(2,1)S(1)}, bf16[128,512]{1,0:T(8,128)(2,1)S(1)}, u32[]{:S(2)}, u32[]{:S(2)}) collective-permute-start(bf16[128,512]{1,0:T(8,128)(2,1)S(1)} %get-tuple-element.33), channel_id=1, source_target_pairs={{0,8},{4,12},{8,0},{12,4},{1,9},{5,13},{9,1},{13,5},{2,10},{6,14},... | collective-permute-start | bytes 393224 | tf_op jit(solution)/shard_map/ppermute | solution.py:581
  11.9 0.0 collective-permute-start.1
  11.9 0.0 collective-permute-done.2
  11.9 7.4 %all-gather = bf16[128,4,512]{2,1,0:T(4,128)(2,1)S(1)} all-gather(bf16[32,4,512]{2,1,0:T(4,128)(2,1)S(1)} %collective-permute-done.2), channel_id=2, replica_groups=mesh['grp'=2,'kv'=4,'tp'=4] {'tp'}, dimensions={0}, use_global_device_ids=true | all-gather | bytes 655360 | tf_op jit(solution)/shard_map/all_gather | solution.py:587
  19.3 0.0 copy-start
  19.3 1.1 %shard_map.176 = (f32[104,1024]{1,0:T(8,128)S(1)}, bf16[104,1024]{1,0:T(8,128)(2,1)S(1)}, bf16[104,1024]{1,0:T(8,128)(2,1)S(1)}, f32[32,1024]{1,0:T(8,128)S(1)},...) custom-call(bf16[4,32,4,512]{3,2,1,0:T(4,128)(2,1)S(1)} %bitcast.9, f32[8,512]{1,0:T(8,128)S(1)} %get-tuple-element.36.gain_ref, ...), custom_call_target="tpu_custom_call" | custom-call | flops 536870912 | bytes 1048576 | tf_op jit(solution)/shard_map/pallas_call | solution.py:126
  20.5 0.0 collective-permute-done.refs_1_
  20.5 0.0 collective-permute-done.1.refs_3_
  20.5 1.3 %collective-permute-start.6 = (bf16[128,512]{1,0:T(8,128)(2,1)S(1)}, bf16[128,512]{1,0:T(8,128)(2,1)S(1)}, u32[]{:S(2)}, u32[]{:S(2)}) collective-permute-start(bf16[128,512]{1,0:T(8,128)(2,1)S(1)} %collective-permute-done.refs_1_), channel_id=1, source_target_pairs={{0,16},{16,0},{1,17},{17,1},{2,18},{18,2},{3,19},{19,3},{4,20},{20... | collective-permute-start | bytes 393224 | tf_op jit(solution)/shard_map/ppermute | solution.py:612
  21.8 1.3 %collective-permute-start.8 = (bf16[128,512]{1,0:T(8,128)(2,1)S(1)}, bf16[128,512]{1,0:T(8,128)(2,1)S(1)}, u32[]{:S(2)}, u32[]{:S(2)}) collective-permute-start(bf16[128,512]{1,0:T(8,128)(2,1)S(1)} %collective-permute-done.refs_1_), channel_id=1, source_target_pairs={{0,4},{4,0},{8,12},{12,8},{1,5},{5,1},{9,13},{13,9},{2,6},{6,2},{1... | collective-permute-start | bytes 393224 | tf_op jit(solution)/shard_map/ppermute | solution.py:581
  23.1 0.2 collective-permute-start.3
  23.3 0.5 shard_map.177
  23.8 2.1 %collective-permute-start.4 = (bf16[104,1024]{1,0:T(8,128)(2,1)S(1)}, bf16[104,1024]{1,0:T(8,128)(2,1)S(1)}, u32[]{:S(2)}, u32[]{:S(2)}) collective-permute-start(bf16[104,1024]{1,0:T(8,128)(2,1)S(1)} %get-tuple-element.42), channel_id=1, source_target_pairs={{0,8},{4,12},{8,0},{12,4},{1,9},{5,13},{9,1},{13,5},{2,10},{6,14},... | collective-permute-start | bytes 638984 | tf_op jit(solution)/shard_map/ppermute | solution.py:581
  25.9 0.4 collective-permute-start.5
  26.3 0.0 collective-permute-done.6.refs_2_
  26.3 0.4 collective-permute-start.7
  26.7 0.0 collective-permute-done.8.refs_5_
  26.7 1.1 %collective-permute-start.9 = (bf16[128,512]{1,0:T(8,128)(2,1)S(1)}, bf16[128,512]{1,0:T(8,128)(2,1)S(1)}, u32[]{:S(2)}, u32[]{:S(2)}) collective-permute-start(bf16[128,512]{1,0:T(8,128)(2,1)S(1)} %collective-permute-done.8.refs_5_), channel_id=1, source_target_pairs={{0,16},{16,0},{1,17},{17,1},{2,18},{18,2},{3,19},{19,3},{4,20},{20... | collective-permute-start | bytes 393224 | tf_op jit(solution)/shard_map/ppermute | solution.py:612
  27.8 2.6 %collective-permute-done.7.refs_4_ = bf16[128,512]{1,0:T(8,128)(2,1)S(1)} collective-permute-done((bf16[128,512]{1,0:T(8,128)(2,1)S(1)}, bf16[128,512]{1,0:T(8,128)(2,1)S(1)}, u32[]{:S(2)}, u32[]{:S(2)}) %collective-permute-start.7) | collective-permute-done | bytes 131104 | tf_op jit(solution)/shard_map/ppermute | solution.py:612
  30.4 1.1 %collective-permute-start.13 = (bf16[32,1024]{1,0:T(8,128)(2,1)S(1)}, bf16[32,1024]{1,0:T(8,128)(2,1)S(1)}, u32[]{:S(2)}, u32[]{:S(2)}) collective-permute-start(bf16[32,1024]{1,0:T(8,128)(2,1)S(1)} %get-tuple-element.51), channel_id=1, source_target_pairs={{0,4},{4,0},{8,12},{12,8},{1,5},{5,1},{9,13},{13,9},{2,6},{6,2},{1... | collective-permute-start | bytes 196616 | tf_op jit(solution)/shard_map/ppermute | solution.py:581
  31.5 2.8 %collective-permute-done.3.refs_1_ = bf16[104,1024]{1,0:T(8,128)(2,1)S(1)} collective-permute-done((bf16[104,1024]{1,0:T(8,128)(2,1)S(1)}, bf16[104,1024]{1,0:T(8,128)(2,1)S(1)}, u32[]{:S(2)}, u32[]{:S(2)}) %collective-permute-start.3) | collective-permute-done | bytes 213024 | tf_op jit(solution)/shard_map/ppermute | solution.py:581
  34.3 2.6 %collective-permute-start.14 = (bf16[32,1024]{1,0:T(8,128)(2,1)S(1)}, bf16[32,1024]{1,0:T(8,128)(2,1)S(1)}, u32[]{:S(2)}, u32[]{:S(2)}) collective-permute-start(bf16[32,1024]{1,0:T(8,128)(2,1)S(1)} %get-tuple-element.52), channel_id=1, source_target_pairs={{0,8},{4,12},{8,0},{12,4},{1,9},{5,13},{9,1},{13,5},{2,10},{6,14},... | collective-permute-start | bytes 196616 | tf_op jit(solution)/shard_map/ppermute | solution.py:581
  36.9 0.0 collective-permute-done.9.refs_6_
  36.9 0.8 %collective-permute-start.15 = (bf16[32,1024]{1,0:T(8,128)(2,1)S(1)}, bf16[32,1024]{1,0:T(8,128)(2,1)S(1)}, u32[]{:S(2)}, u32[]{:S(2)}) collective-permute-start(bf16[32,1024]{1,0:T(8,128)(2,1)S(1)} %get-tuple-element.53), channel_id=1, source_target_pairs={{0,12},{4,8},{8,4},{12,0},{1,13},{5,9},{9,5},{13,1},{2,14},{6,10},... | collective-permute-start | bytes 196616 | tf_op jit(solution)/shard_map/ppermute | solution.py:581
  37.7 0.0 copy-done
  37.7 1.1 %assemble.1.refs_4_ = bf16[4,256,512]{2,1,0:T(8,128)(2,1)S(1)} custom-call(bf16[256,512]{1,0:T(8,128)(2,1)S(1)} %copy-done, bf16[128,512]{1,0:T(8,128)(2,1)S(1)} %collective-permute-done.refs_1_, bf16[128,512]{1,0:T(8,128)(2,1)S(1)} %collective-permute-done.6.refs_2_, bf16[128,512]{1,0:T(8,128)(2,1)S(1)} %collective-permute-done.1.refs_3_, ...), custom_call_target="tpu_custom_call" | custom-call | flops 4000000 | bytes 1048576 | tf_op jit(solution)/shard_map/assemble/pallas_call | solution.py:154
  38.8 0.0 collective-permute-done.4.refs_2_
  38.8 8.4 %collective-permute-done.5.refs_3_ = bf16[104,1024]{1,0:T(8,128)(2,1)S(1)} collective-permute-done((bf16[104,1024]{1,0:T(8,128)(2,1)S(1)}, bf16[104,1024]{1,0:T(8,128)(2,1)S(1)}, u32[]{:S(2)}, u32[]{:S(2)}) %collective-permute-start.5) | collective-permute-done | bytes 213024 | tf_op jit(solution)/shard_map/ppermute | solution.py:581
  47.3 2.0 %propose.2 = (f32[96,512]{1,0:T(8,128)S(1)}, bf16[96,512]{1,0:T(8,128)(2,1)S(1)}, bf16[96,512]{1,0:T(8,128)(2,1)S(1)}, bf16[96,512]{1,0:T(8,128)(2,1)S(1)}, f32[8,1024]{1,0:T(8,128)S(1)}) custom-call(f32[8,256]{1,0:T(8,128)S(1)} %get-tuple-element.31.const_ref, bf16[32,64,256]{2,1,0:T(8,128)(2,1)S(1)} %get-tuple-element.32.s_ref, ...), custom_call_target="tpu_custom_call" | custom-call | flops 96000000 | bytes 2097152 | tf_op jit(solution)/shard_map/propose/pallas_call | solution.py:482
  49.3 3.3 %collective-permute-start.10 = (bf16[96,512]{1,0:T(8,128)(2,1)S(1)}, bf16[96,512]{1,0:T(8,128)(2,1)S(1)}, u32[]{:S(2)}, u32[]{:S(2)}) collective-permute-start(bf16[96,512]{1,0:T(8,128)(2,1)S(1)} %get-tuple-element.47), channel_id=1, source_target_pairs={{0,1},{1,0},{2,3},{3,2},{4,5},{5,4},{6,7},{7,6},{8,9},{9,8},{10,11... | collective-permute-start | bytes 294920 | tf_op jit(solution)/shard_map/ppermute | solution.py:646
  52.6 0.5 collective-permute-start.11
  53.1 0.0 collective-permute-done.13.refs_1_
  53.1 1.2 %collective-permute-start.12 = (bf16[96,512]{1,0:T(8,128)(2,1)S(1)}, bf16[96,512]{1,0:T(8,128)(2,1)S(1)}, u32[]{:S(2)}, u32[]{:S(2)}) collective-permute-start(bf16[96,512]{1,0:T(8,128)(2,1)S(1)} %get-tuple-element.49), channel_id=1, source_target_pairs={{0,3},{1,2},{2,1},{3,0},{4,7},{5,6},{6,5},{7,4},{8,11},{9,10},{10,... | collective-permute-start | bytes 294920 | tf_op jit(solution)/shard_map/ppermute | solution.py:646
  54.3 0.0 collective-permute-done.14.refs_2_
  54.3 0.0 collective-permute-done.15.refs_3_
  54.3 1.2 %propose.3 = (f32[32,512]{1,0:T(8,128)S(1)}, bf16[32,512]{1,0:T(8,128)(2,1)S(1)}, bf16[32,512]{1,0:T(8,128)(2,1)S(1)}, bf16[32,512]{1,0:T(8,128)(2,1)S(1)}) custom-call(f32[8,256]{1,0:T(8,128)S(1)} %get-tuple-element.31.const_ref, bf16[32,64,256]{2,1,0:T(8,128)(2,1)S(1)} %get-tuple-element.32.s_ref, f32[32,1024]{1,0:T(8,128)S(1)} %get-tuple-element.50.refs_0_, ...), custom_call_target="tpu_custom_call" | custom-call | flops 32000000 | bytes 2097152 | tf_op jit(solution)/shard_map/propose/pallas_call | solution.py:482
  55.5 0.2 collective-permute-start.16
  55.7 0.5 collective-permute-start.17
  56.2 0.6 collective-permute-done.16.refs_5_
  56.8 0.9 %collective-permute-start.18 = (bf16[32,512]{1,0:T(8,128)(2,1)S(1)}, bf16[32,512]{1,0:T(8,128)(2,1)S(1)}, u32[]{:S(2)}, u32[]{:S(2)}) collective-permute-start(bf16[32,512]{1,0:T(8,128)(2,1)S(1)} %get-tuple-element.58), channel_id=1, source_target_pairs={{0,3},{1,2},{2,1},{3,0},{4,7},{5,6},{6,5},{7,4},{8,11},{9,10},{10,... | collective-permute-start | bytes 98312 | tf_op jit(solution)/shard_map/ppermute | solution.py:646
  57.7 1.7 %collective-permute-done.17.refs_6_ = bf16[32,512]{1,0:T(8,128)(2,1)S(1)} collective-permute-done((bf16[32,512]{1,0:T(8,128)(2,1)S(1)}, bf16[32,512]{1,0:T(8,128)(2,1)S(1)}, u32[]{:S(2)}, u32[]{:S(2)}) %collective-permute-start.17) | collective-permute-done | bytes 32800 | tf_op jit(solution)/shard_map/ppermute | solution.py:646
  59.4 1.2 %collective-permute-done.18.refs_7_ = bf16[32,512]{1,0:T(8,128)(2,1)S(1)} collective-permute-done((bf16[32,512]{1,0:T(8,128)(2,1)S(1)}, bf16[32,512]{1,0:T(8,128)(2,1)S(1)}, u32[]{:S(2)}, u32[]{:S(2)}) %collective-permute-start.18) | collective-permute-done | bytes 32800 | tf_op jit(solution)/shard_map/ppermute | solution.py:646
  60.6 0.0 collective-permute-done.10.refs_1_
  60.6 0.0 collective-permute-done.11.refs_2_
  60.6 0.0 collective-permute-done.12.refs_3_
  60.6 0.8 %finish.1 = bf16[32,4,512]{2,1,0:T(4,128)(2,1)} custom-call(f32[96,512]{1,0:T(8,128)S(1)} %get-tuple-element.46.refs_0_, bf16[96,512]{1,0:T(8,128)(2,1)S(1)} %collective-permute-done.10.refs_1_, bf16[96,512]{1,0:T(8,128)(2,1)S(1)} %collective-permute-done.11.refs_2_, bf16[96,512]{1,0:T(8,128)(2,1)S(1)} %collective-permute-done.12.refs_3_, ...), custom_call_target="tpu_custom_call" | custom-call | tf_op jit(solution)/shard_map/finish/pallas_call | solution.py:514
Async XLA Ops:
  0.6 11.2 %collective-permute-start.2 = (bf16[32,4,512]{2,1,0:T(4,128)(2,1)}, bf16[32,4,512]{2,1,0:T(4,128)(2,1)S(1)}, u32[]{:S(2)}, u32[]{:S(2)}) collective-permute-start(bf16[32,4,512]{2,1,0:T(4,128)(2,1)} %param.17), channel_id=1, source_target_pairs={{0,0},{1,5},{2,10},{3,15},{4,1},{5,4},{6,11},{7,14},{8,2},{9,7},{1... | collective-permute-start | bytes 393224 | tf_op jit(solution)/shard_map/ppermute | solution.py:572
  8.6 11.8 %collective-permute-start = (bf16[128,512]{1,0:T(8,128)(2,1)S(1)}, bf16[128,512]{1,0:T(8,128)(2,1)S(1)}, u32[]{:S(2)}, u32[]{:S(2)}) collective-permute-start(bf16[128,512]{1,0:T(8,128)(2,1)S(1)} %get-tuple-element.33), channel_id=1, source_target_pairs={{0,8},{4,12},{8,0},{12,4},{1,9},{5,13},{9,1},{13,5},{2,10},{6,14},... | collective-permute-start | bytes 393224 | tf_op jit(solution)/shard_map/ppermute | solution.py:581
  11.9 8.6 %collective-permute-start.1 = (bf16[128,512]{1,0:T(8,128)(2,1)S(1)}, bf16[128,512]{1,0:T(8,128)(2,1)S(1)}, u32[]{:S(2)}, u32[]{:S(2)}) collective-permute-start(bf16[128,512]{1,0:T(8,128)(2,1)S(1)} %get-tuple-element.33), channel_id=1, source_target_pairs={{0,4},{4,0},{8,12},{12,8},{1,5},{5,1},{9,13},{13,9},{2,6},{6,2},{1... | collective-permute-start | bytes 393224 | tf_op jit(solution)/shard_map/ppermute | solution.py:581
  19.3 18.4 %copy-start = (bf16[256,512]{1,0:T(8,128)(2,1)S(1)}, bf16[256,512]{1,0:T(8,128)(2,1)}, u32[]{:S(2)}) copy-start(bf16[256,512]{1,0:T(8,128)(2,1)} %refs_0_.3) | copy-start | bytes 786436
  20.5 5.8 %collective-permute-start.6 = (bf16[128,512]{1,0:T(8,128)(2,1)S(1)}, bf16[128,512]{1,0:T(8,128)(2,1)S(1)}, u32[]{:S(2)}, u32[]{:S(2)}) collective-permute-start(bf16[128,512]{1,0:T(8,128)(2,1)S(1)} %collective-permute-done.refs_1_), channel_id=1, source_target_pairs={{0,16},{16,0},{1,17},{17,1},{2,18},{18,2},{3,19},{19,3},{4,20},{20... | collective-permute-start | bytes 393224 | tf_op jit(solution)/shard_map/ppermute | solution.py:612
  21.8 4.9 %collective-permute-start.8 = (bf16[128,512]{1,0:T(8,128)(2,1)S(1)}, bf16[128,512]{1,0:T(8,128)(2,1)S(1)}, u32[]{:S(2)}, u32[]{:S(2)}) collective-permute-start(bf16[128,512]{1,0:T(8,128)(2,1)S(1)} %collective-permute-done.refs_1_), channel_id=1, source_target_pairs={{0,4},{4,0},{8,12},{12,8},{1,5},{5,1},{9,13},{13,9},{2,6},{6,2},{1... | collective-permute-start | bytes 393224 | tf_op jit(solution)/shard_map/ppermute | solution.py:581
  23.1 11.2 %collective-permute-start.3 = (bf16[104,1024]{1,0:T(8,128)(2,1)S(1)}, bf16[104,1024]{1,0:T(8,128)(2,1)S(1)}, u32[]{:S(2)}, u32[]{:S(2)}) collective-permute-start(bf16[104,1024]{1,0:T(8,128)(2,1)S(1)} %get-tuple-element.41), channel_id=1, source_target_pairs={{0,4},{4,0},{8,12},{12,8},{1,5},{5,1},{9,13},{13,9},{2,6},{6,2},{1... | collective-permute-start | bytes 638984 | tf_op jit(solution)/shard_map/ppermute | solution.py:581
  23.8 15.1 %collective-permute-start.4 = (bf16[104,1024]{1,0:T(8,128)(2,1)S(1)}, bf16[104,1024]{1,0:T(8,128)(2,1)S(1)}, u32[]{:S(2)}, u32[]{:S(2)}) collective-permute-start(bf16[104,1024]{1,0:T(8,128)(2,1)S(1)} %get-tuple-element.42), channel_id=1, source_target_pairs={{0,8},{4,12},{8,0},{12,4},{1,9},{5,13},{9,1},{13,5},{2,10},{6,14},... | collective-permute-start | bytes 638984 | tf_op jit(solution)/shard_map/ppermute | solution.py:581
  25.9 21.4 %collective-permute-start.5 = (bf16[104,1024]{1,0:T(8,128)(2,1)S(1)}, bf16[104,1024]{1,0:T(8,128)(2,1)S(1)}, u32[]{:S(2)}, u32[]{:S(2)}) collective-permute-start(bf16[104,1024]{1,0:T(8,128)(2,1)S(1)} %get-tuple-element.43), channel_id=1, source_target_pairs={{0,12},{4,8},{8,4},{12,0},{1,13},{5,9},{9,5},{13,1},{2,14},{6,10},... | collective-permute-start | bytes 638984 | tf_op jit(solution)/shard_map/ppermute | solution.py:581
  26.3 4.1 %collective-permute-start.7 = (bf16[128,512]{1,0:T(8,128)(2,1)S(1)}, bf16[128,512]{1,0:T(8,128)(2,1)S(1)}, u32[]{:S(2)}, u32[]{:S(2)}) collective-permute-start(bf16[128,512]{1,0:T(8,128)(2,1)S(1)} %collective-permute-done.1.refs_3_), channel_id=1, source_target_pairs={{0,16},{16,0},{1,17},{17,1},{2,18},{18,2},{3,19},{19,3},{4,20},{20... | collective-permute-start | bytes 393224 | tf_op jit(solution)/shard_map/ppermute | solution.py:612
  26.7 10.2 %collective-permute-start.9 = (bf16[128,512]{1,0:T(8,128)(2,1)S(1)}, bf16[128,512]{1,0:T(8,128)(2,1)S(1)}, u32[]{:S(2)}, u32[]{:S(2)}) collective-permute-start(bf16[128,512]{1,0:T(8,128)(2,1)S(1)} %collective-permute-done.8.refs_5_), channel_id=1, source_target_pairs={{0,16},{16,0},{1,17},{17,1},{2,18},{18,2},{3,19},{19,3},{4,20},{20... | collective-permute-start | bytes 393224 | tf_op jit(solution)/shard_map/ppermute | solution.py:612
  30.4 22.7 %collective-permute-start.13 = (bf16[32,1024]{1,0:T(8,128)(2,1)S(1)}, bf16[32,1024]{1,0:T(8,128)(2,1)S(1)}, u32[]{:S(2)}, u32[]{:S(2)}) collective-permute-start(bf16[32,1024]{1,0:T(8,128)(2,1)S(1)} %get-tuple-element.51), channel_id=1, source_target_pairs={{0,4},{4,0},{8,12},{12,8},{1,5},{5,1},{9,13},{13,9},{2,6},{6,2},{1... | collective-permute-start | bytes 196616 | tf_op jit(solution)/shard_map/ppermute | solution.py:581
  34.3 20.0 %collective-permute-start.14 = (bf16[32,1024]{1,0:T(8,128)(2,1)S(1)}, bf16[32,1024]{1,0:T(8,128)(2,1)S(1)}, u32[]{:S(2)}, u32[]{:S(2)}) collective-permute-start(bf16[32,1024]{1,0:T(8,128)(2,1)S(1)} %get-tuple-element.52), channel_id=1, source_target_pairs={{0,8},{4,12},{8,0},{12,4},{1,9},{5,13},{9,1},{13,5},{2,10},{6,14},... | collective-permute-start | bytes 196616 | tf_op jit(solution)/shard_map/ppermute | solution.py:581
  36.9 17.4 %collective-permute-start.15 = (bf16[32,1024]{1,0:T(8,128)(2,1)S(1)}, bf16[32,1024]{1,0:T(8,128)(2,1)S(1)}, u32[]{:S(2)}, u32[]{:S(2)}) collective-permute-start(bf16[32,1024]{1,0:T(8,128)(2,1)S(1)} %get-tuple-element.53), channel_id=1, source_target_pairs={{0,12},{4,8},{8,4},{12,0},{1,13},{5,9},{9,5},{13,1},{2,14},{6,10},... | collective-permute-start | bytes 196616 | tf_op jit(solution)/shard_map/ppermute | solution.py:581
  49.3 11.3 %collective-permute-start.10 = (bf16[96,512]{1,0:T(8,128)(2,1)S(1)}, bf16[96,512]{1,0:T(8,128)(2,1)S(1)}, u32[]{:S(2)}, u32[]{:S(2)}) collective-permute-start(bf16[96,512]{1,0:T(8,128)(2,1)S(1)} %get-tuple-element.47), channel_id=1, source_target_pairs={{0,1},{1,0},{2,3},{3,2},{4,5},{5,4},{6,7},{7,6},{8,9},{9,8},{10,11... | collective-permute-start | bytes 294920 | tf_op jit(solution)/shard_map/ppermute | solution.py:646
  52.6 8.0 %collective-permute-start.11 = (bf16[96,512]{1,0:T(8,128)(2,1)S(1)}, bf16[96,512]{1,0:T(8,128)(2,1)S(1)}, u32[]{:S(2)}, u32[]{:S(2)}) collective-permute-start(bf16[96,512]{1,0:T(8,128)(2,1)S(1)} %get-tuple-element.48), channel_id=1, source_target_pairs={{0,2},{1,3},{2,0},{3,1},{4,6},{5,7},{6,4},{7,5},{8,10},{9,11},{10,... | collective-permute-start | bytes 294920 | tf_op jit(solution)/shard_map/ppermute | solution.py:646
  53.1 7.5 %collective-permute-start.12 = (bf16[96,512]{1,0:T(8,128)(2,1)S(1)}, bf16[96,512]{1,0:T(8,128)(2,1)S(1)}, u32[]{:S(2)}, u32[]{:S(2)}) collective-permute-start(bf16[96,512]{1,0:T(8,128)(2,1)S(1)} %get-tuple-element.49), channel_id=1, source_target_pairs={{0,3},{1,2},{2,1},{3,0},{4,7},{5,6},{6,5},{7,4},{8,11},{9,10},{10,... | collective-permute-start | bytes 294920 | tf_op jit(solution)/shard_map/ppermute | solution.py:646
  55.5 1.3 %collective-permute-start.16 = (bf16[32,512]{1,0:T(8,128)(2,1)S(1)}, bf16[32,512]{1,0:T(8,128)(2,1)S(1)}, u32[]{:S(2)}, u32[]{:S(2)}) collective-permute-start(bf16[32,512]{1,0:T(8,128)(2,1)S(1)} %get-tuple-element.56), channel_id=1, source_target_pairs={{0,1},{1,0},{2,3},{3,2},{4,5},{5,4},{6,7},{7,6},{8,9},{9,8},{10,11... | collective-permute-start | bytes 98312 | tf_op jit(solution)/shard_map/ppermute | solution.py:646
  55.7 3.7 %collective-permute-start.17 = (bf16[32,512]{1,0:T(8,128)(2,1)S(1)}, bf16[32,512]{1,0:T(8,128)(2,1)S(1)}, u32[]{:S(2)}, u32[]{:S(2)}) collective-permute-start(bf16[32,512]{1,0:T(8,128)(2,1)S(1)} %get-tuple-element.57), channel_id=1, source_target_pairs={{0,2},{1,3},{2,0},{3,1},{4,6},{5,7},{6,4},{7,5},{8,10},{9,11},{10,... | collective-permute-start | bytes 98312 | tf_op jit(solution)/shard_map/ppermute | solution.py:646
  56.8 3.9 %collective-permute-start.18 = (bf16[32,512]{1,0:T(8,128)(2,1)S(1)}, bf16[32,512]{1,0:T(8,128)(2,1)S(1)}, u32[]{:S(2)}, u32[]{:S(2)}) collective-permute-start(bf16[32,512]{1,0:T(8,128)(2,1)S(1)} %get-tuple-element.58), channel_id=1, source_target_pairs={{0,3},{1,2},{2,1},{3,0},{4,7},{5,6},{6,5},{7,4},{8,11},{9,10},{10,... | collective-permute-start | bytes 98312 | tf_op jit(solution)/shard_map/ppermute | solution.py:646

commit v6 on v5

--- a/solution.py
+++ b/solution.py
@@ -215,13 +215,6 @@
         part = block_of(axes[1], held[8].shape[1])
         views += [ref.at[:, part] for ref in sources[8:11]]
     copies = fetch(views, held, sems)
-    if count:
-        half = sources[-1].at[block_of(axes[0], outs[6].shape[0])]
-        wide = sources[11].shape[1]
-        targets = [outs[3].at[:, i * wide : (i + 1) * wide] for i in range(count)]
-        copies += fetch(
-            [half] + list(sources[11:-1]), [outs[6]] + targets, sems.at[pl.ds(11, count + 1)]
-        )
     for copy in copies[:5]:
         copy.wait()
     heads = width // size
@@ -243,6 +236,13 @@
     inv = [lax.rsqrt(raw[t, t] + EPS) for t in range(steps)]
 
     copies[5].wait()
+    if count:
+        half = sources[-1].at[block_of(axes[0], outs[6].shape[0])]
+        wide = sources[11].shape[1]
+        targets = [outs[3].at[:, i * wide : (i + 1) * wide] for i in range(count)]
+        copies += fetch(
+            [half] + list(sources[11:-1]), [outs[6]] + targets, sems.at[pl.ds(11, count + 1)]
+        )
 
     def read(s, carry):
         kb = kscr[pl.ds(s * heads * steps, heads * steps), :][:, :size].astype(BF16)
@@ -250,7 +250,7 @@
         put_rows(pscr, s * 8, 8, seen)
         return carry
 
-    lax.fori_loop(0, seqs, read, 0, unroll=8)
+    lax.fori_loop(0, seqs, read, 0, unroll=min(seqs, 32))
     highest = lax.Precision.HIGHEST
     cumul, solved = [], []
     for t in range(steps):
@@ -278,7 +278,7 @@
         low_ref[s] = new.astype(BF16)
         return carry
 
-    lax.fori_loop(0, seqs, write, 0, unroll=8)
+    lax.fori_loop(0, seqs, write, 0, unroll=min(seqs, 32))
     for copy in copies[6:]:
         copy.wait()
     if count:
@@ -439,7 +439,7 @@
         put_rows(pscr, s * 8, 8, jnp.where(upper, from_query, from_key))
         return carry
 
-    lax.fori_loop(0, seqs, read, 0, unroll=8)
+    lax.fori_loop(0, seqs, read, 0, unroll=seqs)
     value, gate = column(2), column(3)
     cumul, solved, outs = [], [], []
     for t in range(steps):

time: 61.6 us -> 65.1 us (1.057)
  starting transfers between devices: 23.7 us -> 28.3 us
  Pallas kernels: 12.2 us -> 10.8 us
    ppermute x9, starting transfers between devices: 11.7 us -> 16.3 us  [swap(): return lax.ppermute(array, 'kv', [(i, i ^ bit) for i in range(n)])]
    pallas_call x1, Pallas kernels: 5.4 us -> 4.46 us  [early(): pl.pallas_call(functools.partial(early_kernel, steps, size, axes, count),...]
  transfers between devices with their start and end apart: 19 -> 19, of which waited for: 6 -> 6; matrix products, arithmetic and copies ran while one was open for 0% -> 0% of each run, Pallas kernels for 18% -> 15%
where the time goes in v6:
time: 65.1 us; the launch traced here: 64.9 us
  starting transfers between devices  28.3 us (43%)
  waiting for transfers between devices  17.5 us (27%)
  Pallas kernels  10.8 us (17%)
  blocking collectives  7.45 us (11%)
  between operations  0.73 us (1%)
    ppermute x9, starting transfers between devices, swap(): return lax.ppermute(array, 'kv', [(i, i ^ bit) for i in range(n)])  16.3 us
    ppermute x9, waiting for transfers between devices, swap(): return lax.ppermute(array, 'kv', [(i, i ^ bit) for i in range(n)])  11.4 us
    all_gather x1, blocking collectives, layer(): gathered = lax.all_gather(turned, 'tp')  7.45 us
    ppermute x6, starting transfers between devices, layer(): lax.ppermute(out[s], 'tp', [(i, i ^ s) for i in range(n_tp)])  6.68 us
    pallas_call x1, Pallas kernels, early(): pl.pallas_call(functools.partial(early_kernel, steps, size, axes, count),...  4.46 us
    ppermute x6, waiting for transfers between devices, layer(): lax.ppermute(out[s], 'tp', [(i, i ^ s) for i in range(n_tp)])  3.43 us
    pallas_call x2, Pallas kernels, propose(): pl.pallas_call(functools.partial(propose_kernel, dims, axis, spans, first...  2.79 us
    ppermute x3, starting transfers between devices, layer(): other = lax.ppermute(halves[i], 'grp', ring(n_grp, 1))  2.77 us
  transfers between devices with their start and end apart: 19, of which 6 were waited for; matrix products, arithmetic and copies ran while one was open for 0% of the time, Pallas kernels for 15%

profile of v6, /device:TPU:9, one launch (start us, length us, event | category | flops | bytes accessed | tf_op | source)
XLA Modules:
  0.0 64.9 jit_solution(11714468059955140484)
XLA Ops:
  0.6 2.6 %collective-permute-start.2 = (bf16[32,4,512]{2,1,0:T(4,128)(2,1)}, bf16[32,4,512]{2,1,0:T(4,128)(2,1)S(1)}, u32[]{:S(2)}, u32[]{:S(2)}) collective-permute-start(bf16[32,4,512]{2,1,0:T(4,128)(2,1)} %param.17), channel_id=1, source_target_pairs={{0,0},{1,5},{2,10},{3,15},{4,1},{5,4},{6,11},{7,14},{8,2},{9,7},{1... | collective-permute-start | bytes 393224 | tf_op jit(solution)/shard_map/ppermute | solution.py:572
  3.2 4.5 %early.1 = (f32[32,64,256]{2,1,0:T(8,128)}, bf16[32,64,256]{2,1,0:T(8,128)(2,1)S(1)}, f32[8,256]{1,0:T(8,128)S(1)}, bf16[512,1024]{1,0:T(8,128)(2,1)S(1)}, f32[8...) custom-call(bf16[32,4,256]{2,1,0:T(4,128)(2,1)} %refs_0_.2, ...), custom_call_target="tpu_custom_call" | custom-call | flops 128000000 | bytes 4194304 | tf_op jit(solution)/shard_map/early/pallas_call | solution.py:340
  7.7 3.2 %collective-permute-start = (bf16[128,512]{1,0:T(8,128)(2,1)S(1)}, bf16[128,512]{1,0:T(8,128)(2,1)S(1)}, u32[]{:S(2)}, u32[]{:S(2)}) collective-permute-start(bf16[128,512]{1,0:T(8,128)(2,1)S(1)} %get-tuple-element.33), channel_id=1, source_target_pairs={{0,8},{4,12},{8,0},{12,4},{1,9},{5,13},{9,1},{13,5},{2,10},{6,14},... | collective-permute-start | bytes 393224 | tf_op jit(solution)/shard_map/ppermute | solution.py:581
  10.9 0.0 collective-permute-start.1
  10.9 0.0 collective-permute-done.2
  10.9 7.4 %all-gather = bf16[128,4,512]{2,1,0:T(4,128)(2,1)S(1)} all-gather(bf16[32,4,512]{2,1,0:T(4,128)(2,1)S(1)} %collective-permute-done.2), channel_id=2, replica_groups=mesh['grp'=2,'kv'=4,'tp'=4] {'tp'}, dimensions={0}, use_global_device_ids=true | all-gather | bytes 655360 | tf_op jit(solution)/shard_map/all_gather | solution.py:587
  18.4 0.0 copy-start
  18.4 1.1 %shard_map.176 = (f32[104,1024]{1,0:T(8,128)S(1)}, bf16[104,1024]{1,0:T(8,128)(2,1)S(1)}, bf16[104,1024]{1,0:T(8,128)(2,1)S(1)}, f32[32,1024]{1,0:T(8,128)S(1)},...) custom-call(bf16[4,32,4,512]{3,2,1,0:T(4,128)(2,1)S(1)} %bitcast.9, f32[8,512]{1,0:T(8,128)S(1)} %get-tuple-element.36.gain_ref, ...), custom_call_target="tpu_custom_call" | custom-call | flops 536870912 | bytes 1048576 | tf_op jit(solution)/shard_map/pallas_call | solution.py:126
  19.5 0.0 collective-permute-done.refs_1_
  19.6 0.0 collective-permute-done.1.refs_3_
  19.6 1.3 %collective-permute-start.6 = (bf16[128,512]{1,0:T(8,128)(2,1)S(1)}, bf16[128,512]{1,0:T(8,128)(2,1)S(1)}, u32[]{:S(2)}, u32[]{:S(2)}) collective-permute-start(bf16[128,512]{1,0:T(8,128)(2,1)S(1)} %collective-permute-done.refs_1_), channel_id=1, source_target_pairs={{0,16},{16,0},{1,17},{17,1},{2,18},{18,2},{3,19},{19,3},{4,20},{20... | collective-permute-start | bytes 393224 | tf_op jit(solution)/shard_map/ppermute | solution.py:612
  20.9 6.1 %collective-permute-start.8 = (bf16[128,512]{1,0:T(8,128)(2,1)S(1)}, bf16[128,512]{1,0:T(8,128)(2,1)S(1)}, u32[]{:S(2)}, u32[]{:S(2)}) collective-permute-start(bf16[128,512]{1,0:T(8,128)(2,1)S(1)} %collective-permute-done.refs_1_), channel_id=1, source_target_pairs={{0,4},{4,0},{8,12},{12,8},{1,5},{5,1},{9,13},{13,9},{2,6},{6,2},{1... | collective-permute-start | bytes 393224 | tf_op jit(solution)/shard_map/ppermute | solution.py:581
  26.9 0.0 collective-permute-start.3
  26.9 0.5 shard_map.177
  27.4 0.1 collective-permute-start.4
  27.5 2.6 %collective-permute-start.5 = (bf16[104,1024]{1,0:T(8,128)(2,1)S(1)}, bf16[104,1024]{1,0:T(8,128)(2,1)S(1)}, u32[]{:S(2)}, u32[]{:S(2)}) collective-permute-start(bf16[104,1024]{1,0:T(8,128)(2,1)S(1)} %get-tuple-element.43), channel_id=1, source_target_pairs={{0,12},{4,8},{8,4},{12,0},{1,13},{5,9},{9,5},{13,1},{2,14},{6,10},... | collective-permute-start | bytes 638984 | tf_op jit(solution)/shard_map/ppermute | solution.py:581
  30.1 0.0 collective-permute-done.6.refs_2_
  30.1 0.2 collective-permute-start.7
  30.4 0.0 collective-permute-done.8.refs_5_
  30.4 1.2 %collective-permute-start.9 = (bf16[128,512]{1,0:T(8,128)(2,1)S(1)}, bf16[128,512]{1,0:T(8,128)(2,1)S(1)}, u32[]{:S(2)}, u32[]{:S(2)}) collective-permute-start(bf16[128,512]{1,0:T(8,128)(2,1)S(1)} %collective-permute-done.8.refs_5_), channel_id=1, source_target_pairs={{0,16},{16,0},{1,17},{17,1},{2,18},{18,2},{3,19},{19,3},{4,20},{20... | collective-permute-start | bytes 393224 | tf_op jit(solution)/shard_map/ppermute | solution.py:612
  31.6 2.6 %collective-permute-done.7.refs_4_ = bf16[128,512]{1,0:T(8,128)(2,1)S(1)} collective-permute-done((bf16[128,512]{1,0:T(8,128)(2,1)S(1)}, bf16[128,512]{1,0:T(8,128)(2,1)S(1)}, u32[]{:S(2)}, u32[]{:S(2)}) %collective-permute-start.7) | collective-permute-done | bytes 131104 | tf_op jit(solution)/shard_map/ppermute | solution.py:612
  34.3 0.9 %collective-permute-start.13 = (bf16[32,1024]{1,0:T(8,128)(2,1)S(1)}, bf16[32,1024]{1,0:T(8,128)(2,1)S(1)}, u32[]{:S(2)}, u32[]{:S(2)}) collective-permute-start(bf16[32,1024]{1,0:T(8,128)(2,1)S(1)} %get-tuple-element.51), channel_id=1, source_target_pairs={{0,4},{4,0},{8,12},{12,8},{1,5},{5,1},{9,13},{13,9},{2,6},{6,2},{1... | collective-permute-start | bytes 196616 | tf_op jit(solution)/shard_map/ppermute | solution.py:581
  35.2 1.4 %collective-permute-done.3.refs_1_ = bf16[104,1024]{1,0:T(8,128)(2,1)S(1)} collective-permute-done((bf16[104,1024]{1,0:T(8,128)(2,1)S(1)}, bf16[104,1024]{1,0:T(8,128)(2,1)S(1)}, u32[]{:S(2)}, u32[]{:S(2)}) %collective-permute-start.3) | collective-permute-done | bytes 213024 | tf_op jit(solution)/shard_map/ppermute | solution.py:581
  36.6 1.3 %collective-permute-start.14 = (bf16[32,1024]{1,0:T(8,128)(2,1)S(1)}, bf16[32,1024]{1,0:T(8,128)(2,1)S(1)}, u32[]{:S(2)}, u32[]{:S(2)}) collective-permute-start(bf16[32,1024]{1,0:T(8,128)(2,1)S(1)} %get-tuple-element.52), channel_id=1, source_target_pairs={{0,8},{4,12},{8,0},{12,4},{1,9},{5,13},{9,1},{13,5},{2,10},{6,14},... | collective-permute-start | bytes 196616 | tf_op jit(solution)/shard_map/ppermute | solution.py:581
  37.9 0.0 collective-permute-done.9.refs_6_
  38.0 2.1 %collective-permute-start.15 = (bf16[32,1024]{1,0:T(8,128)(2,1)S(1)}, bf16[32,1024]{1,0:T(8,128)(2,1)S(1)}, u32[]{:S(2)}, u32[]{:S(2)}) collective-permute-start(bf16[32,1024]{1,0:T(8,128)(2,1)S(1)} %get-tuple-element.53), channel_id=1, source_target_pairs={{0,12},{4,8},{8,4},{12,0},{1,13},{5,9},{9,5},{13,1},{2,14},{6,10},... | collective-permute-start | bytes 196616 | tf_op jit(solution)/shard_map/ppermute | solution.py:581
  40.0 0.0 copy-done
  40.0 1.1 %assemble.1.refs_4_ = bf16[4,256,512]{2,1,0:T(8,128)(2,1)S(1)} custom-call(bf16[256,512]{1,0:T(8,128)(2,1)S(1)} %copy-done, bf16[128,512]{1,0:T(8,128)(2,1)S(1)} %collective-permute-done.refs_1_, bf16[128,512]{1,0:T(8,128)(2,1)S(1)} %collective-permute-done.6.refs_2_, bf16[128,512]{1,0:T(8,128)(2,1)S(1)} %collective-permute-done.1.refs_3_, ...), custom_call_target="tpu_custom_call" | custom-call | flops 4000000 | bytes 1048576 | tf_op jit(solution)/shard_map/assemble/pallas_call | solution.py:154
  41.1 0.0 collective-permute-done.4.refs_2_
  41.1 10.0 %collective-permute-done.5.refs_3_ = bf16[104,1024]{1,0:T(8,128)(2,1)S(1)} collective-permute-done((bf16[104,1024]{1,0:T(8,128)(2,1)S(1)}, bf16[104,1024]{1,0:T(8,128)(2,1)S(1)}, u32[]{:S(2)}, u32[]{:S(2)}) %collective-permute-start.5) | collective-permute-done | bytes 213024 | tf_op jit(solution)/shard_map/ppermute | solution.py:581
  51.1 1.6 %propose.2 = (f32[96,512]{1,0:T(8,128)S(1)}, bf16[96,512]{1,0:T(8,128)(2,1)S(1)}, bf16[96,512]{1,0:T(8,128)(2,1)S(1)}, bf16[96,512]{1,0:T(8,128)(2,1)S(1)}, f32[8,1024]{1,0:T(8,128)S(1)}) custom-call(f32[8,256]{1,0:T(8,128)S(1)} %get-tuple-element.31.const_ref, bf16[32,64,256]{2,1,0:T(8,128)(2,1)S(1)} %get-tuple-element.32.s_ref, ...), custom_call_target="tpu_custom_call" | custom-call | flops 96000000 | bytes 2097152 | tf_op jit(solution)/shard_map/propose/pallas_call | solution.py:482
  52.7 3.3 %collective-permute-start.10 = (bf16[96,512]{1,0:T(8,128)(2,1)S(1)}, bf16[96,512]{1,0:T(8,128)(2,1)S(1)}, u32[]{:S(2)}, u32[]{:S(2)}) collective-permute-start(bf16[96,512]{1,0:T(8,128)(2,1)S(1)} %get-tuple-element.47), channel_id=1, source_target_pairs={{0,1},{1,0},{2,3},{3,2},{4,5},{5,4},{6,7},{7,6},{8,9},{9,8},{10,11... | collective-permute-start | bytes 294920 | tf_op jit(solution)/shard_map/ppermute | solution.py:646
  56.0 0.5 collective-permute-start.11
  56.5 0.0 collective-permute-done.13.refs_1_
  56.5 1.2 %collective-permute-start.12 = (bf16[96,512]{1,0:T(8,128)(2,1)S(1)}, bf16[96,512]{1,0:T(8,128)(2,1)S(1)}, u32[]{:S(2)}, u32[]{:S(2)}) collective-permute-start(bf16[96,512]{1,0:T(8,128)(2,1)S(1)} %get-tuple-element.49), channel_id=1, source_target_pairs={{0,3},{1,2},{2,1},{3,0},{4,7},{5,6},{6,5},{7,4},{8,11},{9,10},{10,... | collective-permute-start | bytes 294920 | tf_op jit(solution)/shard_map/ppermute | solution.py:646
  57.7 0.0 collective-permute-done.14.refs_2_
  57.7 0.0 collective-permute-done.15.refs_3_
  57.7 1.2 %propose.3 = (f32[32,512]{1,0:T(8,128)S(1)}, bf16[32,512]{1,0:T(8,128)(2,1)S(1)}, bf16[32,512]{1,0:T(8,128)(2,1)S(1)}, bf16[32,512]{1,0:T(8,128)(2,1)S(1)}) custom-call(f32[8,256]{1,0:T(8,128)S(1)} %get-tuple-element.31.const_ref, bf16[32,64,256]{2,1,0:T(8,128)(2,1)S(1)} %get-tuple-element.32.s_ref, f32[32,1024]{1,0:T(8,128)S(1)} %get-tuple-element.50.refs_0_, ...), custom_call_target="tpu_custom_call" | custom-call | flops 32000000 | bytes 2097152 | tf_op jit(solution)/shard_map/propose/pallas_call | solution.py:482
  58.9 0.2 collective-permute-start.16
  59.1 0.5 collective-permute-start.17
  59.7 0.5 collective-permute-done.16.refs_5_
  60.2 0.9 %collective-permute-start.18 = (bf16[32,512]{1,0:T(8,128)(2,1)S(1)}, bf16[32,512]{1,0:T(8,128)(2,1)S(1)}, u32[]{:S(2)}, u32[]{:S(2)}) collective-permute-start(bf16[32,512]{1,0:T(8,128)(2,1)S(1)} %get-tuple-element.58), channel_id=1, source_target_pairs={{0,3},{1,2},{2,1},{3,0},{4,7},{5,6},{6,5},{7,4},{8,11},{9,10},{10,... | collective-permute-start | bytes 98312 | tf_op jit(solution)/shard_map/ppermute | solution.py:646
  61.1 1.7 %collective-permute-done.17.refs_6_ = bf16[32,512]{1,0:T(8,128)(2,1)S(1)} collective-permute-done((bf16[32,512]{1,0:T(8,128)(2,1)S(1)}, bf16[32,512]{1,0:T(8,128)(2,1)S(1)}, u32[]{:S(2)}, u32[]{:S(2)}) %collective-permute-start.17) | collective-permute-done | bytes 32800 | tf_op jit(solution)/shard_map/ppermute | solution.py:646
  62.8 1.2 %collective-permute-done.18.refs_7_ = bf16[32,512]{1,0:T(8,128)(2,1)S(1)} collective-permute-done((bf16[32,512]{1,0:T(8,128)(2,1)S(1)}, bf16[32,512]{1,0:T(8,128)(2,1)S(1)}, u32[]{:S(2)}, u32[]{:S(2)}) %collective-permute-start.18) | collective-permute-done | bytes 32800 | tf_op jit(solution)/shard_map/ppermute | solution.py:646
  64.0 0.0 collective-permute-done.10.refs_1_
  64.0 0.0 collective-permute-done.11.refs_2_
  64.0 0.0 collective-permute-done.12.refs_3_
  64.0 0.8 %finish.1 = bf16[32,4,512]{2,1,0:T(4,128)(2,1)} custom-call(f32[96,512]{1,0:T(8,128)S(1)} %get-tuple-element.46.refs_0_, bf16[96,512]{1,0:T(8,128)(2,1)S(1)} %collective-permute-done.10.refs_1_, bf16[96,512]{1,0:T(8,128)(2,1)S(1)} %collective-permute-done.11.refs_2_, bf16[96,512]{1,0:T(8,128)(2,1)S(1)} %collective-permute-done.12.refs_3_, ...), custom_call_target="tpu_custom_call" | custom-call | tf_op jit(solution)/shard_map/finish/pallas_call | solution.py:514
Async XLA Ops:
  0.6 10.3 %collective-permute-start.2 = (bf16[32,4,512]{2,1,0:T(4,128)(2,1)}, bf16[32,4,512]{2,1,0:T(4,128)(2,1)S(1)}, u32[]{:S(2)}, u32[]{:S(2)}) collective-permute-start(bf16[32,4,512]{2,1,0:T(4,128)(2,1)} %param.17), channel_id=1, source_target_pairs={{0,0},{1,5},{2,10},{3,15},{4,1},{5,4},{6,11},{7,14},{8,2},{9,7},{1... | collective-permute-start | bytes 393224 | tf_op jit(solution)/shard_map/ppermute | solution.py:572
  7.7 11.9 %collective-permute-start = (bf16[128,512]{1,0:T(8,128)(2,1)S(1)}, bf16[128,512]{1,0:T(8,128)(2,1)S(1)}, u32[]{:S(2)}, u32[]{:S(2)}) collective-permute-start(bf16[128,512]{1,0:T(8,128)(2,1)S(1)} %get-tuple-element.33), channel_id=1, source_target_pairs={{0,8},{4,12},{8,0},{12,4},{1,9},{5,13},{9,1},{13,5},{2,10},{6,14},... | collective-permute-start | bytes 393224 | tf_op jit(solution)/shard_map/ppermute | solution.py:581
  10.9 8.6 %collective-permute-start.1 = (bf16[128,512]{1,0:T(8,128)(2,1)S(1)}, bf16[128,512]{1,0:T(8,128)(2,1)S(1)}, u32[]{:S(2)}, u32[]{:S(2)}) collective-permute-start(bf16[128,512]{1,0:T(8,128)(2,1)S(1)} %get-tuple-element.33), channel_id=1, source_target_pairs={{0,4},{4,0},{8,12},{12,8},{1,5},{5,1},{9,13},{13,9},{2,6},{6,2},{1... | collective-permute-start | bytes 393224 | tf_op jit(solution)/shard_map/ppermute | solution.py:581
  18.4 21.6 %copy-start = (bf16[256,512]{1,0:T(8,128)(2,1)S(1)}, bf16[256,512]{1,0:T(8,128)(2,1)}, u32[]{:S(2)}) copy-start(bf16[256,512]{1,0:T(8,128)(2,1)} %refs_0_.3) | copy-start | bytes 786436
  19.6 10.6 %collective-permute-start.6 = (bf16[128,512]{1,0:T(8,128)(2,1)S(1)}, bf16[128,512]{1,0:T(8,128)(2,1)S(1)}, u32[]{:S(2)}, u32[]{:S(2)}) collective-permute-start(bf16[128,512]{1,0:T(8,128)(2,1)S(1)} %collective-permute-done.refs_1_), channel_id=1, source_target_pairs={{0,16},{16,0},{1,17},{17,1},{2,18},{18,2},{3,19},{19,3},{4,20},{20... | collective-permute-start | bytes 393224 | tf_op jit(solution)/shard_map/ppermute | solution.py:612
  20.9 9.5 %collective-permute-start.8 = (bf16[128,512]{1,0:T(8,128)(2,1)S(1)}, bf16[128,512]{1,0:T(8,128)(2,1)S(1)}, u32[]{:S(2)}, u32[]{:S(2)}) collective-permute-start(bf16[128,512]{1,0:T(8,128)(2,1)S(1)} %collective-permute-done.refs_1_), channel_id=1, source_target_pairs={{0,4},{4,0},{8,12},{12,8},{1,5},{5,1},{9,13},{13,9},{2,6},{6,2},{1... | collective-permute-start | bytes 393224 | tf_op jit(solution)/shard_map/ppermute | solution.py:581
  26.9 9.7 %collective-permute-start.3 = (bf16[104,1024]{1,0:T(8,128)(2,1)S(1)}, bf16[104,1024]{1,0:T(8,128)(2,1)S(1)}, u32[]{:S(2)}, u32[]{:S(2)}) collective-permute-start(bf16[104,1024]{1,0:T(8,128)(2,1)S(1)} %get-tuple-element.41), channel_id=1, source_target_pairs={{0,4},{4,0},{8,12},{12,8},{1,5},{5,1},{9,13},{13,9},{2,6},{6,2},{1... | collective-permute-start | bytes 638984 | tf_op jit(solution)/shard_map/ppermute | solution.py:581
  27.4 13.7 %collective-permute-start.4 = (bf16[104,1024]{1,0:T(8,128)(2,1)S(1)}, bf16[104,1024]{1,0:T(8,128)(2,1)S(1)}, u32[]{:S(2)}, u32[]{:S(2)}) collective-permute-start(bf16[104,1024]{1,0:T(8,128)(2,1)S(1)} %get-tuple-element.42), channel_id=1, source_target_pairs={{0,8},{4,12},{8,0},{12,4},{1,9},{5,13},{9,1},{13,5},{2,10},{6,14},... | collective-permute-start | bytes 638984 | tf_op jit(solution)/shard_map/ppermute | solution.py:581
  27.5 23.6 %collective-permute-start.5 = (bf16[104,1024]{1,0:T(8,128)(2,1)S(1)}, bf16[104,1024]{1,0:T(8,128)(2,1)S(1)}, u32[]{:S(2)}, u32[]{:S(2)}) collective-permute-start(bf16[104,1024]{1,0:T(8,128)(2,1)S(1)} %get-tuple-element.43), channel_id=1, source_target_pairs={{0,12},{4,8},{8,4},{12,0},{1,13},{5,9},{9,5},{13,1},{2,14},{6,10},... | collective-permute-start | bytes 638984 | tf_op jit(solution)/shard_map/ppermute | solution.py:581
  30.1 4.1 %collective-permute-start.7 = (bf16[128,512]{1,0:T(8,128)(2,1)S(1)}, bf16[128,512]{1,0:T(8,128)(2,1)S(1)}, u32[]{:S(2)}, u32[]{:S(2)}) collective-permute-start(bf16[128,512]{1,0:T(8,128)(2,1)S(1)} %collective-permute-done.1.refs_3_), channel_id=1, source_target_pairs={{0,16},{16,0},{1,17},{17,1},{2,18},{18,2},{3,19},{19,3},{4,20},{20... | collective-permute-start | bytes 393224 | tf_op jit(solution)/shard_map/ppermute | solution.py:612
  30.4 7.6 %collective-permute-start.9 = (bf16[128,512]{1,0:T(8,128)(2,1)S(1)}, bf16[128,512]{1,0:T(8,128)(2,1)S(1)}, u32[]{:S(2)}, u32[]{:S(2)}) collective-permute-start(bf16[128,512]{1,0:T(8,128)(2,1)S(1)} %collective-permute-done.8.refs_5_), channel_id=1, source_target_pairs={{0,16},{16,0},{1,17},{17,1},{2,18},{18,2},{3,19},{19,3},{4,20},{20... | collective-permute-start | bytes 393224 | tf_op jit(solution)/shard_map/ppermute | solution.py:612
  34.3 22.3 %collective-permute-start.13 = (bf16[32,1024]{1,0:T(8,128)(2,1)S(1)}, bf16[32,1024]{1,0:T(8,128)(2,1)S(1)}, u32[]{:S(2)}, u32[]{:S(2)}) collective-permute-start(bf16[32,1024]{1,0:T(8,128)(2,1)S(1)} %get-tuple-element.51), channel_id=1, source_target_pairs={{0,4},{4,0},{8,12},{12,8},{1,5},{5,1},{9,13},{13,9},{2,6},{6,2},{1... | collective-permute-start | bytes 196616 | tf_op jit(solution)/shard_map/ppermute | solution.py:581
  36.6 21.1 %collective-permute-start.14 = (bf16[32,1024]{1,0:T(8,128)(2,1)S(1)}, bf16[32,1024]{1,0:T(8,128)(2,1)S(1)}, u32[]{:S(2)}, u32[]{:S(2)}) collective-permute-start(bf16[32,1024]{1,0:T(8,128)(2,1)S(1)} %get-tuple-element.52), channel_id=1, source_target_pairs={{0,8},{4,12},{8,0},{12,4},{1,9},{5,13},{9,1},{13,5},{2,10},{6,14},... | collective-permute-start | bytes 196616 | tf_op jit(solution)/shard_map/ppermute | solution.py:581
  38.0 19.8 %collective-permute-start.15 = (bf16[32,1024]{1,0:T(8,128)(2,1)S(1)}, bf16[32,1024]{1,0:T(8,128)(2,1)S(1)}, u32[]{:S(2)}, u32[]{:S(2)}) collective-permute-start(bf16[32,1024]{1,0:T(8,128)(2,1)S(1)} %get-tuple-element.53), channel_id=1, source_target_pairs={{0,12},{4,8},{8,4},{12,0},{1,13},{5,9},{9,5},{13,1},{2,14},{6,10},... | collective-permute-start | bytes 196616 | tf_op jit(solution)/shard_map/ppermute | solution.py:581
  52.7 11.3 %collective-permute-start.10 = (bf16[96,512]{1,0:T(8,128)(2,1)S(1)}, bf16[96,512]{1,0:T(8,128)(2,1)S(1)}, u32[]{:S(2)}, u32[]{:S(2)}) collective-permute-start(bf16[96,512]{1,0:T(8,128)(2,1)S(1)} %get-tuple-element.47), channel_id=1, source_target_pairs={{0,1},{1,0},{2,3},{3,2},{4,5},{5,4},{6,7},{7,6},{8,9},{9,8},{10,11... | collective-permute-start | bytes 294920 | tf_op jit(solution)/shard_map/ppermute | solution.py:646
  56.0 8.0 %collective-permute-start.11 = (bf16[96,512]{1,0:T(8,128)(2,1)S(1)}, bf16[96,512]{1,0:T(8,128)(2,1)S(1)}, u32[]{:S(2)}, u32[]{:S(2)}) collective-permute-start(bf16[96,512]{1,0:T(8,128)(2,1)S(1)} %get-tuple-element.48), channel_id=1, source_target_pairs={{0,2},{1,3},{2,0},{3,1},{4,6},{5,7},{6,4},{7,5},{8,10},{9,11},{10,... | collective-permute-start | bytes 294920 | tf_op jit(solution)/shard_map/ppermute | solution.py:646
  56.5 7.5 %collective-permute-start.12 = (bf16[96,512]{1,0:T(8,128)(2,1)S(1)}, bf16[96,512]{1,0:T(8,128)(2,1)S(1)}, u32[]{:S(2)}, u32[]{:S(2)}) collective-permute-start(bf16[96,512]{1,0:T(8,128)(2,1)S(1)} %get-tuple-element.49), channel_id=1, source_target_pairs={{0,3},{1,2},{2,1},{3,0},{4,7},{5,6},{6,5},{7,4},{8,11},{9,10},{10,... | collective-permute-start | bytes 294920 | tf_op jit(solution)/shard_map/ppermute | solution.py:646
  58.9 1.3 %collective-permute-start.16 = (bf16[32,512]{1,0:T(8,128)(2,1)S(1)}, bf16[32,512]{1,0:T(8,128)(2,1)S(1)}, u32[]{:S(2)}, u32[]{:S(2)}) collective-permute-start(bf16[32,512]{1,0:T(8,128)(2,1)S(1)} %get-tuple-element.56), channel_id=1, source_target_pairs={{0,1},{1,0},{2,3},{3,2},{4,5},{5,4},{6,7},{7,6},{8,9},{9,8},{10,11... | collective-permute-start | bytes 98312 | tf_op jit(solution)/shard_map/ppermute | solution.py:646
  59.1 3.7 %collective-permute-start.17 = (bf16[32,512]{1,0:T(8,128)(2,1)S(1)}, bf16[32,512]{1,0:T(8,128)(2,1)S(1)}, u32[]{:S(2)}, u32[]{:S(2)}) collective-permute-start(bf16[32,512]{1,0:T(8,128)(2,1)S(1)} %get-tuple-element.57), channel_id=1, source_target_pairs={{0,2},{1,3},{2,0},{3,1},{4,6},{5,7},{6,4},{7,5},{8,10},{9,11},{10,... | collective-permute-start | bytes 98312 | tf_op jit(solution)/shard_map/ppermute | solution.py:646
  60.2 3.8 %collective-permute-start.18 = (bf16[32,512]{1,0:T(8,128)(2,1)S(1)}, bf16[32,512]{1,0:T(8,128)(2,1)S(1)}, u32[]{:S(2)}, u32[]{:S(2)}) collective-permute-start(bf16[32,512]{1,0:T(8,128)(2,1)S(1)} %get-tuple-element.58), channel_id=1, source_target_pairs={{0,3},{1,2},{2,1},{3,0},{4,7},{5,6},{6,5},{7,4},{8,11},{9,10},{10,... | collective-permute-start | bytes 98312 | tf_op jit(solution)/shard_map/ppermute | solution.py:646
